TPU v7x, 32 devices: a whole 2x2x4 slice. The times are simulated.
32 devices in a mesh: dp: 4 (over y, x), kv: 4 (over z), tp: 2 (over core).
Axes of the slice: x: 2, y: 2, z: 4, core: 2. Of those that a mesh axis runs over, the one named last changes fastest.
Arguments:
- tokens: bfloat16 [16, 4096], P('dp', 'kv'), parts along dimension 0, may hold values from -13 to 13
- norm_gain: float32 [4096], P('kv'), may hold values from 0.1 to 1.9
- query_weight: bfloat16 [4096, 2048], P('kv', 'tp'), may hold values from -0.09375 to 0.09375
- key_weight: bfloat16 [4096, 2048], P('kv', 'tp'), may hold values from -0.09375 to 0.09375
- value_weight: bfloat16 [4096, 4096], P('kv', 'tp'), may hold values from -0.09375 to 0.09375
- gate_weight: bfloat16 [4096, 2, 8], replicated, may hold values from -0.09375 to 0.09375
- forget_bias: float32 [8], P('tp'), may hold values from 0.5 to 4
- state_matrix: float32 [16, 8, 512, 256], P(('dp', 'kv'), 'tp'), parts along dimension 0, may hold values from -1.8 to 1.8
- state_normalizer: float32 [16, 8, 256], P(('dp', 'kv'), 'tp'), parts along dimension 0, may hold values from -1.2 to 1.2
- state_max: float32 [16, 8], P(('dp', 'kv'), 'tp'), parts along dimension 0, may hold values from -2 to 86
- block_keys: bfloat16 [16, 8, 64, 256], P(('dp', 'kv'), 'tp'), parts along dimension 0, may hold values from -5 to 5
- block_values: bfloat16 [16, 8, 64, 512], P(('dp', 'kv'), 'tp'), parts along dimension 0, may hold values from -5 to 5
- block_input: float32 [16, 8, 64], P(('dp', 'kv'), 'tp'), parts along dimension 0, may hold values from -4.5 to 86.5
- block_logf: float32 [16, 8, 64], P(('dp', 'kv'), 'tp'), parts along dimension 0, may hold values from -1 to 0
- lengths: int32 [16], P(('dp', 'kv')), parts along dimension 0, may hold values from 1 to 2048, 4096 in all
- out_weight: bfloat16 [4096, 4096], P('tp', 'kv'), may hold values from -0.09375 to 0.09375
- mixer_gain: float32 [4096], replicated, may hold values from 0.1 to 1.9
- up_weight: bfloat16 [8192, 4096], P(('kv', 'tp')), may hold values from -0.09375 to 0.09375
- down_weight: bfloat16 [8192, 4096], P(('kv', 'tp')), may hold values from -0.09375 to 0.09375
Outputs:
- mixed: bfloat16 [16, 4096], P('dp', ('kv', 'tp')), parts along dimension 0
There are 4 independent parts, one for each index of `dp`. A program takes and returns all parts, laid end to end along the dimension named above; an argument that names none is the same for every part. Nothing has to cross between parts.
Inputs may be any that keep to these rules, and one draw needn't show every extreme that they name: `lengths`: each sequence's count of earlier positions; the state holds the first multiple of 64 of them and the block arrays the rest.
All inputs are finite; a program needn't handle non-finite values.
Results may differ from a plain program's by a relative error of at most 0.016.
Values may be sent and summed in bfloat16 or wider, within the bound.
No kernel may reach another device: no remote copies, remote signals or barrier semaphores. Data moves between devices by JAX's collectives and lax.ppermute only.
A program may use at most 64 MiB of HBM per device.

v0:
```python
import jax
import jax.numpy as jnp
from jax import lax
from jax.experimental import pallas as pl
from jax.experimental.pallas import tpu as pltpu
from jax.sharding import PartitionSpec as P

D = 4096
DK = 256
DV = 512
SPAN_LOCATIONS = 64


epsilon = 1e-06
highest = lax.Precision.HIGHEST


def memory_cell(
    query,
    key,
    value,
    gates,
    forget_bias,
    state_matrix,
    state_normalizer,
    state_max,
    block_keys,
    block_values,
    block_input,
    block_logf,
    lengths,
):
    live = lengths % SPAN_LOCATIONS
    positions = lax.broadcasted_iota(jnp.int32, (1, 1, SPAN_LOCATIONS), 2)
    inside = positions < live[:, None, None]
    new_input = gates[:, 0]
    new_logf = jax.nn.log_sigmoid(gates[:, 1] + forget_bias)
    cumulative = jnp.cumsum(jnp.where(inside, block_logf, jnp.float32(0.0)), axis=2)
    total = cumulative[:, :, -1] + new_logf
    carried_log = total + state_max
    cache_log = jnp.where(inside, total[:, :, None] - cumulative + block_input, -jnp.inf)
    stable = jnp.maximum(jnp.maximum(carried_log, jnp.max(cache_log, axis=2)), new_input)
    carried_weight = jnp.exp(carried_log - stable)
    new_weight = jnp.exp(new_input - stable)
    cache_weight = jnp.exp(cache_log - stable[:, :, None])
    scores = jnp.einsum("bhk,bhsk->bhs", query, block_keys, preferred_element_type=jnp.float32)
    mixing = (scores * DK ** (-0.5) * cache_weight).astype(jnp.bfloat16)
    query_wide = query.astype(jnp.float32)
    own_term = jnp.sum(query_wide * key.astype(jnp.float32), axis=2) * DK ** (-0.5) * new_weight
    carried = jnp.einsum("bhvk,bhk->bhv", state_matrix, query_wide, precision=highest)
    from_cache = jnp.einsum(
        "bhs,bhsv->bhv", mixing, block_values, preferred_element_type=jnp.float32
    )
    numerator = (
        carried_weight[:, :, None] * carried
        + from_cache
        + own_term[:, :, None] * value.astype(jnp.float32)
    )
    normalizer = (
        carried_weight * jnp.sum(state_normalizer * query_wide, axis=2)
        + jnp.sum(mixing.astype(jnp.float32), axis=2)
        + own_term
    )
    divisor = jnp.maximum(jnp.maximum(jnp.abs(normalizer), jnp.exp(-stable)), jnp.float32(1.0))
    hidden = numerator / divisor[:, :, None]
    return hidden.astype(jnp.bfloat16)


def absorb_columns(mixer_gain, up_weight):

    def absorb(carry, piece, start):
        widened = piece.astype(jnp.float32)
        mixer_in = (widened * mixer_gain).astype(jnp.bfloat16)
        product = lax.dot_general(
            mixer_in, up_weight, (((1,), (1,)), ((), ())), preferred_element_type=jnp.float32
        )
        return (product, jnp.sum(widened * widened, axis=1))

    return absorb


def down_terms(carry, down_weight):
    accumulated, squares = carry
    scaled = accumulated * lax.rsqrt(squares / D + epsilon)[:, None]
    activated = jnp.square(jax.nn.relu(scaled)).astype(jnp.bfloat16)
    return jnp.dot(activated, down_weight, preferred_element_type=jnp.float32)


DIRECT_LIMIT = 8


def partner_pairs(size, distance):
    if size & (size - 1) == 0:
        return [(i, i ^ distance) for i in range(size)]
    return [(i, (i + distance) % size) for i in range(size)]


def partner_of(position, size, distance, receiving):
    if size & (size - 1) == 0:
        return position ^ distance
    return (position - distance) % size if receiving else (position + distance) % size


def gather_direct(piece, axis):
    size = lax.axis_size(axis)
    if size > DIRECT_LIMIT:
        return lax.all_gather(piece, axis, axis=0)
    position = lax.axis_index(axis)
    received = [piece] + [
        lax.ppermute(piece, axis, partner_pairs(size, d)) for d in range(1, size)
    ]
    stacked = jnp.stack(received)
    places = jnp.arange(size)
    if size & (size - 1) == 0:
        order = position ^ places
    else:
        order = (position - places) % size
    return stacked[order]


def scatter_sum_direct(parts, axis):
    size = lax.axis_size(axis)
    if size > DIRECT_LIMIT:
        return lax.psum_scatter(parts, axis, scatter_dimension=0, tiled=False)
    position = lax.axis_index(axis)

    def entry(index):
        return lax.dynamic_index_in_dim(parts, index, 0, keepdims=False)

    total = entry(position)
    for d in range(1, size):
        out = entry(partner_of(position, size, d, False))
        total = total + lax.ppermute(out, axis, partner_pairs(size, d))
    return total


def shards_general(
    tokens,
    norm_gain,
    query_weight,
    key_weight,
    value_weight,
    gate_weight,
    forget_bias,
    state_matrix,
    state_normalizer,
    state_max,
    block_keys,
    block_values,
    block_input,
    block_logf,
    lengths,
    out_weight,
    mixer_gain,
    up_weight,
    down_weight,
):
    position = lax.axis_index("kv")
    head_half = lax.axis_index("tp")
    columns = tokens.shape[1]
    local_heads = forget_bias.shape[0]
    local_rows = lengths.shape[0]
    widened = tokens.astype(jnp.float32)
    squares = jnp.sum(widened * widened, axis=1)
    normed = (widened * norm_gain).astype(jnp.bfloat16)
    gate_rows = lax.dynamic_slice_in_dim(gate_weight, position * columns, columns, 0)
    gate_rows = lax.dynamic_slice_in_dim(
        gate_rows, head_half * local_heads, local_heads, 2
    ).reshape(columns, 2 * local_heads)
    query_part = jnp.dot(normed, query_weight, preferred_element_type=jnp.float32)
    key_part = jnp.dot(normed, key_weight, preferred_element_type=jnp.float32)
    value_part = jnp.dot(normed, value_weight, preferred_element_type=jnp.float32)
    gate_part = jnp.dot(normed, gate_rows, preferred_element_type=jnp.float32)
    parts = jnp.concatenate(
        [query_part, key_part, value_part, gate_part, squares[:, None]], axis=1
    )
    parts = parts.reshape(-1, local_rows, parts.shape[1])
    sums = scatter_sum_direct(parts, "kv")
    q_end = query_part.shape[1]
    k_end = q_end + key_part.shape[1]
    v_end = k_end + value_part.shape[1]
    g_end = v_end + gate_part.shape[1]
    query_sum, key_sum, value_sum, gate_sum, own_squares = (
        sums[:, :q_end],
        sums[:, q_end:k_end],
        sums[:, k_end:v_end],
        sums[:, v_end:g_end],
        sums[:, g_end],
    )
    row_scale = lax.rsqrt(own_squares / D + epsilon)[:, None]
    query = (query_sum * row_scale).astype(jnp.bfloat16).reshape(local_rows, local_heads, DK)
    key = (key_sum * row_scale).astype(jnp.bfloat16).reshape(local_rows, local_heads, DK)
    value = (value_sum * row_scale).astype(jnp.bfloat16).reshape(local_rows, local_heads, DV)
    gates = (gate_sum * row_scale).reshape(local_rows, 2, local_heads)
    hidden = memory_cell(
        query,
        key,
        value,
        gates,
        forget_bias,
        state_matrix,
        state_normalizer,
        state_max,
        block_keys,
        block_values,
        block_input,
        block_logf,
        lengths,
    )
    hidden = hidden.reshape(local_rows, local_heads * DV)
    every_hidden = gather_direct(hidden, "kv").reshape(-1, hidden.shape[1])
    partial_out = jnp.dot(
        every_hidden, out_weight, preferred_element_type=jnp.float32
    ).astype(jnp.bfloat16)
    attended = jnp.sum(gather_direct(partial_out, "tp").astype(jnp.float32), axis=0)
    residual = (widened + attended).astype(jnp.bfloat16)
    absorb = absorb_columns(mixer_gain, up_weight)
    hidden_units = up_weight.shape[0]
    rows = residual.shape[0]
    initial = (jnp.zeros((rows, hidden_units), jnp.float32), jnp.zeros((rows,), jnp.float32))
    pieces = gather_direct(residual, "kv")
    whole = jnp.moveaxis(pieces, 0, 1).reshape(rows, -1)
    carry = absorb(initial, whole, jnp.int32(0))
    terms = down_terms(carry, down_weight)
    share = columns // lax.axis_size("tp")
    terms = terms.reshape(rows, -1, lax.axis_size("tp"), share)
    by_core = scatter_sum_direct(jnp.moveaxis(terms, 2, 0), "tp")
    mixed_terms = scatter_sum_direct(jnp.moveaxis(by_core, 1, 0), "kv")
    own_residual = lax.dynamic_slice_in_dim(residual, head_half * share, share, 1)
    return (own_residual.astype(jnp.float32) + mixed_terms).astype(jnp.bfloat16)


def dot_nt(left, right):
    return lax.dot_general(
        left, right, (((1,), (1,)), ((), ())), preferred_element_type=jnp.float32
    )


VMEM_SPEC = pl.BlockSpec(memory_space=pltpu.VMEM)
SMEM_SPEC = pl.BlockSpec(memory_space=pltpu.SMEM)
ANY_SPEC = pl.BlockSpec(memory_space=pl.ANY)


def call(body, outs, in_specs, args, scratch=(), limit=8, flops=20000000000, aliases=None):
    return pl.pallas_call(
        body,
        out_shape=outs,
        in_specs=in_specs,
        out_specs=[VMEM_SPEC] * len(outs),
        scratch_shapes=list(scratch),
        input_output_aliases=aliases or {},
        compiler_params=pltpu.CompilerParams(vmem_limit_bytes=limit << 20),
        cost_estimate=pl.CostEstimate(flops=flops, bytes_accessed=1000000, transcendentals=0),
    )(*args)


def resident(weight):
    return pltpu.with_memory_space_constraint(weight, pltpu.VMEM)


def streamed(weight):
    return pltpu.with_memory_space_constraint(weight, pltpu.HBM)


def struct(shape, kind):
    return jax.ShapeDtypeStruct(shape, kind)


LANES = 128


def project(tokens, norm_gain, query_weight, key_weight, value_weight, gate_weight):
    rows, columns = tokens.shape
    size = lax.axis_size("kv")
    weights = (query_weight, key_weight, value_weight)
    widths = [w.shape[1] for w in weights]
    starts = [sum(widths[:i]) for i in range(3)]
    width = sum(widths)
    gate_count = gate_weight.shape[1] * gate_weight.shape[2]
    gates = jnp.transpose(gate_weight, (1, 2, 0)).reshape(gate_count, -1)
    cuts = [0, columns]

    def body(tokens_hbm, gain_hbm, q_hbm, k_hbm, v_hbm, gate_hbm, *rest):
        outs = rest[:size]
        tokens_ref, gain_ref, weight_ref, gate_ref, sums_ref = rest[size : size + 5]
        sems, gate_sem, tokens_sem, gain_sem = rest[size + 5 :]
        position = lax.axis_index("kv")
        tokens_copy = pltpu.make_async_copy(tokens_hbm, tokens_ref, tokens_sem)
        gain_copy = pltpu.make_async_copy(gain_hbm, gain_ref, gain_sem)
        tokens_copy.start()
        gain_copy.start()
        copies = []
        for c in range(len(cuts) - 1):
            at = pl.ds(cuts[c], cuts[c + 1] - cuts[c])
            for w, source in enumerate((q_hbm, k_hbm, v_hbm)):
                copy = pltpu.make_async_copy(
                    source.at[at, :],
                    weight_ref.at[at, pl.ds(starts[w], widths[w])],
                    sems.at[c, w],
                )
                copy.start()
                copies.append(copy)
        gate_copy = pltpu.make_async_copy(
            gate_hbm.at[:, pl.ds(pl.multiple_of(position * columns, columns), columns)],
            gate_ref,
            gate_sem,
        )
        gate_copy.start()
        tokens_copy.wait()
        gain_copy.wait()
        widened = tokens_ref[...].astype(jnp.float32)
        squares = jnp.sum(widened * widened, axis=1, keepdims=True)
        normed = (widened * gain_ref[...]).astype(jnp.bfloat16)
        for c in range(len(cuts) - 1):
            piece = normed[:, cuts[c] : cuts[c + 1]]
            for w in range(3):
                copies[3 * c + w].wait()
                at = slice(starts[w], starts[w] + widths[w])
                product = jnp.dot(
                    piece,
                    weight_ref[cuts[c] : cuts[c + 1], at],
                    preferred_element_type=jnp.float32,
                )
                if c:
                    product = product + sums_ref[:, at]
                sums_ref[:, at] = product
        gate_copy.wait()
        gate_sums = dot_nt(normed, gate_ref[...])
        pad = jnp.zeros((rows, LANES - gate_count), jnp.float32)
        extra = jnp.concatenate([gate_sums, pad], axis=1)
        lane = lax.broadcasted_iota(jnp.int32, (rows, LANES), 1)
        sums_ref[:, width:] = jnp.where(lane == gate_count, squares, extra)
        for d in range(size):
            outs[d][...] = sums_ref[pl.ds(partner_of(position, size, d, False), 1), :]

    return call(
        body,
        [struct((1, width + LANES), jnp.float32)] * size,
        [ANY_SPEC] * 6,
        [streamed(a) for a in (tokens, norm_gain.reshape(1, -1), *weights, gates)],
        [
            pltpu.VMEM(tokens.shape, tokens.dtype),
            pltpu.VMEM((1, columns), norm_gain.dtype),
            pltpu.VMEM((columns, width), query_weight.dtype),
            pltpu.VMEM((gate_count, columns), gates.dtype),
            pltpu.VMEM((rows, width + LANES), jnp.float32),
            pltpu.SemaphoreType.DMA((len(cuts) - 1, 3)),
            pltpu.SemaphoreType.DMA(()),
            pltpu.SemaphoreType.DMA(()),
            pltpu.SemaphoreType.DMA(()),
        ],
        limit=16,
    )


def prepare(state_matrix, block_input, block_logf, lengths):
    _, heads, dv, dk = state_matrix.shape
    span = (heads, SPAN_LOCATIONS)

    def body(state_hbm, input_ref, logf_ref, lengths_ref, high_ref, low_ref, log_ref, *rest):
        sum_ref, state_ref, sems = rest
        copies = [
            pltpu.make_async_copy(state_hbm.at[0, h], state_ref.at[h], sems.at[h])
            for h in range(heads)
        ]
        for copy in copies:
            copy.start()
        live = jnp.broadcast_to(lengths_ref[...] & (SPAN_LOCATIONS - 1), span)
        inside = lax.broadcasted_iota(jnp.int32, span, 1) < live
        rest = jnp.where(inside, logf_ref[0], 0.0)
        square = (SPAN_LOCATIONS, SPAN_LOCATIONS)
        upto = (
            lax.broadcasted_iota(jnp.int32, square, 0) <= lax.broadcasted_iota(jnp.int32, square, 1)
        ).astype(jnp.float32).astype(jnp.bfloat16)
        cumulative = jnp.zeros(span, jnp.float32)
        for _ in range(3):
            term = rest.astype(jnp.bfloat16)
            rest = rest - term.astype(jnp.float32)
            cumulative = cumulative + jnp.dot(term, upto, preferred_element_type=jnp.float32)
        total = cumulative[:, SPAN_LOCATIONS - 1 :]
        sum_ref[...] = jnp.broadcast_to(total, (heads, LANES))
        log_ref[...] = jnp.where(inside, total - cumulative + input_ref[0], -jnp.inf)
        for h in range(heads):
            copies[h].wait()
            state = state_ref[h]
            high = state.astype(jnp.bfloat16)
            high_ref[h] = high
            low_ref[h] = (state - high.astype(jnp.float32)).astype(jnp.bfloat16)

    term = struct((heads, dv, dk), jnp.bfloat16)
    return call(
        body,
        [term, term, struct(span, jnp.float32), struct((heads, LANES), jnp.float32)],
        [ANY_SPEC] + [VMEM_SPEC] * 3,
        [streamed(state_matrix), block_input, block_logf, lengths.reshape(1, 1)],
        [
            pltpu.VMEM((heads, dv, dk), state_matrix.dtype),
            pltpu.SemaphoreType.DMA((heads,)),
        ],
    )


def recall(
    parts,
    forget_bias,
    prepared,
    state_normalizer,
    state_max,
    block_keys,
    block_values,
):
    *state_terms, cache_base, logf_sum = prepared
    heads, dv, dk = state_terms[0].shape
    all_heads = heads * lax.axis_size("tp")
    scale = dk ** (-0.5)
    count = len(parts)

    def body(*refs):
        (
            bias_ref,
            high_ref,
            low_ref,
            normalizer_ref,
            max_ref,
            keys_ref,
            values_ref,
            base_ref,
            sum_ref,
            out_ref,
        ) = refs[count:]
        half = lax.axis_index("tp")
        row = refs[0][...]
        for r in refs[1:count]:
            row = row + r[...]
        q_end, k_end = heads * dk, 2 * heads * dk
        v_end = k_end + heads * dv
        extra = row[:, v_end:]
        squares = extra[:, 2 * all_heads : 2 * all_heads + 1]
        row_scale = lax.rsqrt(squares / D + epsilon)
        row = row[:, :v_end] * row_scale

        def by_head(start, size):
            return jnp.concatenate(
                [row[:, start + h * size : start + (h + 1) * size] for h in range(heads)], axis=0
            ).astype(jnp.bfloat16)

        query, key, value = by_head(0, dk), by_head(q_end, dk), by_head(k_end, dv)
        gates = jnp.broadcast_to(extra * row_scale, (heads, LANES))
        lane = lax.broadcasted_iota(jnp.int32, (heads, LANES), 1)
        head = lax.broadcasted_iota(jnp.int32, (heads, LANES), 0)

        def column(values, first):
            return jnp.sum(jnp.where(lane == head + first, values, 0.0), axis=1, keepdims=True)

        lane_h = lax.broadcasted_iota(jnp.int32, (heads, heads), 1)
        head_h = lax.broadcasted_iota(jnp.int32, (heads, heads), 0)

        def own_column(ref):
            values = jnp.broadcast_to(ref[...], (heads, heads))
            return jnp.sum(jnp.where(lane_h == head_h, values, 0.0), axis=1, keepdims=True)

        new_input = column(gates, half * heads)
        new_logf = jax.nn.log_sigmoid(
            column(gates, all_heads + half * heads) + own_column(bias_ref)
        )
        total = sum_ref[:, :1] + new_logf
        carried_log = total + own_column(max_ref)
        cache_log = base_ref[...] + new_logf
        stable = jnp.maximum(
            jnp.maximum(carried_log, jnp.max(cache_log, axis=1, keepdims=True)), new_input
        )
        carried_weight = jnp.exp(carried_log - stable)
        new_weight = jnp.exp(new_input - stable)
        cache_weight = jnp.exp(cache_log - stable)

        def pick(make, size):
            rows = lax.broadcasted_iota(jnp.int32, (heads, size), 0)
            out = jnp.zeros((heads, size), jnp.float32)
            for h in range(heads):
                out = jnp.where(rows == h, make(h), out)
            return out

        scores = pick(lambda h: dot_nt(query, keys_ref[0, h]), SPAN_LOCATIONS)
        mixing = (scores * scale * cache_weight).astype(jnp.bfloat16)
        query_wide = query.astype(jnp.float32)
        own_term = (
            jnp.sum(query_wide * key.astype(jnp.float32), axis=1, keepdims=True)
            * scale
            * new_weight
        )

        def carry(h):
            return dot_nt(query, high_ref[h]) + dot_nt(query, low_ref[h])

        carried = pick(carry, dv)
        from_cache = pick(
            lambda h: jnp.dot(mixing, values_ref[0, h], preferred_element_type=jnp.float32), dv
        )
        numerator = carried_weight * carried + from_cache + own_term * value.astype(jnp.float32)
        normalizer = (
            carried_weight * jnp.sum(normalizer_ref[0] * query_wide, axis=1, keepdims=True)
            + jnp.sum(mixing.astype(jnp.float32), axis=1, keepdims=True)
            + own_term
        )
        divisor = jnp.maximum(jnp.maximum(jnp.abs(normalizer), jnp.exp(-stable)), 1.0)
        out_ref[...] = (numerator / divisor).astype(jnp.bfloat16)

    return call(
        body,
        [struct((heads, dv), jnp.bfloat16)],
        [VMEM_SPEC] * (count + 9),
        (
            *parts,
            forget_bias.reshape(1, -1),
            *[resident(term) for term in state_terms],
            state_normalizer,
            state_max,
            resident(block_keys),
            resident(block_values),
            cache_base,
            logf_sum,
        ),
    )[0]


def attend(pieces, out_weight):
    size = len(pieces)
    heads, dv = pieces[0].shape

    def body(*refs):
        weight_ref, out_ref, hidden_ref = refs[size:]
        position = lax.axis_index("kv")
        for n, d in enumerate([0, *distances(size)]):
            piece = refs[n][...].astype(jnp.float32)
            at = pl.ds(partner_of(position, size, d, True), 1)
            for h in range(heads):
                hidden_ref[at, h * dv : (h + 1) * dv] = piece[h : h + 1]
        out_ref[...] = jnp.dot(
            hidden_ref[...].astype(jnp.bfloat16),
            weight_ref[...],
            preferred_element_type=jnp.float32,
        ).astype(jnp.bfloat16)

    return call(
        body,
        [struct((size, out_weight.shape[1]), jnp.bfloat16)],
        [VMEM_SPEC] * (size + 1),
        (*pieces, resident(out_weight)),
        [pltpu.VMEM((size, heads * dv), jnp.float32)],
    )[0]


def add_features(refs, partners, gain_ref, up_ref, product, squares):
    size = lax.axis_size("kv")
    for ref, d in zip(refs, partners):
        columns = ref.shape[1]
        j = partner_of(lax.axis_index("kv"), size, d, True)
        at = pl.ds(pl.multiple_of(j * columns, columns), columns)
        wide = ref[...].astype(jnp.float32)
        squares = squares + jnp.sum(wide * wide, axis=1, keepdims=True)
        mixer_in = (wide * gain_ref[:, at]).astype(jnp.bfloat16)
        product = product + dot_nt(mixer_in, up_ref[:, at])
    return product, squares


def absorb(pieces, partners, mixer_gain, up_weight):
    rows = pieces[0].shape[0]
    units = up_weight.shape[0]
    count = len(pieces)

    def body(*refs):
        gain_ref, up_ref, product_ref, squares_ref = refs[count:]
        product, squares = add_features(
            refs[:count],
            partners,
            gain_ref,
            up_ref,
            jnp.zeros((rows, units), jnp.float32),
            jnp.zeros((rows, 1), jnp.float32),
        )
        product_ref[...] = product
        squares_ref[...] = jnp.broadcast_to(squares, (rows, LANES))

    return call(
        body,
        [struct((rows, units), jnp.float32), struct((rows, LANES), jnp.float32)],
        [VMEM_SPEC] * (count + 2),
        (*pieces, mixer_gain, up_weight),
        flops=20000000000,
    )


def mix(pieces, partners, before, residual, mixer_gain, up_weight, down_weight):
    size = lax.axis_size("kv")
    count = len(pieces)
    rows, columns = residual.shape
    blocks = [*distances(size), 0]
    share = columns // 2

    def body(*refs):
        product_ref, squares_ref, residual_ref, gain_ref, up_ref, down_ref, *outs = refs[count:]
        position = lax.axis_index("kv")
        product, squares = add_features(
            refs[:count], partners, gain_ref, up_ref, product_ref[...], squares_ref[:, :1]
        )
        scaled = product * lax.rsqrt(squares / D + epsilon)
        activated = jnp.square(jnp.maximum(scaled, 0.0)).astype(jnp.bfloat16)
        for n, d in enumerate(blocks):
            j = partner_of(position, size, d, False)
            at = pl.ds(pl.multiple_of(j * columns, columns), columns)
            terms = jnp.dot(activated, down_ref[:, at], preferred_element_type=jnp.float32)
            if d == 0:
                half = lax.broadcasted_iota(jnp.int32, (rows, columns), 1) // share
                kept = residual_ref[...].astype(jnp.float32)
                terms = terms + jnp.where(half == lax.axis_index("tp"), kept, 0.0)
            outs[n][...] = terms

    return call(
        body,
        [struct((rows, columns), jnp.float32)] * len(blocks),
        [VMEM_SPEC] * (count + 6),
        (*pieces, *before, residual, mixer_gain, up_weight, down_weight),
        flops=20000000000,
    )


def exchange_pairs(size, cores, distance):
    return [
        (i * cores + t, j * cores + (cores - 1 - t))
        for i, j in partner_pairs(size, distance)
        for t in range(cores)
    ]


def distances(size):
    return [*range(size // 2, size), *range(1, size // 2)]


def to_partners(outgoing, crossed):
    size, cores = lax.axis_size("kv"), lax.axis_size("tp")
    received = []
    for d in distances(size):
        if crossed:
            pairs = exchange_pairs(size, cores, d)
            received.append(lax.ppermute(outgoing[d], ("kv", "tp"), pairs))
        else:
            received.append(lax.ppermute(outgoing[d], "kv", partner_pairs(size, d)))
    return received


def direct(mesh, arrays_shape):
    size, cores = mesh["kv"], mesh["tp"]
    sequences, features = arrays_shape
    groups = mesh["dp"] * size
    return (
        2 < size <= DIRECT_LIMIT
        and cores == 2
        and sequences == groups
        and features % (size * 2 * LANES) == 0
    )


def shards_direct(
    tokens,
    norm_gain,
    query_weight,
    key_weight,
    value_weight,
    gate_weight,
    forget_bias,
    state_matrix,
    state_normalizer,
    state_max,
    block_keys,
    block_values,
    block_input,
    block_logf,
    lengths,
    out_weight,
    mixer_gain,
    up_weight,
    down_weight,
):
    head_half = lax.axis_index("tp")
    size = lax.axis_size("kv")
    swap = [(0, 1), (1, 0)]
    parts = project(tokens, norm_gain, query_weight, key_weight, value_weight, gate_weight)
    prepared = prepare(state_matrix, block_input, block_logf, lengths)
    parts = [parts[0]] + to_partners(parts, False)
    hidden = recall(
        parts,
        forget_bias,
        prepared,
        state_normalizer,
        state_max,
        block_keys,
        block_values,
    )
    pieces = [hidden] + to_partners([hidden] * size, False)
    partial_out = attend(pieces, out_weight)
    other_out = lax.ppermute(partial_out, "tp", swap)
    attended = partial_out.astype(jnp.float32) + other_out.astype(jnp.float32)
    residual = (tokens.astype(jnp.float32) + attended).astype(jnp.bfloat16)
    gain = mixer_gain.reshape(1, -1)
    pieces = to_partners([residual] * size, True)
    order = distances(size)
    up_weight, down_weight = resident(up_weight), resident(down_weight)
    absorbed = absorb([residual, pieces[0]], [0, order[0]], gain, up_weight)
    *terms, own = mix(
        pieces[1:], order[1:], absorbed, residual, gain, up_weight, down_weight
    )
    outgoing = dict(zip(order, terms))
    total = own
    for term in to_partners(outgoing, True):
        total = total + term
    share = tokens.shape[1] // 2
    other = lax.dynamic_slice_in_dim(total, (1 - head_half) * share, share, 1)
    kept = lax.dynamic_slice_in_dim(total, head_half * share, share, 1)
    return (kept + lax.ppermute(other, "tp", swap)).astype(jnp.bfloat16)


def mapped(mesh, function):
    return jax.shard_map(
        function,
        mesh=mesh,
        in_specs=(
            P("dp", "kv"),
            P("kv"),
            P("kv", "tp"),
            P("kv", "tp"),
            P("kv", "tp"),
            P(),
            P("tp"),
            P(("dp", "kv"), "tp", None, None),
            P(("dp", "kv"), "tp", None),
            P(("dp", "kv"), "tp"),
            P(("dp", "kv"), "tp", None, None),
            P(("dp", "kv"), "tp", None, None),
            P(("dp", "kv"), "tp", None),
            P(("dp", "kv"), "tp", None),
            P(("dp", "kv")),
            P("tp", "kv"),
            P(),
            P(("kv", "tp"), None),
            P(("kv", "tp"), None),
        ),
        out_specs=P("dp", ("kv", "tp")),
        check_vma=False,
    )


def solution(mesh):
    sizes = dict(mesh.shape)

    def whole(*arrays):
        return mapped(mesh, shards_general)(*arrays)

    def small(*arrays):
        if not direct(sizes, arrays[0].shape):
            return whole(*arrays)
        return mapped(mesh, shards_direct)(*arrays)

    if not 2 < sizes["kv"] <= DIRECT_LIMIT:
        return whole
    return small
```

profile of v0, /device:TPU:0, one launch (start us, length us, event | category | flops | bytes accessed | tf_op | source)
XLA Modules:
  0.0 40.0 jit_solution(10032462917946621578)
XLA Ops:
  0.0 0.0 copy-start.5
  0.0 0.0 copy-start.6
  0.0 4.4 %shard_map.181 = (f32[1,4224]{1,0:T(1,128)S(1)}, f32[1,4224]{1,0:T(1,128)S(1)}, f32[1,4224]{1,0:T(1,128)S(1)}, f32[1,4224]{1,0:T(1,128)S(1)}) custom-call(bf16[4,1024]{1,0:T(4,128)(2,1)} %tokens_hbm.1, f32[1,1024]{1,0:T(1,128)} %bitcast.16, bf16[1024,1024]{1,0:T(8,128)(2,1)} %q_hbm.1, bf16[1024,1024]{1,0:T(8,128)(2,1)} %k_hbm.1, bf16[1024,2048]{1,0:T(8,128)(2,1)} %v_hbm.1, ...), custom_call_target="tpu_custom_call" | custom-call | flops 20000000000 | bytes 1000000 | tf_op jit(solution)/shard_map/pallas_call | solution.py:245
  4.4 4.1 %collective-permute-start = (f32[1,4224]{1,0:T(1,128)S(1)}, f32[1,4224]{1,0:T(1,128)S(1)}, u32[]{:S(2)}, u32[]{:S(2)}) collective-permute-start(f32[1,4224]{1,0:T(1,128)S(1)} %get-tuple-element.20), channel_id=1, source_target_pairs={{0,4},{2,6},{4,0},{6,2},{1,5},{3,7},{5,1},{7,3},{8,12},{10,14},{12... | collective-permute-start | bytes 50696 | tf_op jit(solution)/shard_map/ppermute | solution.py:647
  8.5 1.3 %collective-permute-start.1 = (f32[1,4224]{1,0:T(1,128)S(1)}, f32[1,4224]{1,0:T(1,128)S(1)}, u32[]{:S(2)}, u32[]{:S(2)}) collective-permute-start(f32[1,4224]{1,0:T(1,128)S(1)} %get-tuple-element.21), channel_id=1, source_target_pairs={{0,6},{2,4},{4,2},{6,0},{1,7},{3,5},{5,3},{7,1},{8,14},{10,12},{12... | collective-permute-start | bytes 50696 | tf_op jit(solution)/shard_map/ppermute | solution.py:647
  9.9 0.2 collective-permute-start.2
  10.7 0.0 copy-done.5
  10.8 0.0 copy-done.6
  10.8 0.0 copy-start.1
  10.8 0.0 copy-start.2
  10.8 0.0 copy-start.4
  10.8 0.0 copy-start.7
  10.8 0.0 copy-start.8
  10.8 1.7 %shard_map.182 = (bf16[4,512,256]{2,1,0:T(8,128)(2,1)S(1)}, bf16[4,512,256]{2,1,0:T(8,128)(2,1)S(1)}, f32[4,64]{1,0:T(4,128)S(1)}, f32[4,128]{1,0:T(4,128)S(1)}) custom-call(f32[1,4,512,256]{3,2,1,0:T(8,128)} %state_hbm.1, f32[1,4,64]{2,1,0:T(4,128)S(1)} %copy-done.5, f32[1,4,64]{2,1,0:T(4,128)S(1)} %copy-done.6, s32[1,1]{1,0:T(1,128)} %bitcast.7.lengths_ref), custom_call_target="tpu_custom_call" | custom-call | flops 20000000000 | bytes 1000000 | tf_op jit(solution)/shard_map/pallas_call | solution.py:245
  12.5 0.0 collective-permute-done.refs_1_
  12.5 1.5 %collective-permute-done.1.refs_2_ = f32[1,4224]{1,0:T(1,128)S(1)} collective-permute-done((f32[1,4224]{1,0:T(1,128)S(1)}, f32[1,4224]{1,0:T(1,128)S(1)}, u32[]{:S(2)}, u32[]{:S(2)}) %collective-permute-start.1) | collective-permute-done | bytes 16928 | tf_op jit(solution)/shard_map/ppermute | solution.py:647
  14.1 0.0 collective-permute-done.2.refs_3_
  14.1 0.0 copy-done.1
  14.1 0.0 copy-done.2
  14.1 0.0 copy-done.4
  14.1 0.0 copy-done.7
  14.1 0.0 copy-done.8
  14.1 0.0 copy-start
  14.1 0.0 slice-start
  14.1 0.8 %shard_map.183.refs_0_ = bf16[4,512]{1,0:T(4,128)(2,1)S(1)} custom-call(f32[1,4224]{1,0:T(1,128)S(1)} %get-tuple-element.19.refs_0_, f32[1,4224]{1,0:T(1,128)S(1)} %collective-permute-done.refs_1_, f32[1,4224]{1,0:T(1,128)S(1)} %collective-permute-done.1.refs_2_, f32[1,4224]{1,0:T(1,128)S(1)} %collective-permute-done.2.refs_3_, f32[1,4]{1,0:T(1,128)S(1)} %bitcast.14, ...), custom_call_target="tpu_custom_call" | custom-call | flops 20000000000 | bytes 1000000 | tf_op jit(solution)/shard_map/pallas_call | solution.py:245
  14.9 0.0 copy-start.9
  14.9 0.0 slice-start.1
  15.0 0.0 copy-start.3
  15.0 1.4 %collective-permute-start.3 = (bf16[4,512]{1,0:T(4,128)(2,1)S(1)}, bf16[4,512]{1,0:T(4,128)(2,1)S(1)}, u32[]{:S(2)}, u32[]{:S(2)}) collective-permute-start(bf16[4,512]{1,0:T(4,128)(2,1)S(1)} %shard_map.183.refs_0_), channel_id=1, source_target_pairs={{0,4},{2,6},{4,0},{6,2},{1,5},{3,7},{5,1},{7,3},{8,12},{10,14},{12... | collective-permute-start | bytes 12296 | tf_op jit(solution)/shard_map/ppermute | solution.py:647
  16.3 1.3 %collective-permute-start.4 = (bf16[4,512]{1,0:T(4,128)(2,1)S(1)}, bf16[4,512]{1,0:T(4,128)(2,1)S(1)}, u32[]{:S(2)}, u32[]{:S(2)}) collective-permute-start(bf16[4,512]{1,0:T(4,128)(2,1)S(1)} %shard_map.183.refs_0_), channel_id=1, source_target_pairs={{0,6},{2,4},{4,2},{6,0},{1,7},{3,5},{5,3},{7,1},{8,14},{10,12},{12... | collective-permute-start | bytes 12296 | tf_op jit(solution)/shard_map/ppermute | solution.py:647
  17.7 0.8 %collective-permute-start.5 = (bf16[4,512]{1,0:T(4,128)(2,1)S(1)}, bf16[4,512]{1,0:T(4,128)(2,1)S(1)}, u32[]{:S(2)}, u32[]{:S(2)}) collective-permute-start(bf16[4,512]{1,0:T(4,128)(2,1)S(1)} %shard_map.183.refs_0_), channel_id=1, source_target_pairs={{0,2},{2,0},{4,6},{6,4},{1,3},{3,1},{5,7},{7,5},{8,10},{10,8},{12,... | collective-permute-start | bytes 12296 | tf_op jit(solution)/shard_map/ppermute | solution.py:647
  18.5 1.0 %collective-permute-done.3.refs_1_ = bf16[4,512]{1,0:T(4,128)(2,1)S(1)} collective-permute-done((bf16[4,512]{1,0:T(4,128)(2,1)S(1)}, bf16[4,512]{1,0:T(4,128)(2,1)S(1)}, u32[]{:S(2)}, u32[]{:S(2)}) %collective-permute-start.3) | collective-permute-done | bytes 4128 | tf_op jit(solution)/shard_map/ppermute | solution.py:647
  19.5 2.2 %collective-permute-done.4.refs_2_ = bf16[4,512]{1,0:T(4,128)(2,1)S(1)} collective-permute-done((bf16[4,512]{1,0:T(4,128)(2,1)S(1)}, bf16[4,512]{1,0:T(4,128)(2,1)S(1)}, u32[]{:S(2)}, u32[]{:S(2)}) %collective-permute-start.4) | collective-permute-done | bytes 4128 | tf_op jit(solution)/shard_map/ppermute | solution.py:647
  21.8 0.0 collective-permute-done.5.refs_3_
  21.8 0.0 copy-done
  21.8 0.0 slice-start.2
  21.8 0.6 %shard_map.184 = bf16[4,1024]{1,0:T(4,128)(2,1)S(1)} custom-call(bf16[4,512]{1,0:T(4,128)(2,1)S(1)} %shard_map.183.refs_0_, bf16[4,512]{1,0:T(4,128)(2,1)S(1)} %collective-permute-done.3.refs_1_, bf16[4,512]{1,0:T(4,128)(2,1)S(1)} %collective-permute-done.4.refs_2_, bf16[4,512]{1,0:T(4,128)(2,1)S(1)} %collective-permute-done.5.refs_3_, ...), custom_call_target="tpu_custom_call" | custom-call | flops 20000000000 | bytes 1000000 | tf_op jit(solution)/shard_map/pallas_call | solution.py:245
  22.4 0.0 slice-start.3
  22.4 0.0 collective-permute-start.6
  22.4 1.2 %collective-permute-done.6 = bf16[4,1024]{1,0:T(4,128)(2,1)S(1)} collective-permute-done((bf16[4,1024]{1,0:T(4,128)(2,1)S(1)}, bf16[4,1024]{1,0:T(4,128)(2,1)S(1)}, u32[]{:S(2)}, u32[]{:S(2)}) %collective-permute-start.6) | collective-permute-done | bytes 8224 | tf_op jit(solution)/shard_map/ppermute | solution.py:701
  23.6 0.0 copy-done.9
  23.6 0.8 %collective-permute-start.9 = (bf16[4,1024]{1,0:T(4,128)(2,1)S(1)}, bf16[4,1024]{1,0:T(4,128)(2,1)S(1)}, u32[]{:S(2)}, u32[]{:S(2)}) collective-permute-start(bf16[4,1024]{1,0:T(4,128)(2,1)S(1)} %add_convert_fusion.refs_0_.refs_4_), channel_id=1, source_target_pairs={{0,5},{1,4},{2,7},{3,6},{4,1},{5,0},{6,3},{7,2},{8,13},{9,12},{10,... | collective-permute-start | bytes 24584 | tf_op jit(solution)/shard_map/ppermute | solution.py:645
  24.4 1.8 %collective-permute-start.7 = (bf16[4,1024]{1,0:T(4,128)(2,1)S(1)}, bf16[4,1024]{1,0:T(4,128)(2,1)S(1)}, u32[]{:S(2)}, u32[]{:S(2)}) collective-permute-start(bf16[4,1024]{1,0:T(4,128)(2,1)S(1)} %add_convert_fusion.refs_0_.refs_4_), channel_id=1, source_target_pairs={{0,7},{1,6},{2,5},{3,4},{4,3},{5,2},{6,1},{7,0},{8,15},{9,14},{10,... | collective-permute-start | bytes 24584 | tf_op jit(solution)/shard_map/ppermute | solution.py:645
  26.1 0.5 %collective-permute-start.8 = (bf16[4,1024]{1,0:T(4,128)(2,1)S(1)}, bf16[4,1024]{1,0:T(4,128)(2,1)S(1)}, u32[]{:S(2)}, u32[]{:S(2)}) collective-permute-start(bf16[4,1024]{1,0:T(4,128)(2,1)S(1)} %add_convert_fusion.refs_0_.refs_4_), channel_id=1, source_target_pairs={{0,3},{1,2},{2,1},{3,0},{4,7},{5,6},{6,5},{7,4},{8,11},{9,10},{10,... | collective-permute-start | bytes 24584 | tf_op jit(solution)/shard_map/ppermute | solution.py:645
  26.7 1.0 %collective-permute-done.9.refs_1_ = bf16[4,1024]{1,0:T(4,128)(2,1)S(1)} collective-permute-done((bf16[4,1024]{1,0:T(4,128)(2,1)S(1)}, bf16[4,1024]{1,0:T(4,128)(2,1)S(1)}, u32[]{:S(2)}, u32[]{:S(2)}) %collective-permute-start.9) | collective-permute-done | bytes 8224 | tf_op jit(solution)/shard_map/ppermute | solution.py:645
  27.7 0.0 slice-done
  27.7 0.0 slice-done.1
  27.7 0.0 copy-done.3
  27.7 1.2 %shard_map.185 = (f32[4,1024]{1,0:T(4,128)S(1)}, f32[4,128]{1,0:T(4,128)S(1)}) custom-call(bf16[4,1024]{1,0:T(4,128)(2,1)S(1)} %add_convert_fusion.refs_0_.refs_4_, bf16[4,1024]{1,0:T(4,128)(2,1)S(1)} %collective-permute-done.9.refs_1_, f32[1,4096]{1,0:T(1,128)S(1)} %bitcast.12, bf16[1024,4096]{1,0:T(8,128)(2,1)S(1)} %bitcast.9), custom_call_target="tpu_custom_call" | custom-call | flops 20000000000 | bytes 1000000 | tf_op jit(solution)/shard_map/pallas_call | solution.py:245
  28.9 0.4 %collective-permute-done.7.refs_0_ = bf16[4,1024]{1,0:T(4,128)(2,1)S(1)} collective-permute-done((bf16[4,1024]{1,0:T(4,128)(2,1)S(1)}, bf16[4,1024]{1,0:T(4,128)(2,1)S(1)}, u32[]{:S(2)}, u32[]{:S(2)}) %collective-permute-start.7) | collective-permute-done | bytes 8224 | tf_op jit(solution)/shard_map/ppermute | solution.py:645
  29.3 0.0 collective-permute-done.8.refs_1_
  29.3 0.0 slice-done.2
  29.3 0.0 slice-done.3
  29.3 2.3 %shard_map.186 = (f32[4,1024]{1,0:T(4,128)S(1)}, f32[4,1024]{1,0:T(4,128)S(1)}, f32[4,1024]{1,0:T(4,128)S(1)}, f32[4,1024]{1,0:T(4,128)S(1)}) custom-call(bf16[4,1024]{1,0:T(4,128)(2,1)S(1)} %collective-permute-done.7.refs_0_, bf16[4,1024]{1,0:T(4,128)(2,1)S(1)} %collective-permute-done.8.refs_1_, f32[4,1024]{1,0:T(4,128)S(1)} %get-tuple-element.27.refs_2_, ...), custom_call_target="tpu_custom_call" | custom-call | flops 20000000000 | bytes 1000000 | tf_op jit(solution)/shard_map/pallas_call | solution.py:245
  31.6 0.4 %collective-permute-start.12 = (f32[4,1024]{1,0:T(4,128)S(1)}, f32[4,1024]{1,0:T(4,128)S(1)}, u32[]{:S(2)}, u32[]{:S(2)}) collective-permute-start(f32[4,1024]{1,0:T(4,128)S(1)} %get-tuple-element.32), channel_id=1, source_target_pairs={{0,3},{1,2},{2,1},{3,0},{4,7},{5,6},{6,5},{7,4},{8,11},{9,10},{10,... | collective-permute-start | bytes 49160 | tf_op jit(solution)/shard_map/ppermute | solution.py:645
  32.1 2.0 %collective-permute-start.11 = (f32[4,1024]{1,0:T(4,128)S(1)}, f32[4,1024]{1,0:T(4,128)S(1)}, u32[]{:S(2)}, u32[]{:S(2)}) collective-permute-start(f32[4,1024]{1,0:T(4,128)S(1)} %get-tuple-element.31), channel_id=1, source_target_pairs={{0,7},{1,6},{2,5},{3,4},{4,3},{5,2},{6,1},{7,0},{8,15},{9,14},{10,... | collective-permute-start | bytes 49160 | tf_op jit(solution)/shard_map/ppermute | solution.py:645
  34.0 0.7 %collective-permute-start.10 = (f32[4,1024]{1,0:T(4,128)S(1)}, f32[4,1024]{1,0:T(4,128)S(1)}, u32[]{:S(2)}, u32[]{:S(2)}) collective-permute-start(f32[4,1024]{1,0:T(4,128)S(1)} %get-tuple-element.30), channel_id=1, source_target_pairs={{0,5},{1,4},{2,7},{3,6},{4,1},{5,0},{6,3},{7,2},{8,13},{9,12},{10,... | collective-permute-start | bytes 49160 | tf_op jit(solution)/shard_map/ppermute | solution.py:645
  34.8 0.1 collective-permute-done.12
  34.8 2.2 %collective-permute-done.11 = f32[4,1024]{1,0:T(4,128)S(1)} collective-permute-done((f32[4,1024]{1,0:T(4,128)S(1)}, f32[4,1024]{1,0:T(4,128)S(1)}, u32[]{:S(2)}, u32[]{:S(2)}) %collective-permute-start.11) | collective-permute-done | bytes 16416 | tf_op jit(solution)/shard_map/ppermute | solution.py:645
  37.0 1.1 %collective-permute-done.10 = f32[4,1024]{1,0:T(4,128)S(1)} collective-permute-done((f32[4,1024]{1,0:T(4,128)S(1)}, f32[4,1024]{1,0:T(4,128)S(1)}, u32[]{:S(2)}, u32[]{:S(2)}) %collective-permute-start.10) | collective-permute-done | bytes 16416 | tf_op jit(solution)/shard_map/ppermute | solution.py:645
  38.1 0.3 collective-permute-start.13
  38.5 0.9 %collective-permute-done.13 = f32[4,512]{1,0:T(4,128)S(1)} collective-permute-done((f32[4,512]{1,0:T(4,128)S(1)}, f32[4,512]{1,0:T(4,128)S(1)}, u32[]{:S(2)}, u32[]{:S(2)}) %collective-permute-start.13) | collective-permute-done | bytes 8224 | tf_op jit(solution)/shard_map/ppermute | solution.py:719
  39.4 0.6 %add_convert_fusion.1 = bf16[4,512]{1,0:T(4,128)(2,1)} fusion(f32[4,512]{1,0:T(4,128)S(1)} %collective-permute-done.13, f32[4,1024]{1,0:T(4,128)S(1)} %add_add_fusion, s32[]{:T(128)S(6)} %select_n.6), kind=kLoop, calls=%fused_computation.2 | loop fusion | flops 4096 | bytes 20484 | tf_op jit(solution)/shard_map/convert_element_type | solution.py:719
  (5 shorter events, 0.0 us)
Async XLA Ops:
  0.0 10.7 %copy-start.5 = (f32[1,4,64]{2,1,0:T(4,128)S(1)}, f32[1,4,64]{2,1,0:T(4,128)}, u32[]{:S(2)}) copy-start(f32[1,4,64]{2,1,0:T(4,128)} %input_ref.1) | copy-start | bytes 3076
  0.0 10.8 %copy-start.6 = (f32[1,4,64]{2,1,0:T(4,128)S(1)}, f32[1,4,64]{2,1,0:T(4,128)}, u32[]{:S(2)}) copy-start(f32[1,4,64]{2,1,0:T(4,128)} %logf_ref.1) | copy-start | bytes 3076
  4.4 8.1 %collective-permute-start = (f32[1,4224]{1,0:T(1,128)S(1)}, f32[1,4224]{1,0:T(1,128)S(1)}, u32[]{:S(2)}, u32[]{:S(2)}) collective-permute-start(f32[1,4224]{1,0:T(1,128)S(1)} %get-tuple-element.20), channel_id=1, source_target_pairs={{0,4},{2,6},{4,0},{6,2},{1,5},{3,7},{5,1},{7,3},{8,12},{10,14},{12... | collective-permute-start | bytes 50696 | tf_op jit(solution)/shard_map/ppermute | solution.py:647
  8.5 5.5 %collective-permute-start.1 = (f32[1,4224]{1,0:T(1,128)S(1)}, f32[1,4224]{1,0:T(1,128)S(1)}, u32[]{:S(2)}, u32[]{:S(2)}) collective-permute-start(f32[1,4224]{1,0:T(1,128)S(1)} %get-tuple-element.21), channel_id=1, source_target_pairs={{0,6},{2,4},{4,2},{6,0},{1,7},{3,5},{5,3},{7,1},{8,14},{10,12},{12... | collective-permute-start | bytes 50696 | tf_op jit(solution)/shard_map/ppermute | solution.py:647
  9.9 4.2 %collective-permute-start.2 = (f32[1,4224]{1,0:T(1,128)S(1)}, f32[1,4224]{1,0:T(1,128)S(1)}, u32[]{:S(2)}, u32[]{:S(2)}) collective-permute-start(f32[1,4224]{1,0:T(1,128)S(1)} %get-tuple-element.22), channel_id=1, source_target_pairs={{0,2},{2,0},{4,6},{6,4},{1,3},{3,1},{5,7},{7,5},{8,10},{10,8},{12,... | collective-permute-start | bytes 50696 | tf_op jit(solution)/shard_map/ppermute | solution.py:647
  10.8 3.3 %copy-start.1 = (bf16[1,4,64,512]{3,2,1,0:T(8,128)(2,1)S(1)}, bf16[1,4,64,512]{3,2,1,0:T(8,128)(2,1)}, u32[]{:S(2)}) copy-start(bf16[1,4,64,512]{3,2,1,0:T(8,128)(2,1)} %refs_10_.1) | copy-start | bytes 786436
  10.8 3.3 %copy-start.2 = (bf16[1,4,64,256]{3,2,1,0:T(8,128)(2,1)S(1)}, bf16[1,4,64,256]{3,2,1,0:T(8,128)(2,1)}, u32[]{:S(2)}) copy-start(bf16[1,4,64,256]{3,2,1,0:T(8,128)(2,1)} %refs_9_.1) | copy-start | bytes 393220
  10.8 3.3 %copy-start.4 = (f32[1,4,256]{2,1,0:T(4,128)S(1)}, f32[1,4,256]{2,1,0:T(4,128)}, u32[]{:S(2)}) copy-start(f32[1,4,256]{2,1,0:T(4,128)} %refs_7_.2) | copy-start | bytes 12292
  10.8 3.3 %copy-start.7 = (f32[4]{0:T(128)S(1)}, f32[4]{0:T(128)}, u32[]{:S(2)}) copy-start(f32[4]{0:T(128)} %param.25) | copy-start | bytes 52
  10.8 3.3 %copy-start.8 = (f32[1,4]{1,0:T(1,128)S(1)}, f32[1,4]{1,0:T(1,128)}, u32[]{:S(2)}) copy-start(f32[1,4]{1,0:T(1,128)} %refs_8_.1) | copy-start | bytes 52
  14.1 7.7 %copy-start = (bf16[2048,1024]{1,0:T(8,128)(2,1)S(1)}, bf16[2048,1024]{1,0:T(8,128)(2,1)}, u32[]{:S(2)}) copy-start(bf16[2048,1024]{1,0:T(8,128)(2,1)} %refs_4_.1) | copy-start | bytes 12582916
  14.1 13.6 %slice-start = ((s8[8388608]{0:T(1024)(128)(4,1)}), s8[4194304]{0:T(1024)(128)(4,1)S(1)}, s32[]{:S(2)}) async-start(s8[8388608]{0:T(1024)(128)(4,1)} %bitcast.8), calls=%async_computation | async-start | bytes 8388608
  14.9 8.7 %copy-start.9 = (bf16[4,1024]{1,0:T(4,128)(2,1)S(1)}, bf16[4,1024]{1,0:T(4,128)(2,1)}, u32[]{:S(2)}) copy-start(bf16[4,1024]{1,0:T(4,128)(2,1)} %tokens_hbm.1) | copy-start | bytes 24580
  14.9 12.7 %slice-start.1 = ((s8[8388608]{0:T(1024)(128)(4,1)}), s8[4194304]{0:T(1024)(128)(4,1)S(1)}, s32[]{:S(2)}) async-start(s8[8388608]{0:T(1024)(128)(4,1)} %bitcast.8), calls=%async_computation.1 | async-start | bytes 8388608
  15.0 12.7 %copy-start.3 = (f32[4096]{0:T(1024)S(1)}, f32[4096]{0:T(1024)}, u32[]{:S(2)}) copy-start(f32[4096]{0:T(1024)} %param.35) | copy-start | bytes 49156
  15.0 4.6 %collective-permute-start.3 = (bf16[4,512]{1,0:T(4,128)(2,1)S(1)}, bf16[4,512]{1,0:T(4,128)(2,1)S(1)}, u32[]{:S(2)}, u32[]{:S(2)}) collective-permute-start(bf16[4,512]{1,0:T(4,128)(2,1)S(1)} %shard_map.183.refs_0_), channel_id=1, source_target_pairs={{0,4},{2,6},{4,0},{6,2},{1,5},{3,7},{5,1},{7,3},{8,12},{10,14},{12... | collective-permute-start | bytes 12296 | tf_op jit(solution)/shard_map/ppermute | solution.py:647
  16.3 5.4 %collective-permute-start.4 = (bf16[4,512]{1,0:T(4,128)(2,1)S(1)}, bf16[4,512]{1,0:T(4,128)(2,1)S(1)}, u32[]{:S(2)}, u32[]{:S(2)}) collective-permute-start(bf16[4,512]{1,0:T(4,128)(2,1)S(1)} %shard_map.183.refs_0_), channel_id=1, source_target_pairs={{0,6},{2,4},{4,2},{6,0},{1,7},{3,5},{5,3},{7,1},{8,14},{10,12},{12... | collective-permute-start | bytes 12296 | tf_op jit(solution)/shard_map/ppermute | solution.py:647
  17.7 4.1 %collective-permute-start.5 = (bf16[4,512]{1,0:T(4,128)(2,1)S(1)}, bf16[4,512]{1,0:T(4,128)(2,1)S(1)}, u32[]{:S(2)}, u32[]{:S(2)}) collective-permute-start(bf16[4,512]{1,0:T(4,128)(2,1)S(1)} %shard_map.183.refs_0_), channel_id=1, source_target_pairs={{0,2},{2,0},{4,6},{6,4},{1,3},{3,1},{5,7},{7,5},{8,10},{10,8},{12,... | collective-permute-start | bytes 12296 | tf_op jit(solution)/shard_map/ppermute | solution.py:647
  21.8 7.6 %slice-start.2 = ((s8[8388608]{0:T(1024)(128)(4,1)}), s8[4194304]{0:T(1024)(128)(4,1)S(1)}, s32[]{:S(2)}) async-start(s8[8388608]{0:T(1024)(128)(4,1)} %bitcast.10), calls=%async_computation.2 | async-start | bytes 8388608
  22.4 6.9 %slice-start.3 = ((s8[8388608]{0:T(1024)(128)(4,1)}), s8[4194304]{0:T(1024)(128)(4,1)S(1)}, s32[]{:S(2)}) async-start(s8[8388608]{0:T(1024)(128)(4,1)} %bitcast.10), calls=%async_computation.3 | async-start | bytes 8388608
  22.4 1.2 %collective-permute-start.6 = (bf16[4,1024]{1,0:T(4,128)(2,1)S(1)}, bf16[4,1024]{1,0:T(4,128)(2,1)S(1)}, u32[]{:S(2)}, u32[]{:S(2)}) collective-permute-start(bf16[4,1024]{1,0:T(4,128)(2,1)S(1)} %shard_map.184), channel_id=1, source_target_pairs={{0,1},{1,0},{2,3},{3,2},{4,5},{5,4},{6,7},{7,6},{8,9},{9,8},{10,11... | collective-permute-start | bytes 24584 | tf_op jit(solution)/shard_map/ppermute | solution.py:701
  23.6 4.0 %collective-permute-start.9 = (bf16[4,1024]{1,0:T(4,128)(2,1)S(1)}, bf16[4,1024]{1,0:T(4,128)(2,1)S(1)}, u32[]{:S(2)}, u32[]{:S(2)}) collective-permute-start(bf16[4,1024]{1,0:T(4,128)(2,1)S(1)} %add_convert_fusion.refs_0_.refs_4_), channel_id=1, source_target_pairs={{0,5},{1,4},{2,7},{3,6},{4,1},{5,0},{6,3},{7,2},{8,13},{9,12},{10,... | collective-permute-start | bytes 24584 | tf_op jit(solution)/shard_map/ppermute | solution.py:645
  24.4 4.9 %collective-permute-start.7 = (bf16[4,1024]{1,0:T(4,128)(2,1)S(1)}, bf16[4,1024]{1,0:T(4,128)(2,1)S(1)}, u32[]{:S(2)}, u32[]{:S(2)}) collective-permute-start(bf16[4,1024]{1,0:T(4,128)(2,1)S(1)} %add_convert_fusion.refs_0_.refs_4_), channel_id=1, source_target_pairs={{0,7},{1,6},{2,5},{3,4},{4,3},{5,2},{6,1},{7,0},{8,15},{9,14},{10,... | collective-permute-start | bytes 24584 | tf_op jit(solution)/shard_map/ppermute | solution.py:645
  26.1 3.2 %collective-permute-start.8 = (bf16[4,1024]{1,0:T(4,128)(2,1)S(1)}, bf16[4,1024]{1,0:T(4,128)(2,1)S(1)}, u32[]{:S(2)}, u32[]{:S(2)}) collective-permute-start(bf16[4,1024]{1,0:T(4,128)(2,1)S(1)} %add_convert_fusion.refs_0_.refs_4_), channel_id=1, source_target_pairs={{0,3},{1,2},{2,1},{3,0},{4,7},{5,6},{6,5},{7,4},{8,11},{9,10},{10,... | collective-permute-start | bytes 24584 | tf_op jit(solution)/shard_map/ppermute | solution.py:645
  31.6 3.2 %collective-permute-start.12 = (f32[4,1024]{1,0:T(4,128)S(1)}, f32[4,1024]{1,0:T(4,128)S(1)}, u32[]{:S(2)}, u32[]{:S(2)}) collective-permute-start(f32[4,1024]{1,0:T(4,128)S(1)} %get-tuple-element.32), channel_id=1, source_target_pairs={{0,3},{1,2},{2,1},{3,0},{4,7},{5,6},{6,5},{7,4},{8,11},{9,10},{10,... | collective-permute-start | bytes 49160 | tf_op jit(solution)/shard_map/ppermute | solution.py:645
  32.1 5.0 %collective-permute-start.11 = (f32[4,1024]{1,0:T(4,128)S(1)}, f32[4,1024]{1,0:T(4,128)S(1)}, u32[]{:S(2)}, u32[]{:S(2)}) collective-permute-start(f32[4,1024]{1,0:T(4,128)S(1)} %get-tuple-element.31), channel_id=1, source_target_pairs={{0,7},{1,6},{2,5},{3,4},{4,3},{5,2},{6,1},{7,0},{8,15},{9,14},{10,... | collective-permute-start | bytes 49160 | tf_op jit(solution)/shard_map/ppermute | solution.py:645
  34.0 4.1 %collective-permute-start.10 = (f32[4,1024]{1,0:T(4,128)S(1)}, f32[4,1024]{1,0:T(4,128)S(1)}, u32[]{:S(2)}, u32[]{:S(2)}) collective-permute-start(f32[4,1024]{1,0:T(4,128)S(1)} %get-tuple-element.30), channel_id=1, source_target_pairs={{0,5},{1,4},{2,7},{3,6},{4,1},{5,0},{6,3},{7,2},{8,13},{9,12},{10,... | collective-permute-start | bytes 49160 | tf_op jit(solution)/shard_map/ppermute | solution.py:645
  38.1 1.2 %collective-permute-start.13 = (f32[4,512]{1,0:T(4,128)S(1)}, f32[4,512]{1,0:T(4,128)S(1)}, u32[]{:S(2)}, u32[]{:S(2)}) collective-permute-start(f32[4,512]{1,0:T(4,128)S(1)} %constant_dynamic-slice_fusion), channel_id=1, source_target_pairs={{0,1},{1,0},{2,3},{3,2},{4,5},{5,4},{6,7},{7,6},{8,9},{9,8},{10,11... | collective-permute-start | bytes 24584 | tf_op jit(solution)/shard_map/ppermute | solution.py:719
where the time goes:
time: 40.1 us; the launch traced here: 40 us
  starting transfers between devices  15.8 us (39%)
  waiting for transfers between devices  11.6 us (29%)
  Pallas kernels  11 us (27%)
  between operations  0.86 us (2%)
  other arithmetic  0.62 us (2%)
    pallas_call x6, Pallas kernels, call(): pl.pallas_call(body, out_shape=outs, in_specs=in_specs, out_specs=[VMEM_S...  11 us
    ppermute x6, starting transfers between devices, to_partners(): received.append(lax.ppermute(outgoing[d], 'kv', partner_pairs(size, d)))  9.26 us
    ppermute x6, starting transfers between devices, to_partners(): received.append(lax.ppermute(outgoing[d], ('kv', 'tp'), pairs))  6.16 us
    ppermute x6, waiting for transfers between devices, to_partners(): received.append(lax.ppermute(outgoing[d], ('kv', 'tp'), pairs))  4.76 us
    ppermute x6, waiting for transfers between devices, to_partners(): received.append(lax.ppermute(outgoing[d], 'kv', partner_pairs(size, d)))  4.76 us
    ppermute x1, waiting for transfers between devices, shards_direct(): other_out = lax.ppermute(partial_out, 'tp', swap)  1.19 us
    ppermute x1, waiting for transfers between devices, shards_direct(): return (kept + lax.ppermute(other, 'tp', swap)).astype(jnp.bfloat16)  0.91 us
  transfers between devices with their start and end apart: 14, of which 10 were waited for; matrix products, arithmetic and copies ran while one was open for 0% of the time, Pallas kernels for 7%

commit v1 on v0

--- a/solution.py
+++ b/solution.py
@@ -353,19 +353,14 @@
     )
 
 
-def prepare(state_matrix, block_input, block_logf, lengths):
-    _, heads, dv, dk = state_matrix.shape
+def prepare(forget_bias, state_normalizer, state_max, block_input, block_logf, lengths):
+    _, heads, dk = state_normalizer.shape
     span = (heads, SPAN_LOCATIONS)
 
-    def body(state_hbm, input_ref, logf_ref, lengths_ref, high_ref, low_ref, log_ref, *rest):
-        sum_ref, state_ref, sems = rest
-        copies = [
-            pltpu.make_async_copy(state_hbm.at[0, h], state_ref.at[h], sems.at[h])
-            for h in range(heads)
-        ]
-        for copy in copies:
-            copy.start()
-        live = jnp.broadcast_to(lengths_ref[...] & (SPAN_LOCATIONS - 1), span)
+    def body(
+        bias_ref, normalizer_ref, max_ref, input_ref, logf_ref, lengths_ref, out_ref
+    ):
+        live = jnp.broadcast_to(lengths_ref[:, :1] & (SPAN_LOCATIONS - 1), span)
         inside = lax.broadcasted_iota(jnp.int32, span, 1) < live
         rest = jnp.where(inside, logf_ref[0], 0.0)
         square = (SPAN_LOCATIONS, SPAN_LOCATIONS)
@@ -378,57 +373,47 @@
             rest = rest - term.astype(jnp.float32)
             cumulative = cumulative + jnp.dot(term, upto, preferred_element_type=jnp.float32)
         total = cumulative[:, SPAN_LOCATIONS - 1 :]
-        sum_ref[...] = jnp.broadcast_to(total, (heads, LANES))
-        log_ref[...] = jnp.where(inside, total - cumulative + input_ref[0], -jnp.inf)
-        for h in range(heads):
-            copies[h].wait()
-            state = state_ref[h]
-            high = state.astype(jnp.bfloat16)
-            high_ref[h] = high
-            low_ref[h] = (state - high.astype(jnp.float32)).astype(jnp.bfloat16)
-
-    term = struct((heads, dv, dk), jnp.bfloat16)
+        base = jnp.where(inside, total - cumulative + input_ref[0], -jnp.inf)
+        lane_h = lax.broadcasted_iota(jnp.int32, (heads, heads), 1)
+        head_h = lax.broadcasted_iota(jnp.int32, (heads, heads), 0)
+
+        def column(ref):
+            values = jnp.broadcast_to(ref[...], (heads, heads))
+            return jnp.sum(jnp.where(lane_h == head_h, values, 0.0), axis=1, keepdims=True)
+
+        lane = lax.broadcasted_iota(jnp.int32, (heads, LANES), 1)
+        scalars = jnp.where(lane == 0, total, 0.0)
+        scalars = jnp.where(lane == 1, column(max_ref), scalars)
+        scalars = jnp.where(lane == 2, column(bias_ref), scalars)
+        out_ref[:, :dk] = normalizer_ref[0]
+        pad = jnp.zeros((heads, LANES - SPAN_LOCATIONS), jnp.float32)
+        out_ref[:, dk : dk + LANES] = jnp.concatenate([base, pad], axis=1)
+        out_ref[:, dk + LANES :] = scalars
+
     return call(
         body,
-        [term, term, struct(span, jnp.float32), struct((heads, LANES), jnp.float32)],
-        [ANY_SPEC] + [VMEM_SPEC] * 3,
-        [streamed(state_matrix), block_input, block_logf, lengths.reshape(1, 1)],
+        [struct((heads, dk + 2 * LANES), jnp.float32)],
+        [VMEM_SPEC] * 6,
         [
-            pltpu.VMEM((heads, dv, dk), state_matrix.dtype),
-            pltpu.SemaphoreType.DMA((heads,)),
+            forget_bias.reshape(1, -1),
+            state_normalizer,
+            state_max,
+            block_input,
+            block_logf,
+            jnp.pad(lengths, (0, LANES - 1)).reshape(1, -1),
         ],
-    )
-
-
-def recall(
-    parts,
-    forget_bias,
-    prepared,
-    state_normalizer,
-    state_max,
-    block_keys,
-    block_values,
-):
-    *state_terms, cache_base, logf_sum = prepared
-    heads, dv, dk = state_terms[0].shape
+    )[0]
+
+
+def recall(parts, prepared, state_matrix, block_keys, block_values):
+    _, heads, dv, dk = state_matrix.shape
     all_heads = heads * lax.axis_size("tp")
     scale = dk ** (-0.5)
     count = len(parts)
 
     def body(*refs):
-        (
-            bias_ref,
-            high_ref,
-            low_ref,
-            normalizer_ref,
-            max_ref,
-            keys_ref,
-            values_ref,
-            base_ref,
-            sum_ref,
-            out_ref,
-        ) = refs[count:]
-        half = lax.axis_index("tp")
+        small_ref, state_ref, keys_ref, values_ref, out_ref = refs[count:]
+        half = 1 - lax.axis_index("tp")
         row = refs[0][...]
         for r in refs[1:count]:
             row = row + r[...]
@@ -452,20 +437,15 @@
         def column(values, first):
             return jnp.sum(jnp.where(lane == head + first, values, 0.0), axis=1, keepdims=True)
 
-        lane_h = lax.broadcasted_iota(jnp.int32, (heads, heads), 1)
-        head_h = lax.broadcasted_iota(jnp.int32, (heads, heads), 0)
-
-        def own_column(ref):
-            values = jnp.broadcast_to(ref[...], (heads, heads))
-            return jnp.sum(jnp.where(lane_h == head_h, values, 0.0), axis=1, keepdims=True)
-
+        small = small_ref[...]
+        cache_base = small[:, dk : dk + SPAN_LOCATIONS]
+        logf_sum, state_max, bias = (
+            small[:, dk + LANES + i : dk + LANES + i + 1] for i in range(3)
+        )
         new_input = column(gates, half * heads)
-        new_logf = jax.nn.log_sigmoid(
-            column(gates, all_heads + half * heads) + own_column(bias_ref)
-        )
-        total = sum_ref[:, :1] + new_logf
-        carried_log = total + own_column(max_ref)
-        cache_log = base_ref[...] + new_logf
+        new_logf = jax.nn.log_sigmoid(column(gates, all_heads + half * heads) + bias)
+        carried_log = logf_sum + new_logf + state_max
+        cache_log = cache_base + new_logf
         stable = jnp.maximum(
             jnp.maximum(carried_log, jnp.max(cache_log, axis=1, keepdims=True)), new_input
         )
@@ -490,7 +470,10 @@
         )
 
         def carry(h):
-            return dot_nt(query, high_ref[h]) + dot_nt(query, low_ref[h])
+            state = state_ref[0, h]
+            high = state.astype(jnp.bfloat16)
+            low = (state - high.astype(jnp.float32)).astype(jnp.bfloat16)
+            return dot_nt(query, high) + dot_nt(query, low)
 
         carried = pick(carry, dv)
         from_cache = pick(
@@ -498,7 +481,7 @@
         )
         numerator = carried_weight * carried + from_cache + own_term * value.astype(jnp.float32)
         normalizer = (
-            carried_weight * jnp.sum(normalizer_ref[0] * query_wide, axis=1, keepdims=True)
+            carried_weight * jnp.sum(small[:, :dk] * query_wide, axis=1, keepdims=True)
             + jnp.sum(mixing.astype(jnp.float32), axis=1, keepdims=True)
             + own_term
         )
@@ -508,18 +491,8 @@
     return call(
         body,
         [struct((heads, dv), jnp.bfloat16)],
-        [VMEM_SPEC] * (count + 9),
-        (
-            *parts,
-            forget_bias.reshape(1, -1),
-            *[resident(term) for term in state_terms],
-            state_normalizer,
-            state_max,
-            resident(block_keys),
-            resident(block_values),
-            cache_base,
-            logf_sum,
-        ),
+        [VMEM_SPEC] * (count + 4),
+        (*parts, prepared, *[resident(w) for w in (state_matrix, block_keys, block_values)]),
     )[0]
 
 
@@ -530,7 +503,7 @@
     def body(*refs):
         weight_ref, out_ref, hidden_ref = refs[size:]
         position = lax.axis_index("kv")
-        for n, d in enumerate([0, *distances(size)]):
+        for n, d in enumerate([*distances(size), 0]):
             piece = refs[n][...].astype(jnp.float32)
             at = pl.ds(partner_of(position, size, d, True), 1)
             for h in range(heads):
@@ -636,16 +609,17 @@
     return [*range(size // 2, size), *range(1, size // 2)]
 
 
-def to_partners(outgoing, crossed):
+def to_partners(outgoing, partners):
     size, cores = lax.axis_size("kv"), lax.axis_size("tp")
     received = []
-    for d in distances(size):
-        if crossed:
-            pairs = exchange_pairs(size, cores, d)
-            received.append(lax.ppermute(outgoing[d], ("kv", "tp"), pairs))
-        else:
-            received.append(lax.ppermute(outgoing[d], "kv", partner_pairs(size, d)))
+    for d in partners:
+        pairs = exchange_pairs(size, cores, d)
+        received.append(lax.ppermute(outgoing[d], ("kv", "tp"), pairs))
     return received
+
+
+def swapped(array):
+    return lax.ppermute(array, "tp", [(0, 1), (1, 0)])
 
 
 def direct(mesh, arrays_shape):
@@ -683,26 +657,25 @@
 ):
     head_half = lax.axis_index("tp")
     size = lax.axis_size("kv")
-    swap = [(0, 1), (1, 0)]
-    parts = project(tokens, norm_gain, query_weight, key_weight, value_weight, gate_weight)
-    prepared = prepare(state_matrix, block_input, block_logf, lengths)
-    parts = [parts[0]] + to_partners(parts, False)
+    order = distances(size)
+    state_matrix = swapped(state_matrix)
+    parts = project(
+        tokens, norm_gain, query_weight, key_weight, value_weight, gate_weight
+    )
+    prepared = prepare(
+        forget_bias, state_normalizer, state_max, block_input, block_logf, lengths
+    )
+    parts = to_partners(parts, [*order, 0])
     hidden = recall(
-        parts,
-        forget_bias,
-        prepared,
-        state_normalizer,
-        state_max,
-        block_keys,
-        block_values,
-    )
-    pieces = [hidden] + to_partners([hidden] * size, False)
+        parts, swapped(prepared), state_matrix, swapped(block_keys), swapped(block_values)
+    )
+    pieces = to_partners([hidden] * size, [*order, 0])
     partial_out = attend(pieces, out_weight)
-    other_out = lax.ppermute(partial_out, "tp", swap)
+    other_out = swapped(partial_out)
     attended = partial_out.astype(jnp.float32) + other_out.astype(jnp.float32)
     residual = (tokens.astype(jnp.float32) + attended).astype(jnp.bfloat16)
     gain = mixer_gain.reshape(1, -1)
-    pieces = to_partners([residual] * size, True)
+    pieces = to_partners([residual] * size, order)
     order = distances(size)
     up_weight, down_weight = resident(up_weight), resident(down_weight)
     absorbed = absorb([residual, pieces[0]], [0, order[0]], gain, up_weight)
@@ -711,12 +684,12 @@
     )
     outgoing = dict(zip(order, terms))
     total = own
-    for term in to_partners(outgoing, True):
+    for term in to_partners(outgoing, order):
         total = total + term
     share = tokens.shape[1] // 2
     other = lax.dynamic_slice_in_dim(total, (1 - head_half) * share, share, 1)
     kept = lax.dynamic_slice_in_dim(total, head_half * share, share, 1)
-    return (kept + lax.ppermute(other, "tp", swap)).astype(jnp.bfloat16)
+    return (kept + swapped(other)).astype(jnp.bfloat16)
 
 
 def mapped(mesh, function):

time: 40.1 us -> 45.3 us (1.13)
  local copies, waits for them, and re-layouts: 0.09 us -> 4.11 us
  starting transfers between devices: 15.8 us -> 17.4 us
  Pallas kernels: 11 us -> 9.53 us
  waiting for transfers between devices: 11.6 us -> 12.6 us
    ppermute x6 -> x14, starting transfers between devices: 6.16 us -> 15.9 us  [to_partners(): received.append(lax.ppermute(outgoing[d], ('kv', 'tp'), pairs))]
    ppermute x8 -> x6, starting transfers between devices: 9.59 us -> 1.55 us  [swapped(): return lax.ppermute(array, 'tp', [(0, 1), (1, 0)])]
    ppermute x6 -> x14, waiting for transfers between devices: 4.76 us -> 10.7 us  [to_partners(): received.append(lax.ppermute(outgoing[d], ('kv', 'tp'), pairs))]
    ppermute x8 -> x6, waiting for transfers between devices: 6.86 us -> 1.89 us  [swapped(): return lax.ppermute(array, 'tp', [(0, 1), (1, 0)])]
    unnamed x28, local copies, waits for them, and re-layouts: 0.08 us -> 4.1 us
    pallas_call x6, Pallas kernels: 11 us -> 9.53 us  [call(): pl.pallas_call(body, out_shape=outs, in_specs=in_specs, out_specs=[VMEM_S...]
  transfers between devices with their start and end apart: 14 -> 20, of which waited for: 10 -> 12; matrix products, arithmetic and copies ran while one was open for 0% -> 0% of each run, Pallas kernels for 7% -> 13%
where the time goes in v1:
time: 45.3 us; the launch traced here: 45.1 us
  starting transfers between devices  17.4 us (38%)
  waiting for transfers between devices  12.6 us (28%)
  Pallas kernels  9.53 us (21%)
  local copies, waits for them, and re-layouts  4.11 us (9%)
  between operations  0.8 us (2%)
  other arithmetic  0.62 us (1%)
    ppermute x14, starting transfers between devices, to_partners(): received.append(lax.ppermute(outgoing[d], ('kv', 'tp'), pairs))  15.9 us
    ppermute x14, waiting for transfers between devices, to_partners(): received.append(lax.ppermute(outgoing[d], ('kv', 'tp'), pairs))  10.7 us
    pallas_call x6, Pallas kernels, call(): pl.pallas_call(body, out_shape=outs, in_specs=in_specs, out_specs=[VMEM_S...  9.53 us
    unnamed x28, local copies, waits for them, and re-layouts  4.1 us
    ppermute x6, waiting for transfers between devices, swapped(): return lax.ppermute(array, 'tp', [(0, 1), (1, 0)])  1.89 us
    ppermute x6, starting transfers between devices, swapped(): return lax.ppermute(array, 'tp', [(0, 1), (1, 0)])  1.55 us
  transfers between devices with their start and end apart: 20, of which 12 were waited for; matrix products, arithmetic and copies ran while one was open for 0% of the time, Pallas kernels for 13%

profile of v1, /device:TPU:0, one launch (start us, length us, event | category | flops | bytes accessed | tf_op | source)
XLA Modules:
  0.0 45.1 jit_solution(9213570673573034815)
XLA Ops:
  0.0 0.5 %collective-permute-start.5 = (f32[1,4,512,256]{3,2,1,0:T(8,128)}, f32[1,4,512,256]{3,2,1,0:T(8,128)S(1)}, u32[]{:S(2)}, u32[]{:S(2)}) collective-permute-start(f32[1,4,512,256]{3,2,1,0:T(8,128)} %param.26), channel_id=1, source_target_pairs={{0,1},{1,0},{2,3},{3,2},{4,5},{5,4},{6,7},{7,6},{8,9},{9,8},{10,11... | collective-permute-start | bytes 6291464 | tf_op jit(solution)/shard_map/ppermute | solution.py:622
  1.2 0.0 copy-start.2
  1.2 0.7 %copy-done.2 = f32[1,4,256]{2,1,0:T(4,128)S(1)} copy-done((f32[1,4,256]{2,1,0:T(4,128)S(1)}, f32[1,4,256]{2,1,0:T(4,128)}, u32[]{:S(2)}) %copy-start.2) | copy-done | bytes 4120
  1.8 0.7 %copy-done.3 = f32[1,4,64]{2,1,0:T(4,128)S(1)} copy-done((f32[1,4,64]{2,1,0:T(4,128)S(1)}, f32[1,4,64]{2,1,0:T(4,128)}, u32[]{:S(2)}) %copy-start.3) | copy-done | bytes 1048
  2.5 0.7 %copy-done.4 = f32[1,4,64]{2,1,0:T(4,128)S(1)} copy-done((f32[1,4,64]{2,1,0:T(4,128)S(1)}, f32[1,4,64]{2,1,0:T(4,128)}, u32[]{:S(2)}) %copy-start.4) | copy-done | bytes 1048
  3.2 0.7 %copy-done.5 = f32[4]{0:T(128)S(1)} copy-done((f32[4]{0:T(128)S(1)}, f32[4]{0:T(128)}, u32[]{:S(2)}) %copy-start.5) | copy-done | bytes 40
  3.9 0.7 %copy-done.6 = f32[1,4]{1,0:T(1,128)S(1)} copy-done((f32[1,4]{1,0:T(1,128)S(1)}, f32[1,4]{1,0:T(1,128)}, u32[]{:S(2)}) %copy-start.6) | copy-done | bytes 40
  4.5 0.2 shard_map.182
  4.7 0.1 collective-permute-start.4
  4.8 0.6 %copy-done.9 = bf16[1,4,64,256]{3,2,1,0:T(8,128)(2,1)S(1)} copy-done((bf16[1,4,64,256]{3,2,1,0:T(8,128)(2,1)S(1)}, bf16[1,4,64,256]{3,2,1,0:T(8,128)(2,1)}, u32[]{:S(2)}) %copy-start.9) | copy-done | bytes 131096
  5.4 0.0 collective-permute-start.6
  5.4 0.1 copy-done.8
  5.5 0.4 collective-permute-start.7
  5.9 4.3 %shard_map.181 = (f32[1,4224]{1,0:T(1,128)S(1)}, f32[1,4224]{1,0:T(1,128)S(1)}, f32[1,4224]{1,0:T(1,128)S(1)}, f32[1,4224]{1,0:T(1,128)S(1)}) custom-call(bf16[4,1024]{1,0:T(4,128)(2,1)} %tokens_hbm.1, f32[1,1024]{1,0:T(1,128)} %bitcast.16, bf16[1024,1024]{1,0:T(8,128)(2,1)} %q_hbm.1, bf16[1024,1024]{1,0:T(8,128)(2,1)} %k_hbm.1, bf16[1024,2048]{1,0:T(8,128)(2,1)} %v_hbm.1, ...), custom_call_target="tpu_custom_call" | custom-call | flops 20000000000 | bytes 1000000 | tf_op jit(solution)/shard_map/pallas_call | solution.py:245
  10.3 3.8 %collective-permute-start = (f32[1,4224]{1,0:T(1,128)S(1)}, f32[1,4224]{1,0:T(1,128)S(1)}, u32[]{:S(2)}, u32[]{:S(2)}) collective-permute-start(f32[1,4224]{1,0:T(1,128)S(1)} %get-tuple-element.15), channel_id=1, source_target_pairs={{0,5},{1,4},{2,7},{3,6},{4,1},{5,0},{6,3},{7,2},{8,13},{9,12},{10,... | collective-permute-start | bytes 50696 | tf_op jit(solution)/shard_map/ppermute | solution.py:617
  14.0 0.0 collective-permute-done.4.refs_4_
  14.1 1.1 %collective-permute-start.1 = (f32[1,4224]{1,0:T(1,128)S(1)}, f32[1,4224]{1,0:T(1,128)S(1)}, u32[]{:S(2)}, u32[]{:S(2)}) collective-permute-start(f32[1,4224]{1,0:T(1,128)S(1)} %get-tuple-element.16), channel_id=1, source_target_pairs={{0,7},{1,6},{2,5},{3,4},{4,3},{5,2},{6,1},{7,0},{8,15},{9,14},{10,... | collective-permute-start | bytes 50696 | tf_op jit(solution)/shard_map/ppermute | solution.py:617
  15.1 0.3 collective-permute-done.refs_0_
  15.5 1.6 %collective-permute-start.2 = (f32[1,4224]{1,0:T(1,128)S(1)}, f32[1,4224]{1,0:T(1,128)S(1)}, u32[]{:S(2)}, u32[]{:S(2)}) collective-permute-start(f32[1,4224]{1,0:T(1,128)S(1)} %get-tuple-element.17), channel_id=1, source_target_pairs={{0,3},{1,2},{2,1},{3,0},{4,7},{5,6},{6,5},{7,4},{8,11},{9,10},{10,... | collective-permute-start | bytes 50696 | tf_op jit(solution)/shard_map/ppermute | solution.py:617
  17.1 2.0 %collective-permute-done.1.refs_1_ = f32[1,4224]{1,0:T(1,128)S(1)} collective-permute-done((f32[1,4224]{1,0:T(1,128)S(1)}, f32[1,4224]{1,0:T(1,128)S(1)}, u32[]{:S(2)}, u32[]{:S(2)}) %collective-permute-start.1) | collective-permute-done | bytes 16928 | tf_op jit(solution)/shard_map/ppermute | solution.py:617
  19.1 0.0 collective-permute-start.3
  19.1 0.0 collective-permute-done.2.refs_2_
  19.1 1.2 %collective-permute-done.3.refs_3_ = f32[1,4224]{1,0:T(1,128)S(1)} collective-permute-done((f32[1,4224]{1,0:T(1,128)S(1)}, f32[1,4224]{1,0:T(1,128)S(1)}, u32[]{:S(2)}, u32[]{:S(2)}) %collective-permute-start.3) | collective-permute-done | bytes 16928 | tf_op jit(solution)/shard_map/ppermute | solution.py:617
  20.3 0.0 collective-permute-done.6.refs_6_
  20.3 0.0 collective-permute-done.7.refs_7_
  20.3 0.0 collective-permute-done.5.refs_5_
  20.3 0.0 slice-start
  20.3 0.8 %shard_map.183 = bf16[4,512]{1,0:T(4,128)(2,1)S(1)} custom-call(f32[1,4224]{1,0:T(1,128)S(1)} %collective-permute-done.refs_0_, f32[1,4224]{1,0:T(1,128)S(1)} %collective-permute-done.1.refs_1_, f32[1,4224]{1,0:T(1,128)S(1)} %collective-permute-done.2.refs_2_, f32[1,4224]{1,0:T(1,128)S(1)} %collective-permute-done.3.refs_3_, ...), custom_call_target="tpu_custom_call" | custom-call | flops 20000000000 | bytes 1000000 | tf_op jit(solution)/shard_map/pallas_call | solution.py:245
  21.2 0.0 copy-start.7
  21.2 0.0 slice-start.1
  21.2 0.0 copy-start.1
  21.2 1.1 %collective-permute-start.8 = (bf16[4,512]{1,0:T(4,128)(2,1)S(1)}, bf16[4,512]{1,0:T(4,128)(2,1)S(1)}, u32[]{:S(2)}, u32[]{:S(2)}) collective-permute-start(bf16[4,512]{1,0:T(4,128)(2,1)S(1)} %shard_map.183), channel_id=1, source_target_pairs={{0,5},{1,4},{2,7},{3,6},{4,1},{5,0},{6,3},{7,2},{8,13},{9,12},{10,... | collective-permute-start | bytes 12296 | tf_op jit(solution)/shard_map/ppermute | solution.py:617
  22.3 1.2 %collective-permute-start.9 = (bf16[4,512]{1,0:T(4,128)(2,1)S(1)}, bf16[4,512]{1,0:T(4,128)(2,1)S(1)}, u32[]{:S(2)}, u32[]{:S(2)}) collective-permute-start(bf16[4,512]{1,0:T(4,128)(2,1)S(1)} %shard_map.183), channel_id=1, source_target_pairs={{0,7},{1,6},{2,5},{3,4},{4,3},{5,2},{6,1},{7,0},{8,15},{9,14},{10,... | collective-permute-start | bytes 12296 | tf_op jit(solution)/shard_map/ppermute | solution.py:617
  23.4 0.8 %collective-permute-start.10 = (bf16[4,512]{1,0:T(4,128)(2,1)S(1)}, bf16[4,512]{1,0:T(4,128)(2,1)S(1)}, u32[]{:S(2)}, u32[]{:S(2)}) collective-permute-start(bf16[4,512]{1,0:T(4,128)(2,1)S(1)} %shard_map.183), channel_id=1, source_target_pairs={{0,3},{1,2},{2,1},{3,0},{4,7},{5,6},{6,5},{7,4},{8,11},{9,10},{10,... | collective-permute-start | bytes 12296 | tf_op jit(solution)/shard_map/ppermute | solution.py:617
  24.3 0.3 collective-permute-start.11
  24.6 0.6 %collective-permute-done.8.refs_0_ = bf16[4,512]{1,0:T(4,128)(2,1)S(1)} collective-permute-done((bf16[4,512]{1,0:T(4,128)(2,1)S(1)}, bf16[4,512]{1,0:T(4,128)(2,1)S(1)}, u32[]{:S(2)}, u32[]{:S(2)}) %collective-permute-start.8) | collective-permute-done | bytes 4128 | tf_op jit(solution)/shard_map/ppermute | solution.py:617
  25.2 1.9 %collective-permute-done.9.refs_1_ = bf16[4,512]{1,0:T(4,128)(2,1)S(1)} collective-permute-done((bf16[4,512]{1,0:T(4,128)(2,1)S(1)}, bf16[4,512]{1,0:T(4,128)(2,1)S(1)}, u32[]{:S(2)}, u32[]{:S(2)}) %collective-permute-start.9) | collective-permute-done | bytes 4128 | tf_op jit(solution)/shard_map/ppermute | solution.py:617
  27.1 0.0 collective-permute-done.10.refs_2_
  27.1 0.0 collective-permute-done.11.refs_3_
  27.1 0.0 copy-done
  27.1 0.0 slice-start.2
  27.1 0.6 %shard_map.184 = bf16[4,1024]{1,0:T(4,128)(2,1)S(1)} custom-call(bf16[4,512]{1,0:T(4,128)(2,1)S(1)} %collective-permute-done.8.refs_0_, bf16[4,512]{1,0:T(4,128)(2,1)S(1)} %collective-permute-done.9.refs_1_, bf16[4,512]{1,0:T(4,128)(2,1)S(1)} %collective-permute-done.10.refs_2_, bf16[4,512]{1,0:T(4,128)(2,1)S(1)} %collective-permute-done.11.refs_3_, ...), custom_call_target="tpu_custom_call" | custom-call | flops 20000000000 | bytes 1000000 | tf_op jit(solution)/shard_map/pallas_call | solution.py:245
  27.8 0.1 collective-permute-start.12
  27.9 1.1 %collective-permute-done.12 = bf16[4,1024]{1,0:T(4,128)(2,1)S(1)} collective-permute-done((bf16[4,1024]{1,0:T(4,128)(2,1)S(1)}, bf16[4,1024]{1,0:T(4,128)(2,1)S(1)}, u32[]{:S(2)}, u32[]{:S(2)}) %collective-permute-start.12) | collective-permute-done | bytes 8224 | tf_op jit(solution)/shard_map/ppermute | solution.py:622
  29.0 1.1 %collective-permute-start.15 = (bf16[4,1024]{1,0:T(4,128)(2,1)S(1)}, bf16[4,1024]{1,0:T(4,128)(2,1)S(1)}, u32[]{:S(2)}, u32[]{:S(2)}) collective-permute-start(bf16[4,1024]{1,0:T(4,128)(2,1)S(1)} %add_convert_fusion.refs_0_.refs_4_), channel_id=1, source_target_pairs={{0,5},{1,4},{2,7},{3,6},{4,1},{5,0},{6,3},{7,2},{8,13},{9,12},{10,... | collective-permute-start | bytes 24584 | tf_op jit(solution)/shard_map/ppermute | solution.py:617
  30.1 1.5 %collective-permute-start.13 = (bf16[4,1024]{1,0:T(4,128)(2,1)S(1)}, bf16[4,1024]{1,0:T(4,128)(2,1)S(1)}, u32[]{:S(2)}, u32[]{:S(2)}) collective-permute-start(bf16[4,1024]{1,0:T(4,128)(2,1)S(1)} %add_convert_fusion.refs_0_.refs_4_), channel_id=1, source_target_pairs={{0,7},{1,6},{2,5},{3,4},{4,3},{5,2},{6,1},{7,0},{8,15},{9,14},{10,... | collective-permute-start | bytes 24584 | tf_op jit(solution)/shard_map/ppermute | solution.py:617
  31.5 0.5 %collective-permute-start.14 = (bf16[4,1024]{1,0:T(4,128)(2,1)S(1)}, bf16[4,1024]{1,0:T(4,128)(2,1)S(1)}, u32[]{:S(2)}, u32[]{:S(2)}) collective-permute-start(bf16[4,1024]{1,0:T(4,128)(2,1)S(1)} %add_convert_fusion.refs_0_.refs_4_), channel_id=1, source_target_pairs={{0,3},{1,2},{2,1},{3,0},{4,7},{5,6},{6,5},{7,4},{8,11},{9,10},{10,... | collective-permute-start | bytes 24584 | tf_op jit(solution)/shard_map/ppermute | solution.py:617
  32.0 1.0 %collective-permute-done.15.refs_1_ = bf16[4,1024]{1,0:T(4,128)(2,1)S(1)} collective-permute-done((bf16[4,1024]{1,0:T(4,128)(2,1)S(1)}, bf16[4,1024]{1,0:T(4,128)(2,1)S(1)}, u32[]{:S(2)}, u32[]{:S(2)}) %collective-permute-start.15) | collective-permute-done | bytes 8224 | tf_op jit(solution)/shard_map/ppermute | solution.py:617
  33.0 0.0 slice-done
  33.0 0.0 copy-done.1
  33.0 1.2 %shard_map.185 = (f32[4,1024]{1,0:T(4,128)S(1)}, f32[4,128]{1,0:T(4,128)S(1)}) custom-call(bf16[4,1024]{1,0:T(4,128)(2,1)S(1)} %add_convert_fusion.refs_0_.refs_4_, bf16[4,1024]{1,0:T(4,128)(2,1)S(1)} %collective-permute-done.15.refs_1_, f32[1,4096]{1,0:T(1,128)S(1)} %bitcast.12, bf16[1024,4096]{1,0:T(8,128)(2,1)S(1)} %bitcast.9), custom_call_target="tpu_custom_call" | custom-call | flops 20000000000 | bytes 1000000 | tf_op jit(solution)/shard_map/pallas_call | solution.py:245
  34.2 0.7 %collective-permute-done.13.refs_0_ = bf16[4,1024]{1,0:T(4,128)(2,1)S(1)} collective-permute-done((bf16[4,1024]{1,0:T(4,128)(2,1)S(1)}, bf16[4,1024]{1,0:T(4,128)(2,1)S(1)}, u32[]{:S(2)}, u32[]{:S(2)}) %collective-permute-start.13) | collective-permute-done | bytes 8224 | tf_op jit(solution)/shard_map/ppermute | solution.py:617
  34.9 0.0 collective-permute-done.14.refs_1_
  34.9 0.0 slice-done.3
  35.0 2.3 %shard_map.186 = (f32[4,1024]{1,0:T(4,128)S(1)}, f32[4,1024]{1,0:T(4,128)S(1)}, f32[4,1024]{1,0:T(4,128)S(1)}, f32[4,1024]{1,0:T(4,128)S(1)}) custom-call(bf16[4,1024]{1,0:T(4,128)(2,1)S(1)} %collective-permute-done.13.refs_0_, bf16[4,1024]{1,0:T(4,128)(2,1)S(1)} %collective-permute-done.14.refs_1_, f32[4,1024]{1,0:T(4,128)S(1)} %get-tuple-element.19.refs_2_, ...), custom_call_target="tpu_custom_call" | custom-call | flops 20000000000 | bytes 1000000 | tf_op jit(solution)/shard_map/pallas_call | solution.py:245
  37.3 0.1 collective-permute-start.18
  37.4 1.7 %collective-permute-start.17 = (f32[4,1024]{1,0:T(4,128)S(1)}, f32[4,1024]{1,0:T(4,128)S(1)}, u32[]{:S(2)}, u32[]{:S(2)}) collective-permute-start(f32[4,1024]{1,0:T(4,128)S(1)} %get-tuple-element.23), channel_id=1, source_target_pairs={{0,7},{1,6},{2,5},{3,4},{4,3},{5,2},{6,1},{7,0},{8,15},{9,14},{10,... | collective-permute-start | bytes 49160 | tf_op jit(solution)/shard_map/ppermute | solution.py:617
  39.2 1.1 %collective-permute-start.16 = (f32[4,1024]{1,0:T(4,128)S(1)}, f32[4,1024]{1,0:T(4,128)S(1)}, u32[]{:S(2)}, u32[]{:S(2)}) collective-permute-start(f32[4,1024]{1,0:T(4,128)S(1)} %get-tuple-element.22), channel_id=1, source_target_pairs={{0,5},{1,4},{2,7},{3,6},{4,1},{5,0},{6,3},{7,2},{8,13},{9,12},{10,... | collective-permute-start | bytes 49160 | tf_op jit(solution)/shard_map/ppermute | solution.py:617
  40.3 0.2 collective-permute-done.18
  40.4 1.9 %collective-permute-done.17 = f32[4,1024]{1,0:T(4,128)S(1)} collective-permute-done((f32[4,1024]{1,0:T(4,128)S(1)}, f32[4,1024]{1,0:T(4,128)S(1)}, u32[]{:S(2)}, u32[]{:S(2)}) %collective-permute-start.17) | collective-permute-done | bytes 16416 | tf_op jit(solution)/shard_map/ppermute | solution.py:617
  42.4 0.8 %collective-permute-done.16 = f32[4,1024]{1,0:T(4,128)S(1)} collective-permute-done((f32[4,1024]{1,0:T(4,128)S(1)}, f32[4,1024]{1,0:T(4,128)S(1)}, u32[]{:S(2)}, u32[]{:S(2)}) %collective-permute-start.16) | collective-permute-done | bytes 16416 | tf_op jit(solution)/shard_map/ppermute | solution.py:617
  43.3 0.4 collective-permute-start.19
  43.7 0.8 %collective-permute-done.19 = f32[4,512]{1,0:T(4,128)S(1)} collective-permute-done((f32[4,512]{1,0:T(4,128)S(1)}, f32[4,512]{1,0:T(4,128)S(1)}, u32[]{:S(2)}, u32[]{:S(2)}) %collective-permute-start.19) | collective-permute-done | bytes 8224 | tf_op jit(solution)/shard_map/ppermute | solution.py:622
  44.5 0.6 %add_convert_fusion.1 = bf16[4,512]{1,0:T(4,128)(2,1)} fusion(f32[4,512]{1,0:T(4,128)S(1)} %collective-permute-done.19, f32[4,1024]{1,0:T(4,128)S(1)} %add_add_fusion, s32[]{:T(128)S(6)} %select_n.6), kind=kLoop, calls=%fused_computation.2 | loop fusion | flops 4096 | bytes 20484 | tf_op jit(solution)/shard_map/convert_element_type | solution.py:692
  (17 shorter events, 0.1 us)
Async XLA Ops:
  0.0 20.3 %collective-permute-start.5 = (f32[1,4,512,256]{3,2,1,0:T(8,128)}, f32[1,4,512,256]{3,2,1,0:T(8,128)S(1)}, u32[]{:S(2)}, u32[]{:S(2)}) collective-permute-start(f32[1,4,512,256]{3,2,1,0:T(8,128)} %param.26), channel_id=1, source_target_pairs={{0,1},{1,0},{2,3},{3,2},{4,5},{5,4},{6,7},{7,6},{8,9},{9,8},{10,11... | collective-permute-start | bytes 6291464 | tf_op jit(solution)/shard_map/ppermute | solution.py:622
  1.2 0.7 %copy-start.2 = (f32[1,4,256]{2,1,0:T(4,128)S(1)}, f32[1,4,256]{2,1,0:T(4,128)}, u32[]{:S(2)}) copy-start(f32[1,4,256]{2,1,0:T(4,128)} %normalizer_ref.1) | copy-start | bytes 12292
  1.8 0.7 %copy-start.3 = (f32[1,4,64]{2,1,0:T(4,128)S(1)}, f32[1,4,64]{2,1,0:T(4,128)}, u32[]{:S(2)}) copy-start(f32[1,4,64]{2,1,0:T(4,128)} %input_ref.1) | copy-start | bytes 3076
  2.5 0.7 %copy-start.4 = (f32[1,4,64]{2,1,0:T(4,128)S(1)}, f32[1,4,64]{2,1,0:T(4,128)}, u32[]{:S(2)}) copy-start(f32[1,4,64]{2,1,0:T(4,128)} %logf_ref.1) | copy-start | bytes 3076
  3.2 0.7 %copy-start.5 = (f32[4]{0:T(128)S(1)}, f32[4]{0:T(128)}, u32[]{:S(2)}) copy-start(f32[4]{0:T(128)} %param.25) | copy-start | bytes 52
  3.9 0.7 %copy-start.6 = (f32[1,4]{1,0:T(1,128)S(1)}, f32[1,4]{1,0:T(1,128)}, u32[]{:S(2)}) copy-start(f32[1,4]{1,0:T(1,128)} %max_ref.1) | copy-start | bytes 52
  4.5 0.9 %copy-start.9 = (bf16[1,4,64,256]{3,2,1,0:T(8,128)(2,1)S(1)}, bf16[1,4,64,256]{3,2,1,0:T(8,128)(2,1)}, u32[]{:S(2)}) copy-start(bf16[1,4,64,256]{3,2,1,0:T(8,128)(2,1)} %param.29) | copy-start | bytes 393220
  4.5 1.0 %copy-start.8 = (bf16[1,4,64,512]{3,2,1,0:T(8,128)(2,1)S(1)}, bf16[1,4,64,512]{3,2,1,0:T(8,128)(2,1)}, u32[]{:S(2)}) copy-start(bf16[1,4,64,512]{3,2,1,0:T(8,128)(2,1)} %param.30) | copy-start | bytes 786436
  4.7 9.3 %collective-permute-start.4 = (f32[4,512]{1,0:T(4,128)S(1)}, f32[4,512]{1,0:T(4,128)S(1)}, u32[]{:S(2)}, u32[]{:S(2)}) collective-permute-start(f32[4,512]{1,0:T(4,128)S(1)} %shard_map.182), channel_id=1, source_target_pairs={{0,1},{1,0},{2,3},{3,2},{4,5},{5,4},{6,7},{7,6},{8,9},{9,8},{10,11... | collective-permute-start | bytes 24584 | tf_op jit(solution)/shard_map/ppermute | solution.py:622
  5.4 14.9 %collective-permute-start.6 = (bf16[1,4,64,256]{3,2,1,0:T(8,128)(2,1)S(1)}, bf16[1,4,64,256]{3,2,1,0:T(8,128)(2,1)S(1)}, u32[]{:S(2)}, u32[]{:S(2)}) collective-permute-start(bf16[1,4,64,256]{3,2,1,0:T(8,128)(2,1)S(1)} %copy-done.9), channel_id=1, source_target_pairs={{0,1},{1,0},{2,3},{3,2},{4,5},{5,4},{6,7},{7,6},{8,9},{9,8},{10,11... | collective-permute-start | bytes 393224 | tf_op jit(solution)/shard_map/ppermute | solution.py:622
  5.5 14.8 %collective-permute-start.7 = (bf16[1,4,64,512]{3,2,1,0:T(8,128)(2,1)S(1)}, bf16[1,4,64,512]{3,2,1,0:T(8,128)(2,1)S(1)}, u32[]{:S(2)}, u32[]{:S(2)}) collective-permute-start(bf16[1,4,64,512]{3,2,1,0:T(8,128)(2,1)S(1)} %copy-done.8), channel_id=1, source_target_pairs={{0,1},{1,0},{2,3},{3,2},{4,5},{5,4},{6,7},{7,6},{8,9},{9,8},{10,11... | collective-permute-start | bytes 786440 | tf_op jit(solution)/shard_map/ppermute | solution.py:622
  10.3 5.2 %collective-permute-start = (f32[1,4224]{1,0:T(1,128)S(1)}, f32[1,4224]{1,0:T(1,128)S(1)}, u32[]{:S(2)}, u32[]{:S(2)}) collective-permute-start(f32[1,4224]{1,0:T(1,128)S(1)} %get-tuple-element.15), channel_id=1, source_target_pairs={{0,5},{1,4},{2,7},{3,6},{4,1},{5,0},{6,3},{7,2},{8,13},{9,12},{10,... | collective-permute-start | bytes 50696 | tf_op jit(solution)/shard_map/ppermute | solution.py:617
  14.1 5.1 %collective-permute-start.1 = (f32[1,4224]{1,0:T(1,128)S(1)}, f32[1,4224]{1,0:T(1,128)S(1)}, u32[]{:S(2)}, u32[]{:S(2)}) collective-permute-start(f32[1,4224]{1,0:T(1,128)S(1)} %get-tuple-element.16), channel_id=1, source_target_pairs={{0,7},{1,6},{2,5},{3,4},{4,3},{5,2},{6,1},{7,0},{8,15},{9,14},{10,... | collective-permute-start | bytes 50696 | tf_op jit(solution)/shard_map/ppermute | solution.py:617
  15.5 3.6 %collective-permute-start.2 = (f32[1,4224]{1,0:T(1,128)S(1)}, f32[1,4224]{1,0:T(1,128)S(1)}, u32[]{:S(2)}, u32[]{:S(2)}) collective-permute-start(f32[1,4224]{1,0:T(1,128)S(1)} %get-tuple-element.17), channel_id=1, source_target_pairs={{0,3},{1,2},{2,1},{3,0},{4,7},{5,6},{6,5},{7,4},{8,11},{9,10},{10,... | collective-permute-start | bytes 50696 | tf_op jit(solution)/shard_map/ppermute | solution.py:617
  19.1 8.0 %copy-start = (bf16[2048,1024]{1,0:T(8,128)(2,1)S(1)}, bf16[2048,1024]{1,0:T(8,128)(2,1)}, u32[]{:S(2)}) copy-start(bf16[2048,1024]{1,0:T(8,128)(2,1)} %refs_4_.1) | copy-start | bytes 12582916
  19.1 1.2 %collective-permute-start.3 = (f32[1,4224]{1,0:T(1,128)S(1)}, f32[1,4224]{1,0:T(1,128)S(1)}, u32[]{:S(2)}, u32[]{:S(2)}) collective-permute-start(f32[1,4224]{1,0:T(1,128)S(1)} %get-tuple-element.18), channel_id=1, source_target_pairs={{0,1},{1,0},{2,3},{3,2},{4,5},{5,4},{6,7},{7,6},{8,9},{9,8},{10,11... | collective-permute-start | bytes 50696 | tf_op jit(solution)/shard_map/ppermute | solution.py:617
  20.3 12.7 %slice-start = ((s8[8388608]{0:T(1024)(128)(4,1)}), s8[4194304]{0:T(1024)(128)(4,1)S(1)}, s32[]{:S(2)}) async-start(s8[8388608]{0:T(1024)(128)(4,1)} %bitcast.8), calls=%async_computation | async-start | bytes 8388608
  21.2 7.8 %copy-start.7 = (bf16[4,1024]{1,0:T(4,128)(2,1)S(1)}, bf16[4,1024]{1,0:T(4,128)(2,1)}, u32[]{:S(2)}) copy-start(bf16[4,1024]{1,0:T(4,128)(2,1)} %tokens_hbm.1) | copy-start | bytes 24580
  21.2 11.8 %slice-start.1 = ((s8[8388608]{0:T(1024)(128)(4,1)}), s8[4194304]{0:T(1024)(128)(4,1)S(1)}, s32[]{:S(2)}) async-start(s8[8388608]{0:T(1024)(128)(4,1)} %bitcast.8), calls=%async_computation.1 | async-start | bytes 8388608
  21.2 11.8 %copy-start.1 = (f32[4096]{0:T(1024)S(1)}, f32[4096]{0:T(1024)}, u32[]{:S(2)}) copy-start(f32[4096]{0:T(1024)} %param.35) | copy-start | bytes 49156
  21.2 4.0 %collective-permute-start.8 = (bf16[4,512]{1,0:T(4,128)(2,1)S(1)}, bf16[4,512]{1,0:T(4,128)(2,1)S(1)}, u32[]{:S(2)}, u32[]{:S(2)}) collective-permute-start(bf16[4,512]{1,0:T(4,128)(2,1)S(1)} %shard_map.183), channel_id=1, source_target_pairs={{0,5},{1,4},{2,7},{3,6},{4,1},{5,0},{6,3},{7,2},{8,13},{9,12},{10,... | collective-permute-start | bytes 12296 | tf_op jit(solution)/shard_map/ppermute | solution.py:617
  22.3 4.8 %collective-permute-start.9 = (bf16[4,512]{1,0:T(4,128)(2,1)S(1)}, bf16[4,512]{1,0:T(4,128)(2,1)S(1)}, u32[]{:S(2)}, u32[]{:S(2)}) collective-permute-start(bf16[4,512]{1,0:T(4,128)(2,1)S(1)} %shard_map.183), channel_id=1, source_target_pairs={{0,7},{1,6},{2,5},{3,4},{4,3},{5,2},{6,1},{7,0},{8,15},{9,14},{10,... | collective-permute-start | bytes 12296 | tf_op jit(solution)/shard_map/ppermute | solution.py:617
  23.4 3.7 %collective-permute-start.10 = (bf16[4,512]{1,0:T(4,128)(2,1)S(1)}, bf16[4,512]{1,0:T(4,128)(2,1)S(1)}, u32[]{:S(2)}, u32[]{:S(2)}) collective-permute-start(bf16[4,512]{1,0:T(4,128)(2,1)S(1)} %shard_map.183), channel_id=1, source_target_pairs={{0,3},{1,2},{2,1},{3,0},{4,7},{5,6},{6,5},{7,4},{8,11},{9,10},{10,... | collective-permute-start | bytes 12296 | tf_op jit(solution)/shard_map/ppermute | solution.py:617
  24.3 2.8 %collective-permute-start.11 = (bf16[4,512]{1,0:T(4,128)(2,1)S(1)}, bf16[4,512]{1,0:T(4,128)(2,1)S(1)}, u32[]{:S(2)}, u32[]{:S(2)}) collective-permute-start(bf16[4,512]{1,0:T(4,128)(2,1)S(1)} %shard_map.183), channel_id=1, source_target_pairs={{0,1},{1,0},{2,3},{3,2},{4,5},{5,4},{6,7},{7,6},{8,9},{9,8},{10,11... | collective-permute-start | bytes 12296 | tf_op jit(solution)/shard_map/ppermute | solution.py:617
  27.1 7.8 %slice-start.2 = ((s8[8388608]{0:T(1024)(128)(4,1)}), s8[4194304]{0:T(1024)(128)(4,1)S(1)}, s32[]{:S(2)}) async-start(s8[8388608]{0:T(1024)(128)(4,1)} %bitcast.10), calls=%async_computation.2 | async-start | bytes 8388608
  27.8 7.2 %slice-start.3 = ((s8[8388608]{0:T(1024)(128)(4,1)}), s8[4194304]{0:T(1024)(128)(4,1)S(1)}, s32[]{:S(2)}) async-start(s8[8388608]{0:T(1024)(128)(4,1)} %bitcast.10), calls=%async_computation.3 | async-start | bytes 8388608
  27.8 1.2 %collective-permute-start.12 = (bf16[4,1024]{1,0:T(4,128)(2,1)S(1)}, bf16[4,1024]{1,0:T(4,128)(2,1)S(1)}, u32[]{:S(2)}, u32[]{:S(2)}) collective-permute-start(bf16[4,1024]{1,0:T(4,128)(2,1)S(1)} %shard_map.184), channel_id=1, source_target_pairs={{0,1},{1,0},{2,3},{3,2},{4,5},{5,4},{6,7},{7,6},{8,9},{9,8},{10,11... | collective-permute-start | bytes 24584 | tf_op jit(solution)/shard_map/ppermute | solution.py:622
  29.0 4.0 %collective-permute-start.15 = (bf16[4,1024]{1,0:T(4,128)(2,1)S(1)}, bf16[4,1024]{1,0:T(4,128)(2,1)S(1)}, u32[]{:S(2)}, u32[]{:S(2)}) collective-permute-start(bf16[4,1024]{1,0:T(4,128)(2,1)S(1)} %add_convert_fusion.refs_0_.refs_4_), channel_id=1, source_target_pairs={{0,5},{1,4},{2,7},{3,6},{4,1},{5,0},{6,3},{7,2},{8,13},{9,12},{10,... | collective-permute-start | bytes 24584 | tf_op jit(solution)/shard_map/ppermute | solution.py:617
  30.1 4.9 %collective-permute-start.13 = (bf16[4,1024]{1,0:T(4,128)(2,1)S(1)}, bf16[4,1024]{1,0:T(4,128)(2,1)S(1)}, u32[]{:S(2)}, u32[]{:S(2)}) collective-permute-start(bf16[4,1024]{1,0:T(4,128)(2,1)S(1)} %add_convert_fusion.refs_0_.refs_4_), channel_id=1, source_target_pairs={{0,7},{1,6},{2,5},{3,4},{4,3},{5,2},{6,1},{7,0},{8,15},{9,14},{10,... | collective-permute-start | bytes 24584 | tf_op jit(solution)/shard_map/ppermute | solution.py:617
  31.5 3.4 %collective-permute-start.14 = (bf16[4,1024]{1,0:T(4,128)(2,1)S(1)}, bf16[4,1024]{1,0:T(4,128)(2,1)S(1)}, u32[]{:S(2)}, u32[]{:S(2)}) collective-permute-start(bf16[4,1024]{1,0:T(4,128)(2,1)S(1)} %add_convert_fusion.refs_0_.refs_4_), channel_id=1, source_target_pairs={{0,3},{1,2},{2,1},{3,0},{4,7},{5,6},{6,5},{7,4},{8,11},{9,10},{10,... | collective-permute-start | bytes 24584 | tf_op jit(solution)/shard_map/ppermute | solution.py:617
  37.3 3.2 %collective-permute-start.18 = (f32[4,1024]{1,0:T(4,128)S(1)}, f32[4,1024]{1,0:T(4,128)S(1)}, u32[]{:S(2)}, u32[]{:S(2)}) collective-permute-start(f32[4,1024]{1,0:T(4,128)S(1)} %get-tuple-element.24), channel_id=1, source_target_pairs={{0,3},{1,2},{2,1},{3,0},{4,7},{5,6},{6,5},{7,4},{8,11},{9,10},{10,... | collective-permute-start | bytes 49160 | tf_op jit(solution)/shard_map/ppermute | solution.py:617
  37.4 5.0 %collective-permute-start.17 = (f32[4,1024]{1,0:T(4,128)S(1)}, f32[4,1024]{1,0:T(4,128)S(1)}, u32[]{:S(2)}, u32[]{:S(2)}) collective-permute-start(f32[4,1024]{1,0:T(4,128)S(1)} %get-tuple-element.23), channel_id=1, source_target_pairs={{0,7},{1,6},{2,5},{3,4},{4,3},{5,2},{6,1},{7,0},{8,15},{9,14},{10,... | collective-permute-start | bytes 49160 | tf_op jit(solution)/shard_map/ppermute | solution.py:617
  39.2 4.1 %collective-permute-start.16 = (f32[4,1024]{1,0:T(4,128)S(1)}, f32[4,1024]{1,0:T(4,128)S(1)}, u32[]{:S(2)}, u32[]{:S(2)}) collective-permute-start(f32[4,1024]{1,0:T(4,128)S(1)} %get-tuple-element.22), channel_id=1, source_target_pairs={{0,5},{1,4},{2,7},{3,6},{4,1},{5,0},{6,3},{7,2},{8,13},{9,12},{10,... | collective-permute-start | bytes 49160 | tf_op jit(solution)/shard_map/ppermute | solution.py:617
  43.3 1.2 %collective-permute-start.19 = (f32[4,512]{1,0:T(4,128)S(1)}, f32[4,512]{1,0:T(4,128)S(1)}, u32[]{:S(2)}, u32[]{:S(2)}) collective-permute-start(f32[4,512]{1,0:T(4,128)S(1)} %constant_dynamic-slice_fusion), channel_id=1, source_target_pairs={{0,1},{1,0},{2,3},{3,2},{4,5},{5,4},{6,7},{7,6},{8,9},{9,8},{10,11... | collective-permute-start | bytes 24584 | tf_op jit(solution)/shard_map/ppermute | solution.py:622

commit v2 on v1

--- a/solution.py
+++ b/solution.py
@@ -269,7 +269,24 @@
 LANES = 128
 
 
-def project(tokens, norm_gain, query_weight, key_weight, value_weight, gate_weight):
+def project(
+    tokens,
+    norm_gain,
+    query_weight,
+    key_weight,
+    value_weight,
+    gate_weight,
+    forget_bias,
+    state_normalizer,
+    state_max,
+    block_keys,
+    block_values,
+    block_input,
+    block_logf,
+):
+    _, heads, dk = state_normalizer.shape
+    span, dv = block_values.shape[2:]
+    packed_width = dk + 2 * LANES
     rows, columns = tokens.shape
     size = lax.axis_size("kv")
     weights = (query_weight, key_weight, value_weight)
@@ -279,11 +296,15 @@
     gate_count = gate_weight.shape[1] * gate_weight.shape[2]
     gates = jnp.transpose(gate_weight, (1, 2, 0)).reshape(gate_count, -1)
     cuts = [0, columns]
+    small = (forget_bias.reshape(1, -1), state_normalizer, state_max, block_input, block_logf)
 
     def body(tokens_hbm, gain_hbm, q_hbm, k_hbm, v_hbm, gate_hbm, *rest):
-        outs = rest[:size]
-        tokens_ref, gain_ref, weight_ref, gate_ref, sums_ref = rest[size : size + 5]
-        sems, gate_sem, tokens_sem, gain_sem = rest[size + 5 :]
+        small_hbm, (keys_hbm, values_hbm), rest = rest[:5], rest[5:7], rest[7:]
+        outs, small_out, block_out = rest[:size], rest[size], rest[size + 1]
+        rest = rest[size + 2 :]
+        tokens_ref, gain_ref, weight_ref, gate_ref, sums_ref = rest[:5]
+        sems, gate_sem, tokens_sem, gain_sem, small_sems, block_sems = rest[5:11]
+        small_refs = rest[11:]
         position = lax.axis_index("kv")
         tokens_copy = pltpu.make_async_copy(tokens_hbm, tokens_ref, tokens_sem)
         gain_copy = pltpu.make_async_copy(gain_hbm, gain_ref, gain_sem)
@@ -306,11 +327,37 @@
             gate_sem,
         )
         gate_copy.start()
+        small_copies = [
+            pltpu.make_async_copy(source, target, small_sems.at[i])
+            for i, (source, target) in enumerate(zip(small_hbm, small_refs))
+        ]
+        block_copies = [
+            pltpu.make_async_copy(keys_hbm.at[0], block_out.at[:, :, pl.ds(0, dk)], block_sems.at[0]),
+            pltpu.make_async_copy(
+                values_hbm.at[0], block_out.at[:, :, pl.ds(dk, dv)], block_sems.at[1]
+            ),
+        ]
+        for copy in small_copies + block_copies:
+            copy.start()
         tokens_copy.wait()
         gain_copy.wait()
         widened = tokens_ref[...].astype(jnp.float32)
         squares = jnp.sum(widened * widened, axis=1, keepdims=True)
         normed = (widened * gain_ref[...]).astype(jnp.bfloat16)
+        for copy in small_copies:
+            copy.wait()
+        bias_ref, normalizer_ref, max_ref, input_ref, logf_ref = small_refs
+        lane_h = lax.broadcasted_iota(jnp.int32, (heads, heads), 1)
+        head_h = lax.broadcasted_iota(jnp.int32, (heads, heads), 0)
+
+        def column(ref):
+            values = jnp.broadcast_to(ref[...], (heads, heads))
+            return jnp.sum(jnp.where(lane_h == head_h, values, 0.0), axis=1, keepdims=True)
+
+        lane = lax.broadcasted_iota(jnp.int32, (heads, LANES), 1)
+        small_out[:, :dk] = normalizer_ref[0]
+        small_out[:, dk : dk + LANES] = jnp.concatenate([input_ref[0], logf_ref[0]], axis=1)
+        small_out[:, dk + LANES :] = jnp.where(lane == 0, column(max_ref), column(bias_ref))
         for c in range(len(cuts) - 1):
             piece = normed[:, cuts[c] : cuts[c + 1]]
             for w in range(3):
@@ -324,6 +371,8 @@
                 if c:
                     product = product + sums_ref[:, at]
                 sums_ref[:, at] = product
+        for copy in block_copies:
+            copy.wait()
         gate_copy.wait()
         gate_sums = dot_nt(normed, gate_ref[...])
         pad = jnp.zeros((rows, LANES - gate_count), jnp.float32)
@@ -335,9 +384,24 @@
 
     return call(
         body,
-        [struct((1, width + LANES), jnp.float32)] * size,
-        [ANY_SPEC] * 6,
-        [streamed(a) for a in (tokens, norm_gain.reshape(1, -1), *weights, gates)],
+        [struct((1, width + LANES), jnp.float32)] * size
+        + [
+            struct((heads, packed_width), jnp.float32),
+            struct((heads, span, dk + dv), block_keys.dtype),
+        ],
+        [ANY_SPEC] * 13,
+        [
+            streamed(a)
+            for a in (
+                tokens,
+                norm_gain.reshape(1, -1),
+                *weights,
+                gates,
+                *small,
+                block_keys,
+                block_values,
+            )
+        ],
         [
             pltpu.VMEM(tokens.shape, tokens.dtype),
             pltpu.VMEM((1, columns), norm_gain.dtype),
@@ -348,71 +412,22 @@
             pltpu.SemaphoreType.DMA(()),
             pltpu.SemaphoreType.DMA(()),
             pltpu.SemaphoreType.DMA(()),
+            pltpu.SemaphoreType.DMA((len(small),)),
+            pltpu.SemaphoreType.DMA((2,)),
+            *[pltpu.VMEM(a.shape, a.dtype) for a in small],
         ],
         limit=16,
     )
 
 
-def prepare(forget_bias, state_normalizer, state_max, block_input, block_logf, lengths):
-    _, heads, dk = state_normalizer.shape
-    span = (heads, SPAN_LOCATIONS)
-
-    def body(
-        bias_ref, normalizer_ref, max_ref, input_ref, logf_ref, lengths_ref, out_ref
-    ):
-        live = jnp.broadcast_to(lengths_ref[:, :1] & (SPAN_LOCATIONS - 1), span)
-        inside = lax.broadcasted_iota(jnp.int32, span, 1) < live
-        rest = jnp.where(inside, logf_ref[0], 0.0)
-        square = (SPAN_LOCATIONS, SPAN_LOCATIONS)
-        upto = (
-            lax.broadcasted_iota(jnp.int32, square, 0) <= lax.broadcasted_iota(jnp.int32, square, 1)
-        ).astype(jnp.float32).astype(jnp.bfloat16)
-        cumulative = jnp.zeros(span, jnp.float32)
-        for _ in range(3):
-            term = rest.astype(jnp.bfloat16)
-            rest = rest - term.astype(jnp.float32)
-            cumulative = cumulative + jnp.dot(term, upto, preferred_element_type=jnp.float32)
-        total = cumulative[:, SPAN_LOCATIONS - 1 :]
-        base = jnp.where(inside, total - cumulative + input_ref[0], -jnp.inf)
-        lane_h = lax.broadcasted_iota(jnp.int32, (heads, heads), 1)
-        head_h = lax.broadcasted_iota(jnp.int32, (heads, heads), 0)
-
-        def column(ref):
-            values = jnp.broadcast_to(ref[...], (heads, heads))
-            return jnp.sum(jnp.where(lane_h == head_h, values, 0.0), axis=1, keepdims=True)
-
-        lane = lax.broadcasted_iota(jnp.int32, (heads, LANES), 1)
-        scalars = jnp.where(lane == 0, total, 0.0)
-        scalars = jnp.where(lane == 1, column(max_ref), scalars)
-        scalars = jnp.where(lane == 2, column(bias_ref), scalars)
-        out_ref[:, :dk] = normalizer_ref[0]
-        pad = jnp.zeros((heads, LANES - SPAN_LOCATIONS), jnp.float32)
-        out_ref[:, dk : dk + LANES] = jnp.concatenate([base, pad], axis=1)
-        out_ref[:, dk + LANES :] = scalars
-
-    return call(
-        body,
-        [struct((heads, dk + 2 * LANES), jnp.float32)],
-        [VMEM_SPEC] * 6,
-        [
-            forget_bias.reshape(1, -1),
-            state_normalizer,
-            state_max,
-            block_input,
-            block_logf,
-            jnp.pad(lengths, (0, LANES - 1)).reshape(1, -1),
-        ],
-    )[0]
-
-
-def recall(parts, prepared, state_matrix, block_keys, block_values):
+def recall(parts, small, state_matrix, blocks, lengths):
     _, heads, dv, dk = state_matrix.shape
     all_heads = heads * lax.axis_size("tp")
     scale = dk ** (-0.5)
     count = len(parts)
 
     def body(*refs):
-        small_ref, state_ref, keys_ref, values_ref, out_ref = refs[count:]
+        small_ref, state_ref, blocks_ref, lengths_ref, out_ref = refs[count:]
         half = 1 - lax.axis_index("tp")
         row = refs[0][...]
         for r in refs[1:count]:
@@ -438,10 +453,25 @@
             return jnp.sum(jnp.where(lane == head + first, values, 0.0), axis=1, keepdims=True)
 
         small = small_ref[...]
-        cache_base = small[:, dk : dk + SPAN_LOCATIONS]
-        logf_sum, state_max, bias = (
-            small[:, dk + LANES + i : dk + LANES + i + 1] for i in range(3)
-        )
+        block_input = small[:, dk : dk + SPAN_LOCATIONS]
+        block_logf = small[:, dk + SPAN_LOCATIONS : dk + 2 * SPAN_LOCATIONS]
+        state_max = small[:, dk + LANES : dk + LANES + 1]
+        bias = small[:, dk + LANES + 1 : dk + LANES + 2]
+        span = (heads, SPAN_LOCATIONS)
+        live = jnp.broadcast_to(lengths_ref[:, :1] & (SPAN_LOCATIONS - 1), span)
+        inside = lax.broadcasted_iota(jnp.int32, span, 1) < live
+        rest = jnp.where(inside, block_logf, 0.0)
+        square = (SPAN_LOCATIONS, SPAN_LOCATIONS)
+        upto = (
+            lax.broadcasted_iota(jnp.int32, square, 0) <= lax.broadcasted_iota(jnp.int32, square, 1)
+        ).astype(jnp.float32).astype(jnp.bfloat16)
+        cumulative = jnp.zeros(span, jnp.float32)
+        for _ in range(3):
+            term = rest.astype(jnp.bfloat16)
+            rest = rest - term.astype(jnp.float32)
+            cumulative = cumulative + jnp.dot(term, upto, preferred_element_type=jnp.float32)
+        logf_sum = cumulative[:, SPAN_LOCATIONS - 1 :]
+        cache_base = jnp.where(inside, logf_sum - cumulative + block_input, -jnp.inf)
         new_input = column(gates, half * heads)
         new_logf = jax.nn.log_sigmoid(column(gates, all_heads + half * heads) + bias)
         carried_log = logf_sum + new_logf + state_max
@@ -460,7 +490,7 @@
                 out = jnp.where(rows == h, make(h), out)
             return out
 
-        scores = pick(lambda h: dot_nt(query, keys_ref[0, h]), SPAN_LOCATIONS)
+        scores = pick(lambda h: dot_nt(query, blocks_ref[h, :, :dk]), SPAN_LOCATIONS)
         mixing = (scores * scale * cache_weight).astype(jnp.bfloat16)
         query_wide = query.astype(jnp.float32)
         own_term = (
@@ -477,7 +507,9 @@
 
         carried = pick(carry, dv)
         from_cache = pick(
-            lambda h: jnp.dot(mixing, values_ref[0, h], preferred_element_type=jnp.float32), dv
+            lambda h: jnp.dot(
+                mixing, blocks_ref[h, :, dk:], preferred_element_type=jnp.float32
+            ), dv
         )
         numerator = carried_weight * carried + from_cache + own_term * value.astype(jnp.float32)
         normalizer = (
@@ -492,7 +524,13 @@
         body,
         [struct((heads, dv), jnp.bfloat16)],
         [VMEM_SPEC] * (count + 4),
-        (*parts, prepared, *[resident(w) for w in (state_matrix, block_keys, block_values)]),
+        (
+            *parts,
+            small,
+            resident(state_matrix),
+            blocks,
+            jnp.pad(lengths, (0, LANES - 1)).reshape(1, -1),
+        ),
     )[0]
 
 
@@ -659,16 +697,23 @@
     size = lax.axis_size("kv")
     order = distances(size)
     state_matrix = swapped(state_matrix)
-    parts = project(
-        tokens, norm_gain, query_weight, key_weight, value_weight, gate_weight
-    )
-    prepared = prepare(
-        forget_bias, state_normalizer, state_max, block_input, block_logf, lengths
+    *parts, small, blocks = project(
+        tokens,
+        norm_gain,
+        query_weight,
+        key_weight,
+        value_weight,
+        gate_weight,
+        forget_bias,
+        state_normalizer,
+        state_max,
+        block_keys,
+        block_values,
+        block_input,
+        block_logf,
     )
     parts = to_partners(parts, [*order, 0])
-    hidden = recall(
-        parts, swapped(prepared), state_matrix, swapped(block_keys), swapped(block_values)
-    )
+    hidden = recall(parts, swapped(small), state_matrix, swapped(blocks), lengths)
     pieces = to_partners([hidden] * size, [*order, 0])
     partial_out = attend(pieces, out_weight)
     other_out = swapped(partial_out)

time: 45.3 us -> 40.4 us (0.89)
  local copies, waits for them, and re-layouts: 4.11 us -> 0.05 us
  waiting for transfers between devices: 12.6 us -> 11.5 us
  Pallas kernels: 9.53 us -> 10 us
    unnamed x28 -> x14, local copies, waits for them, and re-layouts: 4.1 us -> 0.04 us
    ppermute x14, waiting for transfers between devices: 10.7 us -> 9.86 us  [to_partners(): received.append(lax.ppermute(outgoing[d], ('kv', 'tp'), pairs))]
    ppermute x14, starting transfers between devices: 15.9 us -> 15.4 us  [to_partners(): received.append(lax.ppermute(outgoing[d], ('kv', 'tp'), pairs))]
    pallas_call x6 -> x5, Pallas kernels: 9.53 us -> 10 us  [call(): pl.pallas_call(body, out_shape=outs, in_specs=in_specs, out_specs=[VMEM_S...]
    ppermute x6 -> x5, starting transfers between devices: 1.55 us -> 1.87 us  [swapped(): return lax.ppermute(array, 'tp', [(0, 1), (1, 0)])]
    ppermute x6 -> x5, waiting for transfers between devices: 1.89 us -> 1.66 us  [swapped(): return lax.ppermute(array, 'tp', [(0, 1), (1, 0)])]
  transfers between devices with their start and end apart: 20 -> 19, of which waited for: 12 -> 11; matrix products, arithmetic and copies ran while one was open for 0% -> 0% of each run, Pallas kernels for 13% -> 16%
where the time goes in v2:
time: 40.4 us; the launch traced here: 40.2 us
  starting transfers between devices  17.3 us (43%)
  waiting for transfers between devices  11.5 us (28%)
  Pallas kernels  10 us (25%)
  between operations  0.77 us (2%)
  other arithmetic  0.62 us (2%)
    ppermute x14, starting transfers between devices, to_partners(): received.append(lax.ppermute(outgoing[d], ('kv', 'tp'), pairs))  15.4 us
    pallas_call x5, Pallas kernels, call(): pl.pallas_call(body, out_shape=outs, in_specs=in_specs, out_specs=[VMEM_S...  10 us
    ppermute x14, waiting for transfers between devices, to_partners(): received.append(lax.ppermute(outgoing[d], ('kv', 'tp'), pairs))  9.86 us
    ppermute x5, starting transfers between devices, swapped(): return lax.ppermute(array, 'tp', [(0, 1), (1, 0)])  1.87 us
    ppermute x5, waiting for transfers between devices, swapped(): return lax.ppermute(array, 'tp', [(0, 1), (1, 0)])  1.66 us
  transfers between devices with their start and end apart: 19, of which 11 were waited for; matrix products, arithmetic and copies ran while one was open for 0% of the time, Pallas kernels for 16%

profile of v2, /device:TPU:0, one launch (start us, length us, event | category | flops | bytes accessed | tf_op | source)
XLA Modules:
  0.0 40.2 jit_solution(6122501736269969712)
XLA Ops:
  0.0 0.5 %collective-permute-start.5 = (f32[1,4,512,256]{3,2,1,0:T(8,128)}, f32[1,4,512,256]{3,2,1,0:T(8,128)S(1)}, u32[]{:S(2)}, u32[]{:S(2)}) collective-permute-start(f32[1,4,512,256]{3,2,1,0:T(8,128)} %param.26), channel_id=1, source_target_pairs={{0,1},{1,0},{2,3},{3,2},{4,5},{5,4},{6,7},{7,6},{8,9},{9,8},{10,11... | collective-permute-start | bytes 6291464 | tf_op jit(solution)/shard_map/ppermute | solution.py:660
  0.5 5.0 %shard_map.181 = (f32[1,4224]{1,0:T(1,128)S(1)}, f32[1,4224]{1,0:T(1,128)S(1)}, f32[1,4224]{1,0:T(1,128)S(1)}, f32[1,4224]{1,0:T(1,128)S(1)}, f32[4,512]{1,0:T(4,128)S(1)}, /*index=5*/bf16[4,64,768]{2,1,0:T(8,128)(2,1)S(1)}) custom-call(bf16[4,1024]{1,0:T(4,128)(2,1)} %tokens_hbm.1, f32[1,1024]{1,0:T(1,128)} %bitcast.15, bf16[1024,1024]{1,0:T(8,128)(2,1)} %q_hbm.1, ...), custom_call_target="tpu_custom_call" | custom-call | flops 20000000000 | bytes 1000000 | tf_op jit(solution)/shard_map/pallas_call | solution.py:245
  5.5 0.1 collective-permute-start.6
  5.6 3.7 %collective-permute-start = (f32[1,4224]{1,0:T(1,128)S(1)}, f32[1,4224]{1,0:T(1,128)S(1)}, u32[]{:S(2)}, u32[]{:S(2)}) collective-permute-start(f32[1,4224]{1,0:T(1,128)S(1)} %get-tuple-element.17), channel_id=1, source_target_pairs={{0,5},{1,4},{2,7},{3,6},{4,1},{5,0},{6,3},{7,2},{8,13},{9,12},{10,... | collective-permute-start | bytes 50696 | tf_op jit(solution)/shard_map/ppermute | solution.py:655
  9.4 0.4 %collective-permute-start.4 = (f32[4,512]{1,0:T(4,128)S(1)}, f32[4,512]{1,0:T(4,128)S(1)}, u32[]{:S(2)}, u32[]{:S(2)}) collective-permute-start(f32[4,512]{1,0:T(4,128)S(1)} %get-tuple-element.21), channel_id=1, source_target_pairs={{0,1},{1,0},{2,3},{3,2},{4,5},{5,4},{6,7},{7,6},{8,9},{9,8},{10,11... | collective-permute-start | bytes 24584 | tf_op jit(solution)/shard_map/ppermute | solution.py:660
  9.8 1.0 %collective-permute-start.1 = (f32[1,4224]{1,0:T(1,128)S(1)}, f32[1,4224]{1,0:T(1,128)S(1)}, u32[]{:S(2)}, u32[]{:S(2)}) collective-permute-start(f32[1,4224]{1,0:T(1,128)S(1)} %get-tuple-element.18), channel_id=1, source_target_pairs={{0,7},{1,6},{2,5},{3,4},{4,3},{5,2},{6,1},{7,0},{8,15},{9,14},{10,... | collective-permute-start | bytes 50696 | tf_op jit(solution)/shard_map/ppermute | solution.py:655
  11.5 0.0 collective-permute-done.4.refs_4_
  11.5 0.7 %collective-permute-start.2 = (f32[1,4224]{1,0:T(1,128)S(1)}, f32[1,4224]{1,0:T(1,128)S(1)}, u32[]{:S(2)}, u32[]{:S(2)}) collective-permute-start(f32[1,4224]{1,0:T(1,128)S(1)} %get-tuple-element.19), channel_id=1, source_target_pairs={{0,3},{1,2},{2,1},{3,0},{4,7},{5,6},{6,5},{7,4},{8,11},{9,10},{10,... | collective-permute-start | bytes 50696 | tf_op jit(solution)/shard_map/ppermute | solution.py:655
  12.2 0.0 collective-permute-done.refs_0_
  12.2 0.2 collective-permute-start.3
  12.3 0.0 copy-start
  12.3 2.5 %collective-permute-done.1.refs_1_ = f32[1,4224]{1,0:T(1,128)S(1)} collective-permute-done((f32[1,4224]{1,0:T(1,128)S(1)}, f32[1,4224]{1,0:T(1,128)S(1)}, u32[]{:S(2)}, u32[]{:S(2)}) %collective-permute-start.1) | collective-permute-done | bytes 16928 | tf_op jit(solution)/shard_map/ppermute | solution.py:655
  14.9 0.2 collective-permute-done.2.refs_2_
  15.1 0.0 collective-permute-done.3.refs_3_
  15.1 0.0 collective-permute-done.6.refs_6_
  15.1 0.0 collective-permute-done.5.refs_5_
  15.1 0.0 slice-start
  15.1 0.8 %shard_map.182 = bf16[4,512]{1,0:T(4,128)(2,1)S(1)} custom-call(f32[1,4224]{1,0:T(1,128)S(1)} %collective-permute-done.refs_0_, f32[1,4224]{1,0:T(1,128)S(1)} %collective-permute-done.1.refs_1_, f32[1,4224]{1,0:T(1,128)S(1)} %collective-permute-done.2.refs_2_, f32[1,4224]{1,0:T(1,128)S(1)} %collective-permute-done.3.refs_3_, ...), custom_call_target="tpu_custom_call" | custom-call | flops 20000000000 | bytes 1000000 | tf_op jit(solution)/shard_map/pallas_call | solution.py:245
  15.9 0.0 copy-start.2
  16.0 0.0 slice-start.1
  16.0 0.0 copy-start.1
  16.0 0.2 collective-permute-start.10
  16.2 1.3 %collective-permute-start.7 = (bf16[4,512]{1,0:T(4,128)(2,1)S(1)}, bf16[4,512]{1,0:T(4,128)(2,1)S(1)}, u32[]{:S(2)}, u32[]{:S(2)}) collective-permute-start(bf16[4,512]{1,0:T(4,128)(2,1)S(1)} %shard_map.182), channel_id=1, source_target_pairs={{0,5},{1,4},{2,7},{3,6},{4,1},{5,0},{6,3},{7,2},{8,13},{9,12},{10,... | collective-permute-start | bytes 12296 | tf_op jit(solution)/shard_map/ppermute | solution.py:655
  17.5 1.3 %collective-permute-start.8 = (bf16[4,512]{1,0:T(4,128)(2,1)S(1)}, bf16[4,512]{1,0:T(4,128)(2,1)S(1)}, u32[]{:S(2)}, u32[]{:S(2)}) collective-permute-start(bf16[4,512]{1,0:T(4,128)(2,1)S(1)} %shard_map.182), channel_id=1, source_target_pairs={{0,7},{1,6},{2,5},{3,4},{4,3},{5,2},{6,1},{7,0},{8,15},{9,14},{10,... | collective-permute-start | bytes 12296 | tf_op jit(solution)/shard_map/ppermute | solution.py:655
  18.8 0.6 %collective-permute-start.9 = (bf16[4,512]{1,0:T(4,128)(2,1)S(1)}, bf16[4,512]{1,0:T(4,128)(2,1)S(1)}, u32[]{:S(2)}, u32[]{:S(2)}) collective-permute-start(bf16[4,512]{1,0:T(4,128)(2,1)S(1)} %shard_map.182), channel_id=1, source_target_pairs={{0,3},{1,2},{2,1},{3,0},{4,7},{5,6},{6,5},{7,4},{8,11},{9,10},{10,... | collective-permute-start | bytes 12296 | tf_op jit(solution)/shard_map/ppermute | solution.py:655
  19.4 0.0 collective-permute-done.10.refs_3_
  19.4 0.7 %collective-permute-done.7.refs_0_ = bf16[4,512]{1,0:T(4,128)(2,1)S(1)} collective-permute-done((bf16[4,512]{1,0:T(4,128)(2,1)S(1)}, bf16[4,512]{1,0:T(4,128)(2,1)S(1)}, u32[]{:S(2)}, u32[]{:S(2)}) %collective-permute-start.7) | collective-permute-done | bytes 4128 | tf_op jit(solution)/shard_map/ppermute | solution.py:655
  20.1 2.2 %collective-permute-done.8.refs_1_ = bf16[4,512]{1,0:T(4,128)(2,1)S(1)} collective-permute-done((bf16[4,512]{1,0:T(4,128)(2,1)S(1)}, bf16[4,512]{1,0:T(4,128)(2,1)S(1)}, u32[]{:S(2)}, u32[]{:S(2)}) %collective-permute-start.8) | collective-permute-done | bytes 4128 | tf_op jit(solution)/shard_map/ppermute | solution.py:655
  22.3 0.0 collective-permute-done.9.refs_2_
  22.3 0.0 copy-done
  22.3 0.0 slice-start.2
  22.3 0.6 %shard_map.183 = bf16[4,1024]{1,0:T(4,128)(2,1)S(1)} custom-call(bf16[4,512]{1,0:T(4,128)(2,1)S(1)} %collective-permute-done.7.refs_0_, bf16[4,512]{1,0:T(4,128)(2,1)S(1)} %collective-permute-done.8.refs_1_, bf16[4,512]{1,0:T(4,128)(2,1)S(1)} %collective-permute-done.9.refs_2_, bf16[4,512]{1,0:T(4,128)(2,1)S(1)} %collective-permute-done.10.refs_3_, ...), custom_call_target="tpu_custom_call" | custom-call | flops 20000000000 | bytes 1000000 | tf_op jit(solution)/shard_map/pallas_call | solution.py:245
  23.0 0.0 slice-start.3
  23.0 0.4 %collective-permute-start.11 = (bf16[4,1024]{1,0:T(4,128)(2,1)S(1)}, bf16[4,1024]{1,0:T(4,128)(2,1)S(1)}, u32[]{:S(2)}, u32[]{:S(2)}) collective-permute-start(bf16[4,1024]{1,0:T(4,128)(2,1)S(1)} %shard_map.183), channel_id=1, source_target_pairs={{0,1},{1,0},{2,3},{3,2},{4,5},{5,4},{6,7},{7,6},{8,9},{9,8},{10,11... | collective-permute-start | bytes 24584 | tf_op jit(solution)/shard_map/ppermute | solution.py:660
  23.4 0.8 %collective-permute-done.11 = bf16[4,1024]{1,0:T(4,128)(2,1)S(1)} collective-permute-done((bf16[4,1024]{1,0:T(4,128)(2,1)S(1)}, bf16[4,1024]{1,0:T(4,128)(2,1)S(1)}, u32[]{:S(2)}, u32[]{:S(2)}) %collective-permute-start.11) | collective-permute-done | bytes 8224 | tf_op jit(solution)/shard_map/ppermute | solution.py:660
  24.3 0.0 copy-done.2
  24.3 0.8 %collective-permute-start.14 = (bf16[4,1024]{1,0:T(4,128)(2,1)S(1)}, bf16[4,1024]{1,0:T(4,128)(2,1)S(1)}, u32[]{:S(2)}, u32[]{:S(2)}) collective-permute-start(bf16[4,1024]{1,0:T(4,128)(2,1)S(1)} %add_convert_fusion.refs_0_.refs_4_), channel_id=1, source_target_pairs={{0,5},{1,4},{2,7},{3,6},{4,1},{5,0},{6,3},{7,2},{8,13},{9,12},{10,... | collective-permute-start | bytes 24584 | tf_op jit(solution)/shard_map/ppermute | solution.py:655
  25.1 1.4 %collective-permute-start.12 = (bf16[4,1024]{1,0:T(4,128)(2,1)S(1)}, bf16[4,1024]{1,0:T(4,128)(2,1)S(1)}, u32[]{:S(2)}, u32[]{:S(2)}) collective-permute-start(bf16[4,1024]{1,0:T(4,128)(2,1)S(1)} %add_convert_fusion.refs_0_.refs_4_), channel_id=1, source_target_pairs={{0,7},{1,6},{2,5},{3,4},{4,3},{5,2},{6,1},{7,0},{8,15},{9,14},{10,... | collective-permute-start | bytes 24584 | tf_op jit(solution)/shard_map/ppermute | solution.py:655
  26.5 1.0 %collective-permute-start.13 = (bf16[4,1024]{1,0:T(4,128)(2,1)S(1)}, bf16[4,1024]{1,0:T(4,128)(2,1)S(1)}, u32[]{:S(2)}, u32[]{:S(2)}) collective-permute-start(bf16[4,1024]{1,0:T(4,128)(2,1)S(1)} %add_convert_fusion.refs_0_.refs_4_), channel_id=1, source_target_pairs={{0,3},{1,2},{2,1},{3,0},{4,7},{5,6},{6,5},{7,4},{8,11},{9,10},{10,... | collective-permute-start | bytes 24584 | tf_op jit(solution)/shard_map/ppermute | solution.py:655
  27.5 0.9 %collective-permute-done.14.refs_1_ = bf16[4,1024]{1,0:T(4,128)(2,1)S(1)} collective-permute-done((bf16[4,1024]{1,0:T(4,128)(2,1)S(1)}, bf16[4,1024]{1,0:T(4,128)(2,1)S(1)}, u32[]{:S(2)}, u32[]{:S(2)}) %collective-permute-start.14) | collective-permute-done | bytes 8224 | tf_op jit(solution)/shard_map/ppermute | solution.py:655
  28.4 0.0 slice-done
  28.4 0.0 slice-done.1
  28.4 0.0 copy-done.1
  28.4 1.2 %shard_map.184 = (f32[4,1024]{1,0:T(4,128)S(1)}, f32[4,128]{1,0:T(4,128)S(1)}) custom-call(bf16[4,1024]{1,0:T(4,128)(2,1)S(1)} %add_convert_fusion.refs_0_.refs_4_, bf16[4,1024]{1,0:T(4,128)(2,1)S(1)} %collective-permute-done.14.refs_1_, f32[1,4096]{1,0:T(1,128)S(1)} %bitcast.12, bf16[1024,4096]{1,0:T(8,128)(2,1)S(1)} %bitcast.9), custom_call_target="tpu_custom_call" | custom-call | flops 20000000000 | bytes 1000000 | tf_op jit(solution)/shard_map/pallas_call | solution.py:245
  29.6 0.3 collective-permute-done.12.refs_0_
  30.0 0.0 collective-permute-done.13.refs_1_
  30.0 0.0 slice-done.2
  30.0 0.0 slice-done.3
  30.0 2.3 %shard_map.185 = (f32[4,1024]{1,0:T(4,128)S(1)}, f32[4,1024]{1,0:T(4,128)S(1)}, f32[4,1024]{1,0:T(4,128)S(1)}, f32[4,1024]{1,0:T(4,128)S(1)}) custom-call(bf16[4,1024]{1,0:T(4,128)(2,1)S(1)} %collective-permute-done.12.refs_0_, bf16[4,1024]{1,0:T(4,128)(2,1)S(1)} %collective-permute-done.13.refs_1_, f32[4,1024]{1,0:T(4,128)S(1)} %get-tuple-element.23.refs_2_, ...), custom_call_target="tpu_custom_call" | custom-call | flops 20000000000 | bytes 1000000 | tf_op jit(solution)/shard_map/pallas_call | solution.py:245
  32.3 0.9 %collective-permute-start.15 = (f32[4,1024]{1,0:T(4,128)S(1)}, f32[4,1024]{1,0:T(4,128)S(1)}, u32[]{:S(2)}, u32[]{:S(2)}) collective-permute-start(f32[4,1024]{1,0:T(4,128)S(1)} %get-tuple-element.26), channel_id=1, source_target_pairs={{0,5},{1,4},{2,7},{3,6},{4,1},{5,0},{6,3},{7,2},{8,13},{9,12},{10,... | collective-permute-start | bytes 49160 | tf_op jit(solution)/shard_map/ppermute | solution.py:655
  33.2 1.8 %collective-permute-start.16 = (f32[4,1024]{1,0:T(4,128)S(1)}, f32[4,1024]{1,0:T(4,128)S(1)}, u32[]{:S(2)}, u32[]{:S(2)}) collective-permute-start(f32[4,1024]{1,0:T(4,128)S(1)} %get-tuple-element.27), channel_id=1, source_target_pairs={{0,7},{1,6},{2,5},{3,4},{4,3},{5,2},{6,1},{7,0},{8,15},{9,14},{10,... | collective-permute-start | bytes 49160 | tf_op jit(solution)/shard_map/ppermute | solution.py:655
  35.0 0.4 %collective-permute-start.17 = (f32[4,1024]{1,0:T(4,128)S(1)}, f32[4,1024]{1,0:T(4,128)S(1)}, u32[]{:S(2)}, u32[]{:S(2)}) collective-permute-start(f32[4,1024]{1,0:T(4,128)S(1)} %get-tuple-element.28), channel_id=1, source_target_pairs={{0,3},{1,2},{2,1},{3,0},{4,7},{5,6},{6,5},{7,4},{8,11},{9,10},{10,... | collective-permute-start | bytes 49160 | tf_op jit(solution)/shard_map/ppermute | solution.py:655
  35.5 0.9 %collective-permute-done.15 = f32[4,1024]{1,0:T(4,128)S(1)} collective-permute-done((f32[4,1024]{1,0:T(4,128)S(1)}, f32[4,1024]{1,0:T(4,128)S(1)}, u32[]{:S(2)}, u32[]{:S(2)}) %collective-permute-start.15) | collective-permute-done | bytes 16416 | tf_op jit(solution)/shard_map/ppermute | solution.py:655
  36.4 1.8 %collective-permute-done.16 = f32[4,1024]{1,0:T(4,128)S(1)} collective-permute-done((f32[4,1024]{1,0:T(4,128)S(1)}, f32[4,1024]{1,0:T(4,128)S(1)}, u32[]{:S(2)}, u32[]{:S(2)}) %collective-permute-start.16) | collective-permute-done | bytes 16416 | tf_op jit(solution)/shard_map/ppermute | solution.py:655
  38.2 0.2 collective-permute-done.17
  38.4 0.4 %collective-permute-start.18 = (f32[4,512]{1,0:T(4,128)S(1)}, f32[4,512]{1,0:T(4,128)S(1)}, u32[]{:S(2)}, u32[]{:S(2)}) collective-permute-start(f32[4,512]{1,0:T(4,128)S(1)} %constant_dynamic-slice_fusion), channel_id=1, source_target_pairs={{0,1},{1,0},{2,3},{3,2},{4,5},{5,4},{6,7},{7,6},{8,9},{9,8},{10,11... | collective-permute-start | bytes 24584 | tf_op jit(solution)/shard_map/ppermute | solution.py:660
  38.8 0.8 %collective-permute-done.18 = f32[4,512]{1,0:T(4,128)S(1)} collective-permute-done((f32[4,512]{1,0:T(4,128)S(1)}, f32[4,512]{1,0:T(4,128)S(1)}, u32[]{:S(2)}, u32[]{:S(2)}) %collective-permute-start.18) | collective-permute-done | bytes 8224 | tf_op jit(solution)/shard_map/ppermute | solution.py:660
  39.7 0.6 %add_convert_fusion.1 = bf16[4,512]{1,0:T(4,128)(2,1)} fusion(f32[4,512]{1,0:T(4,128)S(1)} %collective-permute-done.18, f32[4,1024]{1,0:T(4,128)S(1)} %add_add_fusion, s32[]{:T(128)S(6)} %select_n.6), kind=kLoop, calls=%fused_computation.2 | loop fusion | flops 4096 | bytes 20484 | tf_op jit(solution)/shard_map/convert_element_type | solution.py:737
  (6 shorter events, 0.0 us)
Async XLA Ops:
  0.0 15.1 %collective-permute-start.5 = (f32[1,4,512,256]{3,2,1,0:T(8,128)}, f32[1,4,512,256]{3,2,1,0:T(8,128)S(1)}, u32[]{:S(2)}, u32[]{:S(2)}) collective-permute-start(f32[1,4,512,256]{3,2,1,0:T(8,128)} %param.26), channel_id=1, source_target_pairs={{0,1},{1,0},{2,3},{3,2},{4,5},{5,4},{6,7},{7,6},{8,9},{9,8},{10,11... | collective-permute-start | bytes 6291464 | tf_op jit(solution)/shard_map/ppermute | solution.py:660
  5.5 9.6 %collective-permute-start.6 = (bf16[4,64,768]{2,1,0:T(8,128)(2,1)S(1)}, bf16[4,64,768]{2,1,0:T(8,128)(2,1)S(1)}, u32[]{:S(2)}, u32[]{:S(2)}) collective-permute-start(bf16[4,64,768]{2,1,0:T(8,128)(2,1)S(1)} %get-tuple-element.22), channel_id=1, source_target_pairs={{0,1},{1,0},{2,3},{3,2},{4,5},{5,4},{6,7},{7,6},{8,9},{9,8},{10,11... | collective-permute-start | bytes 1179656 | tf_op jit(solution)/shard_map/ppermute | solution.py:660
  5.6 6.5 %collective-permute-start = (f32[1,4224]{1,0:T(1,128)S(1)}, f32[1,4224]{1,0:T(1,128)S(1)}, u32[]{:S(2)}, u32[]{:S(2)}) collective-permute-start(f32[1,4224]{1,0:T(1,128)S(1)} %get-tuple-element.17), channel_id=1, source_target_pairs={{0,5},{1,4},{2,7},{3,6},{4,1},{5,0},{6,3},{7,2},{8,13},{9,12},{10,... | collective-permute-start | bytes 50696 | tf_op jit(solution)/shard_map/ppermute | solution.py:655
  9.4 2.1 %collective-permute-start.4 = (f32[4,512]{1,0:T(4,128)S(1)}, f32[4,512]{1,0:T(4,128)S(1)}, u32[]{:S(2)}, u32[]{:S(2)}) collective-permute-start(f32[4,512]{1,0:T(4,128)S(1)} %get-tuple-element.21), channel_id=1, source_target_pairs={{0,1},{1,0},{2,3},{3,2},{4,5},{5,4},{6,7},{7,6},{8,9},{9,8},{10,11... | collective-permute-start | bytes 24584 | tf_op jit(solution)/shard_map/ppermute | solution.py:660
  9.8 5.1 %collective-permute-start.1 = (f32[1,4224]{1,0:T(1,128)S(1)}, f32[1,4224]{1,0:T(1,128)S(1)}, u32[]{:S(2)}, u32[]{:S(2)}) collective-permute-start(f32[1,4224]{1,0:T(1,128)S(1)} %get-tuple-element.18), channel_id=1, source_target_pairs={{0,7},{1,6},{2,5},{3,4},{4,3},{5,2},{6,1},{7,0},{8,15},{9,14},{10,... | collective-permute-start | bytes 50696 | tf_op jit(solution)/shard_map/ppermute | solution.py:655
  11.5 3.6 %collective-permute-start.2 = (f32[1,4224]{1,0:T(1,128)S(1)}, f32[1,4224]{1,0:T(1,128)S(1)}, u32[]{:S(2)}, u32[]{:S(2)}) collective-permute-start(f32[1,4224]{1,0:T(1,128)S(1)} %get-tuple-element.19), channel_id=1, source_target_pairs={{0,3},{1,2},{2,1},{3,0},{4,7},{5,6},{6,5},{7,4},{8,11},{9,10},{10,... | collective-permute-start | bytes 50696 | tf_op jit(solution)/shard_map/ppermute | solution.py:655
  12.2 2.9 %collective-permute-start.3 = (f32[1,4224]{1,0:T(1,128)S(1)}, f32[1,4224]{1,0:T(1,128)S(1)}, u32[]{:S(2)}, u32[]{:S(2)}) collective-permute-start(f32[1,4224]{1,0:T(1,128)S(1)} %get-tuple-element.20), channel_id=1, source_target_pairs={{0,1},{1,0},{2,3},{3,2},{4,5},{5,4},{6,7},{7,6},{8,9},{9,8},{10,11... | collective-permute-start | bytes 50696 | tf_op jit(solution)/shard_map/ppermute | solution.py:655
  12.3 10.0 %copy-start = (bf16[2048,1024]{1,0:T(8,128)(2,1)S(1)}, bf16[2048,1024]{1,0:T(8,128)(2,1)}, u32[]{:S(2)}) copy-start(bf16[2048,1024]{1,0:T(8,128)(2,1)} %refs_4_.1) | copy-start | bytes 12582916
  15.1 13.3 %slice-start = ((s8[8388608]{0:T(1024)(128)(4,1)}), s8[4194304]{0:T(1024)(128)(4,1)S(1)}, s32[]{:S(2)}) async-start(s8[8388608]{0:T(1024)(128)(4,1)} %bitcast.8), calls=%async_computation | async-start | bytes 8388608
  15.9 8.3 %copy-start.2 = (bf16[4,1024]{1,0:T(4,128)(2,1)S(1)}, bf16[4,1024]{1,0:T(4,128)(2,1)}, u32[]{:S(2)}) copy-start(bf16[4,1024]{1,0:T(4,128)(2,1)} %tokens_hbm.1) | copy-start | bytes 24580
  16.0 12.5 %slice-start.1 = ((s8[8388608]{0:T(1024)(128)(4,1)}), s8[4194304]{0:T(1024)(128)(4,1)S(1)}, s32[]{:S(2)}) async-start(s8[8388608]{0:T(1024)(128)(4,1)} %bitcast.8), calls=%async_computation.1 | async-start | bytes 8388608
  16.0 12.4 %copy-start.1 = (f32[4096]{0:T(1024)S(1)}, f32[4096]{0:T(1024)}, u32[]{:S(2)}) copy-start(f32[4096]{0:T(1024)} %param.35) | copy-start | bytes 49156
  16.0 3.4 %collective-permute-start.10 = (bf16[4,512]{1,0:T(4,128)(2,1)S(1)}, bf16[4,512]{1,0:T(4,128)(2,1)S(1)}, u32[]{:S(2)}, u32[]{:S(2)}) collective-permute-start(bf16[4,512]{1,0:T(4,128)(2,1)S(1)} %shard_map.182), channel_id=1, source_target_pairs={{0,1},{1,0},{2,3},{3,2},{4,5},{5,4},{6,7},{7,6},{8,9},{9,8},{10,11... | collective-permute-start | bytes 12296 | tf_op jit(solution)/shard_map/ppermute | solution.py:655
  16.2 3.9 %collective-permute-start.7 = (bf16[4,512]{1,0:T(4,128)(2,1)S(1)}, bf16[4,512]{1,0:T(4,128)(2,1)S(1)}, u32[]{:S(2)}, u32[]{:S(2)}) collective-permute-start(bf16[4,512]{1,0:T(4,128)(2,1)S(1)} %shard_map.182), channel_id=1, source_target_pairs={{0,5},{1,4},{2,7},{3,6},{4,1},{5,0},{6,3},{7,2},{8,13},{9,12},{10,... | collective-permute-start | bytes 12296 | tf_op jit(solution)/shard_map/ppermute | solution.py:655
  17.5 4.8 %collective-permute-start.8 = (bf16[4,512]{1,0:T(4,128)(2,1)S(1)}, bf16[4,512]{1,0:T(4,128)(2,1)S(1)}, u32[]{:S(2)}, u32[]{:S(2)}) collective-permute-start(bf16[4,512]{1,0:T(4,128)(2,1)S(1)} %shard_map.182), channel_id=1, source_target_pairs={{0,7},{1,6},{2,5},{3,4},{4,3},{5,2},{6,1},{7,0},{8,15},{9,14},{10,... | collective-permute-start | bytes 12296 | tf_op jit(solution)/shard_map/ppermute | solution.py:655
  18.8 3.6 %collective-permute-start.9 = (bf16[4,512]{1,0:T(4,128)(2,1)S(1)}, bf16[4,512]{1,0:T(4,128)(2,1)S(1)}, u32[]{:S(2)}, u32[]{:S(2)}) collective-permute-start(bf16[4,512]{1,0:T(4,128)(2,1)S(1)} %shard_map.182), channel_id=1, source_target_pairs={{0,3},{1,2},{2,1},{3,0},{4,7},{5,6},{6,5},{7,4},{8,11},{9,10},{10,... | collective-permute-start | bytes 12296 | tf_op jit(solution)/shard_map/ppermute | solution.py:655
  22.3 7.6 %slice-start.2 = ((s8[8388608]{0:T(1024)(128)(4,1)}), s8[4194304]{0:T(1024)(128)(4,1)S(1)}, s32[]{:S(2)}) async-start(s8[8388608]{0:T(1024)(128)(4,1)} %bitcast.10), calls=%async_computation.2 | async-start | bytes 8388608
  23.0 7.0 %slice-start.3 = ((s8[8388608]{0:T(1024)(128)(4,1)}), s8[4194304]{0:T(1024)(128)(4,1)S(1)}, s32[]{:S(2)}) async-start(s8[8388608]{0:T(1024)(128)(4,1)} %bitcast.10), calls=%async_computation.3 | async-start | bytes 8388608
  23.0 1.3 %collective-permute-start.11 = (bf16[4,1024]{1,0:T(4,128)(2,1)S(1)}, bf16[4,1024]{1,0:T(4,128)(2,1)S(1)}, u32[]{:S(2)}, u32[]{:S(2)}) collective-permute-start(bf16[4,1024]{1,0:T(4,128)(2,1)S(1)} %shard_map.183), channel_id=1, source_target_pairs={{0,1},{1,0},{2,3},{3,2},{4,5},{5,4},{6,7},{7,6},{8,9},{9,8},{10,11... | collective-permute-start | bytes 24584 | tf_op jit(solution)/shard_map/ppermute | solution.py:660
  24.3 4.1 %collective-permute-start.14 = (bf16[4,1024]{1,0:T(4,128)(2,1)S(1)}, bf16[4,1024]{1,0:T(4,128)(2,1)S(1)}, u32[]{:S(2)}, u32[]{:S(2)}) collective-permute-start(bf16[4,1024]{1,0:T(4,128)(2,1)S(1)} %add_convert_fusion.refs_0_.refs_4_), channel_id=1, source_target_pairs={{0,5},{1,4},{2,7},{3,6},{4,1},{5,0},{6,3},{7,2},{8,13},{9,12},{10,... | collective-permute-start | bytes 24584 | tf_op jit(solution)/shard_map/ppermute | solution.py:655
  25.1 4.9 %collective-permute-start.12 = (bf16[4,1024]{1,0:T(4,128)(2,1)S(1)}, bf16[4,1024]{1,0:T(4,128)(2,1)S(1)}, u32[]{:S(2)}, u32[]{:S(2)}) collective-permute-start(bf16[4,1024]{1,0:T(4,128)(2,1)S(1)} %add_convert_fusion.refs_0_.refs_4_), channel_id=1, source_target_pairs={{0,7},{1,6},{2,5},{3,4},{4,3},{5,2},{6,1},{7,0},{8,15},{9,14},{10,... | collective-permute-start | bytes 24584 | tf_op jit(solution)/shard_map/ppermute | solution.py:655
  26.5 3.5 %collective-permute-start.13 = (bf16[4,1024]{1,0:T(4,128)(2,1)S(1)}, bf16[4,1024]{1,0:T(4,128)(2,1)S(1)}, u32[]{:S(2)}, u32[]{:S(2)}) collective-permute-start(bf16[4,1024]{1,0:T(4,128)(2,1)S(1)} %add_convert_fusion.refs_0_.refs_4_), channel_id=1, source_target_pairs={{0,3},{1,2},{2,1},{3,0},{4,7},{5,6},{6,5},{7,4},{8,11},{9,10},{10,... | collective-permute-start | bytes 24584 | tf_op jit(solution)/shard_map/ppermute | solution.py:655
  32.3 4.1 %collective-permute-start.15 = (f32[4,1024]{1,0:T(4,128)S(1)}, f32[4,1024]{1,0:T(4,128)S(1)}, u32[]{:S(2)}, u32[]{:S(2)}) collective-permute-start(f32[4,1024]{1,0:T(4,128)S(1)} %get-tuple-element.26), channel_id=1, source_target_pairs={{0,5},{1,4},{2,7},{3,6},{4,1},{5,0},{6,3},{7,2},{8,13},{9,12},{10,... | collective-permute-start | bytes 49160 | tf_op jit(solution)/shard_map/ppermute | solution.py:655
  33.2 5.0 %collective-permute-start.16 = (f32[4,1024]{1,0:T(4,128)S(1)}, f32[4,1024]{1,0:T(4,128)S(1)}, u32[]{:S(2)}, u32[]{:S(2)}) collective-permute-start(f32[4,1024]{1,0:T(4,128)S(1)} %get-tuple-element.27), channel_id=1, source_target_pairs={{0,7},{1,6},{2,5},{3,4},{4,3},{5,2},{6,1},{7,0},{8,15},{9,14},{10,... | collective-permute-start | bytes 49160 | tf_op jit(solution)/shard_map/ppermute | solution.py:655
  35.0 3.3 %collective-permute-start.17 = (f32[4,1024]{1,0:T(4,128)S(1)}, f32[4,1024]{1,0:T(4,128)S(1)}, u32[]{:S(2)}, u32[]{:S(2)}) collective-permute-start(f32[4,1024]{1,0:T(4,128)S(1)} %get-tuple-element.28), channel_id=1, source_target_pairs={{0,3},{1,2},{2,1},{3,0},{4,7},{5,6},{6,5},{7,4},{8,11},{9,10},{10,... | collective-permute-start | bytes 49160 | tf_op jit(solution)/shard_map/ppermute | solution.py:655
  38.4 1.2 %collective-permute-start.18 = (f32[4,512]{1,0:T(4,128)S(1)}, f32[4,512]{1,0:T(4,128)S(1)}, u32[]{:S(2)}, u32[]{:S(2)}) collective-permute-start(f32[4,512]{1,0:T(4,128)S(1)} %constant_dynamic-slice_fusion), channel_id=1, source_target_pairs={{0,1},{1,0},{2,3},{3,2},{4,5},{5,4},{6,7},{7,6},{8,9},{9,8},{10,11... | collective-permute-start | bytes 24584 | tf_op jit(solution)/shard_map/ppermute | solution.py:660

commit v3 on v2

--- a/solution.py
+++ b/solution.py
@@ -344,20 +344,6 @@
         widened = tokens_ref[...].astype(jnp.float32)
         squares = jnp.sum(widened * widened, axis=1, keepdims=True)
         normed = (widened * gain_ref[...]).astype(jnp.bfloat16)
-        for copy in small_copies:
-            copy.wait()
-        bias_ref, normalizer_ref, max_ref, input_ref, logf_ref = small_refs
-        lane_h = lax.broadcasted_iota(jnp.int32, (heads, heads), 1)
-        head_h = lax.broadcasted_iota(jnp.int32, (heads, heads), 0)
-
-        def column(ref):
-            values = jnp.broadcast_to(ref[...], (heads, heads))
-            return jnp.sum(jnp.where(lane_h == head_h, values, 0.0), axis=1, keepdims=True)
-
-        lane = lax.broadcasted_iota(jnp.int32, (heads, LANES), 1)
-        small_out[:, :dk] = normalizer_ref[0]
-        small_out[:, dk : dk + LANES] = jnp.concatenate([input_ref[0], logf_ref[0]], axis=1)
-        small_out[:, dk + LANES :] = jnp.where(lane == 0, column(max_ref), column(bias_ref))
         for c in range(len(cuts) - 1):
             piece = normed[:, cuts[c] : cuts[c + 1]]
             for w in range(3):
@@ -379,6 +365,20 @@
         extra = jnp.concatenate([gate_sums, pad], axis=1)
         lane = lax.broadcasted_iota(jnp.int32, (rows, LANES), 1)
         sums_ref[:, width:] = jnp.where(lane == gate_count, squares, extra)
+        for copy in small_copies:
+            copy.wait()
+        bias_ref, normalizer_ref, max_ref, input_ref, logf_ref = small_refs
+        lane_h = lax.broadcasted_iota(jnp.int32, (heads, heads), 1)
+        head_h = lax.broadcasted_iota(jnp.int32, (heads, heads), 0)
+
+        def column(ref):
+            values = jnp.broadcast_to(ref[...], (heads, heads))
+            return jnp.sum(jnp.where(lane_h == head_h, values, 0.0), axis=1, keepdims=True)
+
+        lane_s = lax.broadcasted_iota(jnp.int32, (heads, LANES), 1)
+        small_out[:, :dk] = normalizer_ref[0]
+        small_out[:, dk : dk + LANES] = jnp.concatenate([input_ref[0], logf_ref[0]], axis=1)
+        small_out[:, dk + LANES :] = jnp.where(lane_s == 0, column(max_ref), column(bias_ref))
         for d in range(size):
             outs[d][...] = sums_ref[pl.ds(partner_of(position, size, d, False), 1), :]
 
@@ -500,10 +500,7 @@
         )
 
         def carry(h):
-            state = state_ref[0, h]
-            high = state.astype(jnp.bfloat16)
-            low = (state - high.astype(jnp.float32)).astype(jnp.bfloat16)
-            return dot_nt(query, high) + dot_nt(query, low)
+            return dot_nt(query, state_ref[0, h].astype(jnp.bfloat16))
 
         carried = pick(carry, dv)
         from_cache = pick(
@@ -605,7 +602,7 @@
     size = lax.axis_size("kv")
     count = len(pieces)
     rows, columns = residual.shape
-    blocks = [*distances(size), 0]
+    blocks = [*around(size), 0]
     share = columns // 2
 
     def body(*refs):
@@ -617,7 +614,7 @@
         scaled = product * lax.rsqrt(squares / D + epsilon)
         activated = jnp.square(jnp.maximum(scaled, 0.0)).astype(jnp.bfloat16)
         for n, d in enumerate(blocks):
-            j = partner_of(position, size, d, False)
+            j = lax.rem(position + d, size)
             at = pl.ds(pl.multiple_of(j * columns, columns), columns)
             terms = jnp.dot(activated, down_ref[:, at], preferred_element_type=jnp.float32)
             if d == 0:
@@ -635,23 +632,30 @@
     )
 
 
-def exchange_pairs(size, cores, distance):
+def exchange_pairs(size, cores, distance, ring):
+    chips = partner_pairs(size, distance)
+    if ring:
+        chips = [(i, (i + distance) % size) for i in range(size)]
     return [
         (i * cores + t, j * cores + (cores - 1 - t))
-        for i, j in partner_pairs(size, distance)
+        for i, j in chips
         for t in range(cores)
     ]
 
 
+def around(size):
+    return [*range(1, size)]
+
+
 def distances(size):
     return [*range(size // 2, size), *range(1, size // 2)]
 
 
-def to_partners(outgoing, partners):
+def to_partners(outgoing, partners, ring=False):
     size, cores = lax.axis_size("kv"), lax.axis_size("tp")
     received = []
     for d in partners:
-        pairs = exchange_pairs(size, cores, d)
+        pairs = exchange_pairs(size, cores, d, ring)
         received.append(lax.ppermute(outgoing[d], ("kv", "tp"), pairs))
     return received
 
@@ -727,9 +731,10 @@
     *terms, own = mix(
         pieces[1:], order[1:], absorbed, residual, gain, up_weight, down_weight
     )
-    outgoing = dict(zip(order, terms))
+    steps = around(size)
+    outgoing = dict(zip(steps, terms))
     total = own
-    for term in to_partners(outgoing, order):
+    for term in to_partners(outgoing, steps, True):
         total = total + term
     share = tokens.shape[1] // 2
     other = lax.dynamic_slice_in_dim(total, (1 - head_half) * share, share, 1)

time: 40.4 us -> 39.3 us (0.973)
  Pallas kernels: 10 us -> 9.33 us
  waiting for transfers between devices: 11.5 us -> 10.9 us
    ppermute x14, waiting for transfers between devices: 9.86 us -> 9.04 us  [to_partners(): received.append(lax.ppermute(outgoing[d], ('kv', 'tp'), pairs))]
    pallas_call x5, Pallas kernels: 10 us -> 9.33 us  [call(): pl.pallas_call(body, out_shape=outs, in_specs=in_specs, out_specs=[VMEM_S...]
    ppermute x14, starting transfers between devices: 15.4 us -> 15.8 us  [to_partners(): received.append(lax.ppermute(outgoing[d], ('kv', 'tp'), pairs))]
  transfers between devices with their start and end apart: 19 -> 19, of which waited for: 11 -> 10; matrix products, arithmetic and copies ran while one was open for 0% -> 0% of each run, Pallas kernels for 16% -> 15%
where the time goes in v3:
time: 39.3 us; the launch traced here: 39.2 us
  starting transfers between devices  17.4 us (44%)
  waiting for transfers between devices  10.9 us (28%)
  Pallas kernels  9.33 us (24%)
  between operations  0.78 us (2%)
  other arithmetic  0.62 us (2%)
    ppermute x14, starting transfers between devices, to_partners(): received.append(lax.ppermute(outgoing[d], ('kv', 'tp'), pairs))  15.8 us
    pallas_call x5, Pallas kernels, call(): pl.pallas_call(body, out_shape=outs, in_specs=in_specs, out_specs=[VMEM_S...  9.33 us
    ppermute x14, waiting for transfers between devices, to_partners(): received.append(lax.ppermute(outgoing[d], ('kv', 'tp'), pairs))  9.04 us
    ppermute x5, waiting for transfers between devices, swapped(): return lax.ppermute(array, 'tp', [(0, 1), (1, 0)])  1.89 us
    ppermute x5, starting transfers between devices, swapped(): return lax.ppermute(array, 'tp', [(0, 1), (1, 0)])  1.64 us
  transfers between devices with their start and end apart: 19, of which 10 were waited for; matrix products, arithmetic and copies ran while one was open for 0% of the time, Pallas kernels for 15%

profile of v3, /device:TPU:0, one launch (start us, length us, event | category | flops | bytes accessed | tf_op | source)
XLA Modules:
  0.0 39.2 jit_solution(2019378507079712683)
XLA Ops:
  0.0 0.5 %collective-permute-start.5 = (f32[1,4,512,256]{3,2,1,0:T(8,128)}, f32[1,4,512,256]{3,2,1,0:T(8,128)S(1)}, u32[]{:S(2)}, u32[]{:S(2)}) collective-permute-start(f32[1,4,512,256]{3,2,1,0:T(8,128)} %param.26), channel_id=1, source_target_pairs={{0,1},{1,0},{2,3},{3,2},{4,5},{5,4},{6,7},{7,6},{8,9},{9,8},{10,11... | collective-permute-start | bytes 6291464 | tf_op jit(solution)/shard_map/ppermute | solution.py:664
  0.5 4.6 %shard_map.181 = (f32[1,4224]{1,0:T(1,128)S(1)}, f32[1,4224]{1,0:T(1,128)S(1)}, f32[1,4224]{1,0:T(1,128)S(1)}, f32[1,4224]{1,0:T(1,128)S(1)}, f32[4,512]{1,0:T(4,128)S(1)}, /*index=5*/bf16[4,64,768]{2,1,0:T(8,128)(2,1)S(1)}) custom-call(bf16[4,1024]{1,0:T(4,128)(2,1)} %tokens_hbm.1, f32[1,1024]{1,0:T(1,128)} %bitcast.15, bf16[1024,1024]{1,0:T(8,128)(2,1)} %q_hbm.1, ...), custom_call_target="tpu_custom_call" | custom-call | flops 20000000000 | bytes 1000000 | tf_op jit(solution)/shard_map/pallas_call | solution.py:245
  5.1 0.1 collective-permute-start.6
  5.2 3.7 %collective-permute-start = (f32[1,4224]{1,0:T(1,128)S(1)}, f32[1,4224]{1,0:T(1,128)S(1)}, u32[]{:S(2)}, u32[]{:S(2)}) collective-permute-start(f32[1,4224]{1,0:T(1,128)S(1)} %get-tuple-element.17), channel_id=1, source_target_pairs={{0,5},{1,4},{2,7},{3,6},{4,1},{5,0},{6,3},{7,2},{8,13},{9,12},{10,... | collective-permute-start | bytes 50696 | tf_op jit(solution)/shard_map/ppermute | solution.py:659
  8.9 0.4 %collective-permute-start.4 = (f32[4,512]{1,0:T(4,128)S(1)}, f32[4,512]{1,0:T(4,128)S(1)}, u32[]{:S(2)}, u32[]{:S(2)}) collective-permute-start(f32[4,512]{1,0:T(4,128)S(1)} %get-tuple-element.21), channel_id=1, source_target_pairs={{0,1},{1,0},{2,3},{3,2},{4,5},{5,4},{6,7},{7,6},{8,9},{9,8},{10,11... | collective-permute-start | bytes 24584 | tf_op jit(solution)/shard_map/ppermute | solution.py:664
  9.3 1.0 %collective-permute-start.1 = (f32[1,4224]{1,0:T(1,128)S(1)}, f32[1,4224]{1,0:T(1,128)S(1)}, u32[]{:S(2)}, u32[]{:S(2)}) collective-permute-start(f32[1,4224]{1,0:T(1,128)S(1)} %get-tuple-element.18), channel_id=1, source_target_pairs={{0,7},{1,6},{2,5},{3,4},{4,3},{5,2},{6,1},{7,0},{8,15},{9,14},{10,... | collective-permute-start | bytes 50696 | tf_op jit(solution)/shard_map/ppermute | solution.py:659
  11.0 0.0 collective-permute-done.4.refs_4_
  11.0 0.7 %collective-permute-start.2 = (f32[1,4224]{1,0:T(1,128)S(1)}, f32[1,4224]{1,0:T(1,128)S(1)}, u32[]{:S(2)}, u32[]{:S(2)}) collective-permute-start(f32[1,4224]{1,0:T(1,128)S(1)} %get-tuple-element.19), channel_id=1, source_target_pairs={{0,3},{1,2},{2,1},{3,0},{4,7},{5,6},{6,5},{7,4},{8,11},{9,10},{10,... | collective-permute-start | bytes 50696 | tf_op jit(solution)/shard_map/ppermute | solution.py:659
  11.7 0.0 collective-permute-done.refs_0_
  11.7 0.2 collective-permute-start.3
  11.9 0.0 copy-start
  11.9 2.5 %collective-permute-done.1.refs_1_ = f32[1,4224]{1,0:T(1,128)S(1)} collective-permute-done((f32[1,4224]{1,0:T(1,128)S(1)}, f32[1,4224]{1,0:T(1,128)S(1)}, u32[]{:S(2)}, u32[]{:S(2)}) %collective-permute-start.1) | collective-permute-done | bytes 16928 | tf_op jit(solution)/shard_map/ppermute | solution.py:659
  14.4 0.2 collective-permute-done.2.refs_2_
  14.6 0.0 collective-permute-done.3.refs_3_
  14.6 0.0 collective-permute-done.6.refs_6_
  14.6 0.0 collective-permute-done.5.refs_5_
  14.6 0.0 slice-start
  14.7 0.6 %shard_map.182 = bf16[4,512]{1,0:T(4,128)(2,1)S(1)} custom-call(f32[1,4224]{1,0:T(1,128)S(1)} %collective-permute-done.refs_0_, f32[1,4224]{1,0:T(1,128)S(1)} %collective-permute-done.1.refs_1_, f32[1,4224]{1,0:T(1,128)S(1)} %collective-permute-done.2.refs_2_, f32[1,4224]{1,0:T(1,128)S(1)} %collective-permute-done.3.refs_3_, ...), custom_call_target="tpu_custom_call" | custom-call | flops 20000000000 | bytes 1000000 | tf_op jit(solution)/shard_map/pallas_call | solution.py:245
  15.3 0.0 copy-start.2
  15.3 0.0 slice-start.1
  15.3 0.0 copy-start.1
  15.3 0.2 collective-permute-start.10
  15.5 1.3 %collective-permute-start.7 = (bf16[4,512]{1,0:T(4,128)(2,1)S(1)}, bf16[4,512]{1,0:T(4,128)(2,1)S(1)}, u32[]{:S(2)}, u32[]{:S(2)}) collective-permute-start(bf16[4,512]{1,0:T(4,128)(2,1)S(1)} %shard_map.182), channel_id=1, source_target_pairs={{0,5},{1,4},{2,7},{3,6},{4,1},{5,0},{6,3},{7,2},{8,13},{9,12},{10,... | collective-permute-start | bytes 12296 | tf_op jit(solution)/shard_map/ppermute | solution.py:659
  16.8 1.3 %collective-permute-start.8 = (bf16[4,512]{1,0:T(4,128)(2,1)S(1)}, bf16[4,512]{1,0:T(4,128)(2,1)S(1)}, u32[]{:S(2)}, u32[]{:S(2)}) collective-permute-start(bf16[4,512]{1,0:T(4,128)(2,1)S(1)} %shard_map.182), channel_id=1, source_target_pairs={{0,7},{1,6},{2,5},{3,4},{4,3},{5,2},{6,1},{7,0},{8,15},{9,14},{10,... | collective-permute-start | bytes 12296 | tf_op jit(solution)/shard_map/ppermute | solution.py:659
  18.1 0.6 %collective-permute-start.9 = (bf16[4,512]{1,0:T(4,128)(2,1)S(1)}, bf16[4,512]{1,0:T(4,128)(2,1)S(1)}, u32[]{:S(2)}, u32[]{:S(2)}) collective-permute-start(bf16[4,512]{1,0:T(4,128)(2,1)S(1)} %shard_map.182), channel_id=1, source_target_pairs={{0,3},{1,2},{2,1},{3,0},{4,7},{5,6},{6,5},{7,4},{8,11},{9,10},{10,... | collective-permute-start | bytes 12296 | tf_op jit(solution)/shard_map/ppermute | solution.py:659
  18.7 0.0 collective-permute-done.10.refs_3_
  18.7 0.7 %collective-permute-done.7.refs_0_ = bf16[4,512]{1,0:T(4,128)(2,1)S(1)} collective-permute-done((bf16[4,512]{1,0:T(4,128)(2,1)S(1)}, bf16[4,512]{1,0:T(4,128)(2,1)S(1)}, u32[]{:S(2)}, u32[]{:S(2)}) %collective-permute-start.7) | collective-permute-done | bytes 4128 | tf_op jit(solution)/shard_map/ppermute | solution.py:659
  19.4 2.2 %collective-permute-done.8.refs_1_ = bf16[4,512]{1,0:T(4,128)(2,1)S(1)} collective-permute-done((bf16[4,512]{1,0:T(4,128)(2,1)S(1)}, bf16[4,512]{1,0:T(4,128)(2,1)S(1)}, u32[]{:S(2)}, u32[]{:S(2)}) %collective-permute-start.8) | collective-permute-done | bytes 4128 | tf_op jit(solution)/shard_map/ppermute | solution.py:659
  21.6 0.0 collective-permute-done.9.refs_2_
  21.6 0.0 copy-done
  21.6 0.0 slice-start.2
  21.6 0.6 %shard_map.183 = bf16[4,1024]{1,0:T(4,128)(2,1)S(1)} custom-call(bf16[4,512]{1,0:T(4,128)(2,1)S(1)} %collective-permute-done.7.refs_0_, bf16[4,512]{1,0:T(4,128)(2,1)S(1)} %collective-permute-done.8.refs_1_, bf16[4,512]{1,0:T(4,128)(2,1)S(1)} %collective-permute-done.9.refs_2_, bf16[4,512]{1,0:T(4,128)(2,1)S(1)} %collective-permute-done.10.refs_3_, ...), custom_call_target="tpu_custom_call" | custom-call | flops 20000000000 | bytes 1000000 | tf_op jit(solution)/shard_map/pallas_call | solution.py:245
  22.3 0.0 slice-start.3
  22.3 0.4 %collective-permute-start.11 = (bf16[4,1024]{1,0:T(4,128)(2,1)S(1)}, bf16[4,1024]{1,0:T(4,128)(2,1)S(1)}, u32[]{:S(2)}, u32[]{:S(2)}) collective-permute-start(bf16[4,1024]{1,0:T(4,128)(2,1)S(1)} %shard_map.183), channel_id=1, source_target_pairs={{0,1},{1,0},{2,3},{3,2},{4,5},{5,4},{6,7},{7,6},{8,9},{9,8},{10,11... | collective-permute-start | bytes 24584 | tf_op jit(solution)/shard_map/ppermute | solution.py:664
  22.7 0.8 %collective-permute-done.11 = bf16[4,1024]{1,0:T(4,128)(2,1)S(1)} collective-permute-done((bf16[4,1024]{1,0:T(4,128)(2,1)S(1)}, bf16[4,1024]{1,0:T(4,128)(2,1)S(1)}, u32[]{:S(2)}, u32[]{:S(2)}) %collective-permute-start.11) | collective-permute-done | bytes 8224 | tf_op jit(solution)/shard_map/ppermute | solution.py:664
  23.6 0.0 copy-done.2
  23.6 0.8 %collective-permute-start.14 = (bf16[4,1024]{1,0:T(4,128)(2,1)S(1)}, bf16[4,1024]{1,0:T(4,128)(2,1)S(1)}, u32[]{:S(2)}, u32[]{:S(2)}) collective-permute-start(bf16[4,1024]{1,0:T(4,128)(2,1)S(1)} %add_convert_fusion.refs_0_.refs_4_), channel_id=1, source_target_pairs={{0,5},{1,4},{2,7},{3,6},{4,1},{5,0},{6,3},{7,2},{8,13},{9,12},{10,... | collective-permute-start | bytes 24584 | tf_op jit(solution)/shard_map/ppermute | solution.py:659
  24.4 1.4 %collective-permute-start.12 = (bf16[4,1024]{1,0:T(4,128)(2,1)S(1)}, bf16[4,1024]{1,0:T(4,128)(2,1)S(1)}, u32[]{:S(2)}, u32[]{:S(2)}) collective-permute-start(bf16[4,1024]{1,0:T(4,128)(2,1)S(1)} %add_convert_fusion.refs_0_.refs_4_), channel_id=1, source_target_pairs={{0,7},{1,6},{2,5},{3,4},{4,3},{5,2},{6,1},{7,0},{8,15},{9,14},{10,... | collective-permute-start | bytes 24584 | tf_op jit(solution)/shard_map/ppermute | solution.py:659
  25.8 1.0 %collective-permute-start.13 = (bf16[4,1024]{1,0:T(4,128)(2,1)S(1)}, bf16[4,1024]{1,0:T(4,128)(2,1)S(1)}, u32[]{:S(2)}, u32[]{:S(2)}) collective-permute-start(bf16[4,1024]{1,0:T(4,128)(2,1)S(1)} %add_convert_fusion.refs_0_.refs_4_), channel_id=1, source_target_pairs={{0,3},{1,2},{2,1},{3,0},{4,7},{5,6},{6,5},{7,4},{8,11},{9,10},{10,... | collective-permute-start | bytes 24584 | tf_op jit(solution)/shard_map/ppermute | solution.py:659
  26.8 0.9 %collective-permute-done.14.refs_1_ = bf16[4,1024]{1,0:T(4,128)(2,1)S(1)} collective-permute-done((bf16[4,1024]{1,0:T(4,128)(2,1)S(1)}, bf16[4,1024]{1,0:T(4,128)(2,1)S(1)}, u32[]{:S(2)}, u32[]{:S(2)}) %collective-permute-start.14) | collective-permute-done | bytes 8224 | tf_op jit(solution)/shard_map/ppermute | solution.py:659
  27.7 0.0 slice-done
  27.7 0.0 slice-done.1
  27.7 0.0 copy-done.1
  27.7 1.2 %shard_map.184 = (f32[4,1024]{1,0:T(4,128)S(1)}, f32[4,128]{1,0:T(4,128)S(1)}) custom-call(bf16[4,1024]{1,0:T(4,128)(2,1)S(1)} %add_convert_fusion.refs_0_.refs_4_, bf16[4,1024]{1,0:T(4,128)(2,1)S(1)} %collective-permute-done.14.refs_1_, f32[1,4096]{1,0:T(1,128)S(1)} %bitcast.12, bf16[1024,4096]{1,0:T(8,128)(2,1)S(1)} %bitcast.9), custom_call_target="tpu_custom_call" | custom-call | flops 20000000000 | bytes 1000000 | tf_op jit(solution)/shard_map/pallas_call | solution.py:245
  28.9 0.3 collective-permute-done.12.refs_0_
  29.3 0.0 collective-permute-done.13.refs_1_
  29.3 0.0 slice-done.2
  29.3 0.0 slice-done.3
  29.3 2.3 %shard_map.185 = (f32[4,1024]{1,0:T(4,128)S(1)}, f32[4,1024]{1,0:T(4,128)S(1)}, f32[4,1024]{1,0:T(4,128)S(1)}, f32[4,1024]{1,0:T(4,128)S(1)}) custom-call(bf16[4,1024]{1,0:T(4,128)(2,1)S(1)} %collective-permute-done.12.refs_0_, bf16[4,1024]{1,0:T(4,128)(2,1)S(1)} %collective-permute-done.13.refs_1_, f32[4,1024]{1,0:T(4,128)S(1)} %get-tuple-element.23.refs_2_, ...), custom_call_target="tpu_custom_call" | custom-call | flops 20000000000 | bytes 1000000 | tf_op jit(solution)/shard_map/pallas_call | solution.py:245
  31.6 0.6 %collective-permute-start.15 = (f32[4,1024]{1,0:T(4,128)S(1)}, f32[4,1024]{1,0:T(4,128)S(1)}, u32[]{:S(2)}, u32[]{:S(2)}) collective-permute-start(f32[4,1024]{1,0:T(4,128)S(1)} %get-tuple-element.26), channel_id=1, source_target_pairs={{0,3},{1,2},{2,5},{3,4},{4,7},{5,6},{6,1},{7,0},{8,11},{9,10},{10,... | collective-permute-start | bytes 49160 | tf_op jit(solution)/shard_map/ppermute | solution.py:659
  32.2 1.7 %collective-permute-start.16 = (f32[4,1024]{1,0:T(4,128)S(1)}, f32[4,1024]{1,0:T(4,128)S(1)}, u32[]{:S(2)}, u32[]{:S(2)}) collective-permute-start(f32[4,1024]{1,0:T(4,128)S(1)} %get-tuple-element.27), channel_id=1, source_target_pairs={{0,5},{1,4},{2,7},{3,6},{4,1},{5,0},{6,3},{7,2},{8,13},{9,12},{10,... | collective-permute-start | bytes 49160 | tf_op jit(solution)/shard_map/ppermute | solution.py:659
  33.9 1.3 %collective-permute-start.17 = (f32[4,1024]{1,0:T(4,128)S(1)}, f32[4,1024]{1,0:T(4,128)S(1)}, u32[]{:S(2)}, u32[]{:S(2)}) collective-permute-start(f32[4,1024]{1,0:T(4,128)S(1)} %get-tuple-element.28), channel_id=1, source_target_pairs={{0,7},{1,6},{2,1},{3,0},{4,3},{5,2},{6,5},{7,4},{8,15},{9,14},{10,... | collective-permute-start | bytes 49160 | tf_op jit(solution)/shard_map/ppermute | solution.py:659
  35.2 1.4 %collective-permute-done.15 = f32[4,1024]{1,0:T(4,128)S(1)} collective-permute-done((f32[4,1024]{1,0:T(4,128)S(1)}, f32[4,1024]{1,0:T(4,128)S(1)}, u32[]{:S(2)}, u32[]{:S(2)}) %collective-permute-start.15) | collective-permute-done | bytes 16416 | tf_op jit(solution)/shard_map/ppermute | solution.py:659
  36.6 0.0 collective-permute-done.16
  36.6 0.7 %collective-permute-done.17 = f32[4,1024]{1,0:T(4,128)S(1)} collective-permute-done((f32[4,1024]{1,0:T(4,128)S(1)}, f32[4,1024]{1,0:T(4,128)S(1)}, u32[]{:S(2)}, u32[]{:S(2)}) %collective-permute-start.17) | collective-permute-done | bytes 16416 | tf_op jit(solution)/shard_map/ppermute | solution.py:659
  37.3 0.2 collective-permute-start.18
  37.5 1.1 %collective-permute-done.18 = f32[4,512]{1,0:T(4,128)S(1)} collective-permute-done((f32[4,512]{1,0:T(4,128)S(1)}, f32[4,512]{1,0:T(4,128)S(1)}, u32[]{:S(2)}, u32[]{:S(2)}) %collective-permute-start.18) | collective-permute-done | bytes 8224 | tf_op jit(solution)/shard_map/ppermute | solution.py:664
  38.6 0.6 %add_convert_fusion.1 = bf16[4,512]{1,0:T(4,128)(2,1)} fusion(f32[4,512]{1,0:T(4,128)S(1)} %collective-permute-done.18, f32[4,1024]{1,0:T(4,128)S(1)} %add_add_fusion, s32[]{:T(128)S(6)} %select_n.6), kind=kLoop, calls=%fused_computation.2 | loop fusion | flops 4096 | bytes 20484 | tf_op jit(solution)/shard_map/convert_element_type | solution.py:742
  (6 shorter events, 0.0 us)
Async XLA Ops:
  0.0 14.6 %collective-permute-start.5 = (f32[1,4,512,256]{3,2,1,0:T(8,128)}, f32[1,4,512,256]{3,2,1,0:T(8,128)S(1)}, u32[]{:S(2)}, u32[]{:S(2)}) collective-permute-start(f32[1,4,512,256]{3,2,1,0:T(8,128)} %param.26), channel_id=1, source_target_pairs={{0,1},{1,0},{2,3},{3,2},{4,5},{5,4},{6,7},{7,6},{8,9},{9,8},{10,11... | collective-permute-start | bytes 6291464 | tf_op jit(solution)/shard_map/ppermute | solution.py:664
  5.1 9.6 %collective-permute-start.6 = (bf16[4,64,768]{2,1,0:T(8,128)(2,1)S(1)}, bf16[4,64,768]{2,1,0:T(8,128)(2,1)S(1)}, u32[]{:S(2)}, u32[]{:S(2)}) collective-permute-start(bf16[4,64,768]{2,1,0:T(8,128)(2,1)S(1)} %get-tuple-element.22), channel_id=1, source_target_pairs={{0,1},{1,0},{2,3},{3,2},{4,5},{5,4},{6,7},{7,6},{8,9},{9,8},{10,11... | collective-permute-start | bytes 1179656 | tf_op jit(solution)/shard_map/ppermute | solution.py:664
  5.2 6.5 %collective-permute-start = (f32[1,4224]{1,0:T(1,128)S(1)}, f32[1,4224]{1,0:T(1,128)S(1)}, u32[]{:S(2)}, u32[]{:S(2)}) collective-permute-start(f32[1,4224]{1,0:T(1,128)S(1)} %get-tuple-element.17), channel_id=1, source_target_pairs={{0,5},{1,4},{2,7},{3,6},{4,1},{5,0},{6,3},{7,2},{8,13},{9,12},{10,... | collective-permute-start | bytes 50696 | tf_op jit(solution)/shard_map/ppermute | solution.py:659
  8.9 2.1 %collective-permute-start.4 = (f32[4,512]{1,0:T(4,128)S(1)}, f32[4,512]{1,0:T(4,128)S(1)}, u32[]{:S(2)}, u32[]{:S(2)}) collective-permute-start(f32[4,512]{1,0:T(4,128)S(1)} %get-tuple-element.21), channel_id=1, source_target_pairs={{0,1},{1,0},{2,3},{3,2},{4,5},{5,4},{6,7},{7,6},{8,9},{9,8},{10,11... | collective-permute-start | bytes 24584 | tf_op jit(solution)/shard_map/ppermute | solution.py:664
  9.3 5.1 %collective-permute-start.1 = (f32[1,4224]{1,0:T(1,128)S(1)}, f32[1,4224]{1,0:T(1,128)S(1)}, u32[]{:S(2)}, u32[]{:S(2)}) collective-permute-start(f32[1,4224]{1,0:T(1,128)S(1)} %get-tuple-element.18), channel_id=1, source_target_pairs={{0,7},{1,6},{2,5},{3,4},{4,3},{5,2},{6,1},{7,0},{8,15},{9,14},{10,... | collective-permute-start | bytes 50696 | tf_op jit(solution)/shard_map/ppermute | solution.py:659
  11.0 3.6 %collective-permute-start.2 = (f32[1,4224]{1,0:T(1,128)S(1)}, f32[1,4224]{1,0:T(1,128)S(1)}, u32[]{:S(2)}, u32[]{:S(2)}) collective-permute-start(f32[1,4224]{1,0:T(1,128)S(1)} %get-tuple-element.19), channel_id=1, source_target_pairs={{0,3},{1,2},{2,1},{3,0},{4,7},{5,6},{6,5},{7,4},{8,11},{9,10},{10,... | collective-permute-start | bytes 50696 | tf_op jit(solution)/shard_map/ppermute | solution.py:659
  11.7 2.9 %collective-permute-start.3 = (f32[1,4224]{1,0:T(1,128)S(1)}, f32[1,4224]{1,0:T(1,128)S(1)}, u32[]{:S(2)}, u32[]{:S(2)}) collective-permute-start(f32[1,4224]{1,0:T(1,128)S(1)} %get-tuple-element.20), channel_id=1, source_target_pairs={{0,1},{1,0},{2,3},{3,2},{4,5},{5,4},{6,7},{7,6},{8,9},{9,8},{10,11... | collective-permute-start | bytes 50696 | tf_op jit(solution)/shard_map/ppermute | solution.py:659
  11.9 9.8 %copy-start = (bf16[2048,1024]{1,0:T(8,128)(2,1)S(1)}, bf16[2048,1024]{1,0:T(8,128)(2,1)}, u32[]{:S(2)}) copy-start(bf16[2048,1024]{1,0:T(8,128)(2,1)} %refs_4_.1) | copy-start | bytes 12582916
  14.6 13.1 %slice-start = ((s8[8388608]{0:T(1024)(128)(4,1)}), s8[4194304]{0:T(1024)(128)(4,1)S(1)}, s32[]{:S(2)}) async-start(s8[8388608]{0:T(1024)(128)(4,1)} %bitcast.8), calls=%async_computation | async-start | bytes 8388608
  15.3 8.3 %copy-start.2 = (bf16[4,1024]{1,0:T(4,128)(2,1)S(1)}, bf16[4,1024]{1,0:T(4,128)(2,1)}, u32[]{:S(2)}) copy-start(bf16[4,1024]{1,0:T(4,128)(2,1)} %tokens_hbm.1) | copy-start | bytes 24580
  15.3 12.5 %slice-start.1 = ((s8[8388608]{0:T(1024)(128)(4,1)}), s8[4194304]{0:T(1024)(128)(4,1)S(1)}, s32[]{:S(2)}) async-start(s8[8388608]{0:T(1024)(128)(4,1)} %bitcast.8), calls=%async_computation.1 | async-start | bytes 8388608
  15.3 12.4 %copy-start.1 = (f32[4096]{0:T(1024)S(1)}, f32[4096]{0:T(1024)}, u32[]{:S(2)}) copy-start(f32[4096]{0:T(1024)} %param.35) | copy-start | bytes 49156
  15.3 3.4 %collective-permute-start.10 = (bf16[4,512]{1,0:T(4,128)(2,1)S(1)}, bf16[4,512]{1,0:T(4,128)(2,1)S(1)}, u32[]{:S(2)}, u32[]{:S(2)}) collective-permute-start(bf16[4,512]{1,0:T(4,128)(2,1)S(1)} %shard_map.182), channel_id=1, source_target_pairs={{0,1},{1,0},{2,3},{3,2},{4,5},{5,4},{6,7},{7,6},{8,9},{9,8},{10,11... | collective-permute-start | bytes 12296 | tf_op jit(solution)/shard_map/ppermute | solution.py:659
  15.5 3.9 %collective-permute-start.7 = (bf16[4,512]{1,0:T(4,128)(2,1)S(1)}, bf16[4,512]{1,0:T(4,128)(2,1)S(1)}, u32[]{:S(2)}, u32[]{:S(2)}) collective-permute-start(bf16[4,512]{1,0:T(4,128)(2,1)S(1)} %shard_map.182), channel_id=1, source_target_pairs={{0,5},{1,4},{2,7},{3,6},{4,1},{5,0},{6,3},{7,2},{8,13},{9,12},{10,... | collective-permute-start | bytes 12296 | tf_op jit(solution)/shard_map/ppermute | solution.py:659
  16.8 4.8 %collective-permute-start.8 = (bf16[4,512]{1,0:T(4,128)(2,1)S(1)}, bf16[4,512]{1,0:T(4,128)(2,1)S(1)}, u32[]{:S(2)}, u32[]{:S(2)}) collective-permute-start(bf16[4,512]{1,0:T(4,128)(2,1)S(1)} %shard_map.182), channel_id=1, source_target_pairs={{0,7},{1,6},{2,5},{3,4},{4,3},{5,2},{6,1},{7,0},{8,15},{9,14},{10,... | collective-permute-start | bytes 12296 | tf_op jit(solution)/shard_map/ppermute | solution.py:659
  18.1 3.6 %collective-permute-start.9 = (bf16[4,512]{1,0:T(4,128)(2,1)S(1)}, bf16[4,512]{1,0:T(4,128)(2,1)S(1)}, u32[]{:S(2)}, u32[]{:S(2)}) collective-permute-start(bf16[4,512]{1,0:T(4,128)(2,1)S(1)} %shard_map.182), channel_id=1, source_target_pairs={{0,3},{1,2},{2,1},{3,0},{4,7},{5,6},{6,5},{7,4},{8,11},{9,10},{10,... | collective-permute-start | bytes 12296 | tf_op jit(solution)/shard_map/ppermute | solution.py:659
  21.6 7.6 %slice-start.2 = ((s8[8388608]{0:T(1024)(128)(4,1)}), s8[4194304]{0:T(1024)(128)(4,1)S(1)}, s32[]{:S(2)}) async-start(s8[8388608]{0:T(1024)(128)(4,1)} %bitcast.10), calls=%async_computation.2 | async-start | bytes 8388608
  22.3 7.0 %slice-start.3 = ((s8[8388608]{0:T(1024)(128)(4,1)}), s8[4194304]{0:T(1024)(128)(4,1)S(1)}, s32[]{:S(2)}) async-start(s8[8388608]{0:T(1024)(128)(4,1)} %bitcast.10), calls=%async_computation.3 | async-start | bytes 8388608
  22.3 1.3 %collective-permute-start.11 = (bf16[4,1024]{1,0:T(4,128)(2,1)S(1)}, bf16[4,1024]{1,0:T(4,128)(2,1)S(1)}, u32[]{:S(2)}, u32[]{:S(2)}) collective-permute-start(bf16[4,1024]{1,0:T(4,128)(2,1)S(1)} %shard_map.183), channel_id=1, source_target_pairs={{0,1},{1,0},{2,3},{3,2},{4,5},{5,4},{6,7},{7,6},{8,9},{9,8},{10,11... | collective-permute-start | bytes 24584 | tf_op jit(solution)/shard_map/ppermute | solution.py:664
  23.6 4.1 %collective-permute-start.14 = (bf16[4,1024]{1,0:T(4,128)(2,1)S(1)}, bf16[4,1024]{1,0:T(4,128)(2,1)S(1)}, u32[]{:S(2)}, u32[]{:S(2)}) collective-permute-start(bf16[4,1024]{1,0:T(4,128)(2,1)S(1)} %add_convert_fusion.refs_0_.refs_4_), channel_id=1, source_target_pairs={{0,5},{1,4},{2,7},{3,6},{4,1},{5,0},{6,3},{7,2},{8,13},{9,12},{10,... | collective-permute-start | bytes 24584 | tf_op jit(solution)/shard_map/ppermute | solution.py:659
  24.4 4.9 %collective-permute-start.12 = (bf16[4,1024]{1,0:T(4,128)(2,1)S(1)}, bf16[4,1024]{1,0:T(4,128)(2,1)S(1)}, u32[]{:S(2)}, u32[]{:S(2)}) collective-permute-start(bf16[4,1024]{1,0:T(4,128)(2,1)S(1)} %add_convert_fusion.refs_0_.refs_4_), channel_id=1, source_target_pairs={{0,7},{1,6},{2,5},{3,4},{4,3},{5,2},{6,1},{7,0},{8,15},{9,14},{10,... | collective-permute-start | bytes 24584 | tf_op jit(solution)/shard_map/ppermute | solution.py:659
  25.8 3.5 %collective-permute-start.13 = (bf16[4,1024]{1,0:T(4,128)(2,1)S(1)}, bf16[4,1024]{1,0:T(4,128)(2,1)S(1)}, u32[]{:S(2)}, u32[]{:S(2)}) collective-permute-start(bf16[4,1024]{1,0:T(4,128)(2,1)S(1)} %add_convert_fusion.refs_0_.refs_4_), channel_id=1, source_target_pairs={{0,3},{1,2},{2,1},{3,0},{4,7},{5,6},{6,5},{7,4},{8,11},{9,10},{10,... | collective-permute-start | bytes 24584 | tf_op jit(solution)/shard_map/ppermute | solution.py:659
  31.6 5.0 %collective-permute-start.15 = (f32[4,1024]{1,0:T(4,128)S(1)}, f32[4,1024]{1,0:T(4,128)S(1)}, u32[]{:S(2)}, u32[]{:S(2)}) collective-permute-start(f32[4,1024]{1,0:T(4,128)S(1)} %get-tuple-element.26), channel_id=1, source_target_pairs={{0,3},{1,2},{2,5},{3,4},{4,7},{5,6},{6,1},{7,0},{8,11},{9,10},{10,... | collective-permute-start | bytes 49160 | tf_op jit(solution)/shard_map/ppermute | solution.py:659
  32.2 4.4 %collective-permute-start.16 = (f32[4,1024]{1,0:T(4,128)S(1)}, f32[4,1024]{1,0:T(4,128)S(1)}, u32[]{:S(2)}, u32[]{:S(2)}) collective-permute-start(f32[4,1024]{1,0:T(4,128)S(1)} %get-tuple-element.27), channel_id=1, source_target_pairs={{0,5},{1,4},{2,7},{3,6},{4,1},{5,0},{6,3},{7,2},{8,13},{9,12},{10,... | collective-permute-start | bytes 49160 | tf_op jit(solution)/shard_map/ppermute | solution.py:659
  33.9 3.4 %collective-permute-start.17 = (f32[4,1024]{1,0:T(4,128)S(1)}, f32[4,1024]{1,0:T(4,128)S(1)}, u32[]{:S(2)}, u32[]{:S(2)}) collective-permute-start(f32[4,1024]{1,0:T(4,128)S(1)} %get-tuple-element.28), channel_id=1, source_target_pairs={{0,7},{1,6},{2,1},{3,0},{4,3},{5,2},{6,5},{7,4},{8,15},{9,14},{10,... | collective-permute-start | bytes 49160 | tf_op jit(solution)/shard_map/ppermute | solution.py:659
  37.3 1.2 %collective-permute-start.18 = (f32[4,512]{1,0:T(4,128)S(1)}, f32[4,512]{1,0:T(4,128)S(1)}, u32[]{:S(2)}, u32[]{:S(2)}) collective-permute-start(f32[4,512]{1,0:T(4,128)S(1)} %constant_dynamic-slice_fusion), channel_id=1, source_target_pairs={{0,1},{1,0},{2,3},{3,2},{4,5},{5,4},{6,7},{7,6},{8,9},{9,8},{10,11... | collective-permute-start | bytes 24584 | tf_op jit(solution)/shard_map/ppermute | solution.py:664

commit v4 on v3

--- a/solution.py
+++ b/solution.py
@@ -598,38 +598,60 @@
     )
 
 
-def mix(pieces, partners, before, residual, mixer_gain, up_weight, down_weight):
+def mix(pieces, partners, before, mixer_gain, up_weight, down_weight):
     size = lax.axis_size("kv")
     count = len(pieces)
-    rows, columns = residual.shape
-    blocks = [*around(size), 0]
-    share = columns // 2
+    rows, columns = pieces[0].shape
+    blocks = around(size)
+    units = up_weight.shape[0]
 
     def body(*refs):
-        product_ref, squares_ref, residual_ref, gain_ref, up_ref, down_ref, *outs = refs[count:]
+        product_ref, squares_ref, gain_ref, up_ref, down_ref, *outs = refs[count:]
         position = lax.axis_index("kv")
         product, squares = add_features(
             refs[:count], partners, gain_ref, up_ref, product_ref[...], squares_ref[:, :1]
         )
         scaled = product * lax.rsqrt(squares / D + epsilon)
         activated = jnp.square(jnp.maximum(scaled, 0.0)).astype(jnp.bfloat16)
+        outs[-2][...] = activated
+        own = pl.ds(pl.multiple_of(position * columns, columns), columns)
+        outs[-1][...] = down_ref[:, own]
         for n, d in enumerate(blocks):
             j = lax.rem(position + d, size)
             at = pl.ds(pl.multiple_of(j * columns, columns), columns)
             terms = jnp.dot(activated, down_ref[:, at], preferred_element_type=jnp.float32)
-            if d == 0:
-                half = lax.broadcasted_iota(jnp.int32, (rows, columns), 1) // share
-                kept = residual_ref[...].astype(jnp.float32)
-                terms = terms + jnp.where(half == lax.axis_index("tp"), kept, 0.0)
-            outs[n][...] = terms
+            outs[n][...] = terms.astype(outs[n].dtype)
 
     return call(
         body,
-        [struct((rows, columns), jnp.float32)] * len(blocks),
-        [VMEM_SPEC] * (count + 6),
-        (*pieces, *before, residual, mixer_gain, up_weight, down_weight),
+        [struct((rows, columns), jnp.bfloat16)] * len(blocks)
+        + [
+            struct((rows, units), jnp.bfloat16),
+            struct((units, columns), down_weight.dtype),
+        ],
+        [VMEM_SPEC] * (count + 5),
+        (*pieces, *before, mixer_gain, up_weight, down_weight),
         flops=20000000000,
     )
+
+
+def mix_own(activated, residual, own_down):
+    rows, columns = residual.shape
+    share = columns // 2
+
+    def body(activated_ref, residual_ref, down_ref, out_ref):
+        terms = jnp.dot(activated_ref[...], down_ref[...], preferred_element_type=jnp.float32)
+        half = lax.broadcasted_iota(jnp.int32, (rows, columns), 1) // share
+        kept = residual_ref[...].astype(jnp.float32)
+        out_ref[...] = terms + jnp.where(half == lax.axis_index("tp"), kept, 0.0)
+
+    return call(
+        body,
+        [struct((rows, columns), jnp.float32)],
+        [VMEM_SPEC] * 3,
+        (activated, residual, own_down),
+        flops=1000000,
+    )[0]
 
 
 def exchange_pairs(size, cores, distance, ring):
@@ -728,14 +750,15 @@
     order = distances(size)
     up_weight, down_weight = resident(up_weight), resident(down_weight)
     absorbed = absorb([residual, pieces[0]], [0, order[0]], gain, up_weight)
-    *terms, own = mix(
-        pieces[1:], order[1:], absorbed, residual, gain, up_weight, down_weight
-    )
+    *terms, activated, own_down = mix(
+        pieces[1:], order[1:], absorbed, gain, up_weight, down_weight
+    )
+    own = mix_own(activated, residual, own_down)
     steps = around(size)
     outgoing = dict(zip(steps, terms))
     total = own
     for term in to_partners(outgoing, steps, True):
-        total = total + term
+        total = total + term.astype(jnp.float32)
     share = tokens.shape[1] // 2
     other = lax.dynamic_slice_in_dim(total, (1 - head_half) * share, share, 1)
     kept = lax.dynamic_slice_in_dim(total, head_half * share, share, 1)

time: 39.3 us -> 38.8 us (0.987)
  waiting for transfers between devices: 10.9 us -> 10.2 us
    ppermute x14, waiting for transfers between devices: 9.04 us -> 8.39 us  [to_partners(): received.append(lax.ppermute(outgoing[d], ('kv', 'tp'), pairs))]
    pallas_call x5 -> x6, Pallas kernels: 9.33 us -> 9.47 us  [call(): pl.pallas_call(body, out_shape=outs, in_specs=in_specs, out_specs=[VMEM_S...]
  transfers between devices with their start and end apart: 19 -> 19, of which waited for: 10 -> 10; matrix products, arithmetic and copies ran while one was open for 0% -> 0% of each run, Pallas kernels for 15% -> 16%
where the time goes in v4:
time: 38.8 us; the launch traced here: 38.6 us
  starting transfers between devices  17.5 us (45%)
  waiting for transfers between devices  10.2 us (26%)
  Pallas kernels  9.47 us (24%)
  between operations  0.78 us (2%)
  other arithmetic  0.62 us (2%)
    ppermute x14, starting transfers between devices, to_partners(): received.append(lax.ppermute(outgoing[d], ('kv', 'tp'), pairs))  15.8 us
    pallas_call x6, Pallas kernels, call(): pl.pallas_call(body, out_shape=outs, in_specs=in_specs, out_specs=[VMEM_S...  9.47 us
    ppermute x14, waiting for transfers between devices, to_partners(): received.append(lax.ppermute(outgoing[d], ('kv', 'tp'), pairs))  8.39 us
    ppermute x5, waiting for transfers between devices, swapped(): return lax.ppermute(array, 'tp', [(0, 1), (1, 0)])  1.86 us
    ppermute x5, starting transfers between devices, swapped(): return lax.ppermute(array, 'tp', [(0, 1), (1, 0)])  1.67 us
  transfers between devices with their start and end apart: 19, of which 10 were waited for; matrix products, arithmetic and copies ran while one was open for 0% of the time, Pallas kernels for 16%

profile of v4, /device:TPU:0, one launch (start us, length us, event | category | flops | bytes accessed | tf_op | source)
XLA Modules:
  0.0 38.6 jit_solution(696755906062664838)
XLA Ops:
  0.0 0.5 %collective-permute-start.5 = (f32[1,4,512,256]{3,2,1,0:T(8,128)}, f32[1,4,512,256]{3,2,1,0:T(8,128)S(1)}, u32[]{:S(2)}, u32[]{:S(2)}) collective-permute-start(f32[1,4,512,256]{3,2,1,0:T(8,128)} %param.26), channel_id=1, source_target_pairs={{0,1},{1,0},{2,3},{3,2},{4,5},{5,4},{6,7},{7,6},{8,9},{9,8},{10,11... | collective-permute-start | bytes 6291464 | tf_op jit(solution)/shard_map/ppermute | solution.py:686
  0.5 4.6 %shard_map.181 = (f32[1,4224]{1,0:T(1,128)S(1)}, f32[1,4224]{1,0:T(1,128)S(1)}, f32[1,4224]{1,0:T(1,128)S(1)}, f32[1,4224]{1,0:T(1,128)S(1)}, f32[4,512]{1,0:T(4,128)S(1)}, /*index=5*/bf16[4,64,768]{2,1,0:T(8,128)(2,1)S(1)}) custom-call(bf16[4,1024]{1,0:T(4,128)(2,1)} %tokens_hbm.1, f32[1,1024]{1,0:T(1,128)} %bitcast.15, bf16[1024,1024]{1,0:T(8,128)(2,1)} %q_hbm.1, ...), custom_call_target="tpu_custom_call" | custom-call | flops 20000000000 | bytes 1000000 | tf_op jit(solution)/shard_map/pallas_call | solution.py:245
  5.1 0.1 collective-permute-start.6
  5.2 3.7 %collective-permute-start = (f32[1,4224]{1,0:T(1,128)S(1)}, f32[1,4224]{1,0:T(1,128)S(1)}, u32[]{:S(2)}, u32[]{:S(2)}) collective-permute-start(f32[1,4224]{1,0:T(1,128)S(1)} %get-tuple-element.18), channel_id=1, source_target_pairs={{0,5},{1,4},{2,7},{3,6},{4,1},{5,0},{6,3},{7,2},{8,13},{9,12},{10,... | collective-permute-start | bytes 50696 | tf_op jit(solution)/shard_map/ppermute | solution.py:681
  8.9 0.4 %collective-permute-start.4 = (f32[4,512]{1,0:T(4,128)S(1)}, f32[4,512]{1,0:T(4,128)S(1)}, u32[]{:S(2)}, u32[]{:S(2)}) collective-permute-start(f32[4,512]{1,0:T(4,128)S(1)} %get-tuple-element.22), channel_id=1, source_target_pairs={{0,1},{1,0},{2,3},{3,2},{4,5},{5,4},{6,7},{7,6},{8,9},{9,8},{10,11... | collective-permute-start | bytes 24584 | tf_op jit(solution)/shard_map/ppermute | solution.py:686
  9.3 1.0 %collective-permute-start.1 = (f32[1,4224]{1,0:T(1,128)S(1)}, f32[1,4224]{1,0:T(1,128)S(1)}, u32[]{:S(2)}, u32[]{:S(2)}) collective-permute-start(f32[1,4224]{1,0:T(1,128)S(1)} %get-tuple-element.19), channel_id=1, source_target_pairs={{0,7},{1,6},{2,5},{3,4},{4,3},{5,2},{6,1},{7,0},{8,15},{9,14},{10,... | collective-permute-start | bytes 50696 | tf_op jit(solution)/shard_map/ppermute | solution.py:681
  11.0 0.0 collective-permute-done.4.refs_4_
  11.0 0.7 %collective-permute-start.2 = (f32[1,4224]{1,0:T(1,128)S(1)}, f32[1,4224]{1,0:T(1,128)S(1)}, u32[]{:S(2)}, u32[]{:S(2)}) collective-permute-start(f32[1,4224]{1,0:T(1,128)S(1)} %get-tuple-element.20), channel_id=1, source_target_pairs={{0,3},{1,2},{2,1},{3,0},{4,7},{5,6},{6,5},{7,4},{8,11},{9,10},{10,... | collective-permute-start | bytes 50696 | tf_op jit(solution)/shard_map/ppermute | solution.py:681
  11.7 0.0 collective-permute-done.refs_0_
  11.7 0.2 collective-permute-start.3
  11.9 0.0 copy-start
  11.9 2.5 %collective-permute-done.1.refs_1_ = f32[1,4224]{1,0:T(1,128)S(1)} collective-permute-done((f32[1,4224]{1,0:T(1,128)S(1)}, f32[1,4224]{1,0:T(1,128)S(1)}, u32[]{:S(2)}, u32[]{:S(2)}) %collective-permute-start.1) | collective-permute-done | bytes 16928 | tf_op jit(solution)/shard_map/ppermute | solution.py:681
  14.4 0.2 collective-permute-done.2.refs_2_
  14.6 0.0 collective-permute-done.3.refs_3_
  14.6 0.0 collective-permute-done.6.refs_6_
  14.6 0.0 collective-permute-done.5.refs_5_
  14.6 0.0 slice-start
  14.7 0.6 %shard_map.182 = bf16[4,512]{1,0:T(4,128)(2,1)S(1)} custom-call(f32[1,4224]{1,0:T(1,128)S(1)} %collective-permute-done.refs_0_, f32[1,4224]{1,0:T(1,128)S(1)} %collective-permute-done.1.refs_1_, f32[1,4224]{1,0:T(1,128)S(1)} %collective-permute-done.2.refs_2_, f32[1,4224]{1,0:T(1,128)S(1)} %collective-permute-done.3.refs_3_, ...), custom_call_target="tpu_custom_call" | custom-call | flops 20000000000 | bytes 1000000 | tf_op jit(solution)/shard_map/pallas_call | solution.py:245
  15.3 0.0 copy-start.2
  15.3 0.0 slice-start.1
  15.3 0.0 copy-start.1
  15.3 0.2 collective-permute-start.10
  15.5 1.3 %collective-permute-start.7 = (bf16[4,512]{1,0:T(4,128)(2,1)S(1)}, bf16[4,512]{1,0:T(4,128)(2,1)S(1)}, u32[]{:S(2)}, u32[]{:S(2)}) collective-permute-start(bf16[4,512]{1,0:T(4,128)(2,1)S(1)} %shard_map.182), channel_id=1, source_target_pairs={{0,5},{1,4},{2,7},{3,6},{4,1},{5,0},{6,3},{7,2},{8,13},{9,12},{10,... | collective-permute-start | bytes 12296 | tf_op jit(solution)/shard_map/ppermute | solution.py:681
  16.8 1.3 %collective-permute-start.8 = (bf16[4,512]{1,0:T(4,128)(2,1)S(1)}, bf16[4,512]{1,0:T(4,128)(2,1)S(1)}, u32[]{:S(2)}, u32[]{:S(2)}) collective-permute-start(bf16[4,512]{1,0:T(4,128)(2,1)S(1)} %shard_map.182), channel_id=1, source_target_pairs={{0,7},{1,6},{2,5},{3,4},{4,3},{5,2},{6,1},{7,0},{8,15},{9,14},{10,... | collective-permute-start | bytes 12296 | tf_op jit(solution)/shard_map/ppermute | solution.py:681
  18.1 0.6 %collective-permute-start.9 = (bf16[4,512]{1,0:T(4,128)(2,1)S(1)}, bf16[4,512]{1,0:T(4,128)(2,1)S(1)}, u32[]{:S(2)}, u32[]{:S(2)}) collective-permute-start(bf16[4,512]{1,0:T(4,128)(2,1)S(1)} %shard_map.182), channel_id=1, source_target_pairs={{0,3},{1,2},{2,1},{3,0},{4,7},{5,6},{6,5},{7,4},{8,11},{9,10},{10,... | collective-permute-start | bytes 12296 | tf_op jit(solution)/shard_map/ppermute | solution.py:681
  18.7 0.0 collective-permute-done.10.refs_3_
  18.7 0.7 %collective-permute-done.7.refs_0_ = bf16[4,512]{1,0:T(4,128)(2,1)S(1)} collective-permute-done((bf16[4,512]{1,0:T(4,128)(2,1)S(1)}, bf16[4,512]{1,0:T(4,128)(2,1)S(1)}, u32[]{:S(2)}, u32[]{:S(2)}) %collective-permute-start.7) | collective-permute-done | bytes 4128 | tf_op jit(solution)/shard_map/ppermute | solution.py:681
  19.4 2.2 %collective-permute-done.8.refs_1_ = bf16[4,512]{1,0:T(4,128)(2,1)S(1)} collective-permute-done((bf16[4,512]{1,0:T(4,128)(2,1)S(1)}, bf16[4,512]{1,0:T(4,128)(2,1)S(1)}, u32[]{:S(2)}, u32[]{:S(2)}) %collective-permute-start.8) | collective-permute-done | bytes 4128 | tf_op jit(solution)/shard_map/ppermute | solution.py:681
  21.6 0.0 collective-permute-done.9.refs_2_
  21.6 0.0 copy-done
  21.6 0.0 slice-start.2
  21.6 0.6 %shard_map.183 = bf16[4,1024]{1,0:T(4,128)(2,1)S(1)} custom-call(bf16[4,512]{1,0:T(4,128)(2,1)S(1)} %collective-permute-done.7.refs_0_, bf16[4,512]{1,0:T(4,128)(2,1)S(1)} %collective-permute-done.8.refs_1_, bf16[4,512]{1,0:T(4,128)(2,1)S(1)} %collective-permute-done.9.refs_2_, bf16[4,512]{1,0:T(4,128)(2,1)S(1)} %collective-permute-done.10.refs_3_, ...), custom_call_target="tpu_custom_call" | custom-call | flops 20000000000 | bytes 1000000 | tf_op jit(solution)/shard_map/pallas_call | solution.py:245
  22.3 0.0 slice-start.3
  22.3 0.4 %collective-permute-start.11 = (bf16[4,1024]{1,0:T(4,128)(2,1)S(1)}, bf16[4,1024]{1,0:T(4,128)(2,1)S(1)}, u32[]{:S(2)}, u32[]{:S(2)}) collective-permute-start(bf16[4,1024]{1,0:T(4,128)(2,1)S(1)} %shard_map.183), channel_id=1, source_target_pairs={{0,1},{1,0},{2,3},{3,2},{4,5},{5,4},{6,7},{7,6},{8,9},{9,8},{10,11... | collective-permute-start | bytes 24584 | tf_op jit(solution)/shard_map/ppermute | solution.py:686
  22.8 0.8 %collective-permute-done.11 = bf16[4,1024]{1,0:T(4,128)(2,1)S(1)} collective-permute-done((bf16[4,1024]{1,0:T(4,128)(2,1)S(1)}, bf16[4,1024]{1,0:T(4,128)(2,1)S(1)}, u32[]{:S(2)}, u32[]{:S(2)}) %collective-permute-start.11) | collective-permute-done | bytes 8224 | tf_op jit(solution)/shard_map/ppermute | solution.py:686
  23.6 0.0 copy-done.2
  23.6 0.8 %collective-permute-start.14 = (bf16[4,1024]{1,0:T(4,128)(2,1)S(1)}, bf16[4,1024]{1,0:T(4,128)(2,1)S(1)}, u32[]{:S(2)}, u32[]{:S(2)}) collective-permute-start(bf16[4,1024]{1,0:T(4,128)(2,1)S(1)} %add_convert_fusion.refs_0_.residual_ref), channel_id=1, source_target_pairs={{0,5},{1,4},{2,7},{3,6},{4,1},{5,0},{6,3},{7,2},{8,13},{9,12},{10,... | collective-permute-start | bytes 24584 | tf_op jit(solution)/shard_map/ppermute | solution.py:681
  24.4 1.4 %collective-permute-start.12 = (bf16[4,1024]{1,0:T(4,128)(2,1)S(1)}, bf16[4,1024]{1,0:T(4,128)(2,1)S(1)}, u32[]{:S(2)}, u32[]{:S(2)}) collective-permute-start(bf16[4,1024]{1,0:T(4,128)(2,1)S(1)} %add_convert_fusion.refs_0_.residual_ref), channel_id=1, source_target_pairs={{0,7},{1,6},{2,5},{3,4},{4,3},{5,2},{6,1},{7,0},{8,15},{9,14},{10,... | collective-permute-start | bytes 24584 | tf_op jit(solution)/shard_map/ppermute | solution.py:681
  25.8 1.0 %collective-permute-start.13 = (bf16[4,1024]{1,0:T(4,128)(2,1)S(1)}, bf16[4,1024]{1,0:T(4,128)(2,1)S(1)}, u32[]{:S(2)}, u32[]{:S(2)}) collective-permute-start(bf16[4,1024]{1,0:T(4,128)(2,1)S(1)} %add_convert_fusion.refs_0_.residual_ref), channel_id=1, source_target_pairs={{0,3},{1,2},{2,1},{3,0},{4,7},{5,6},{6,5},{7,4},{8,11},{9,10},{10,... | collective-permute-start | bytes 24584 | tf_op jit(solution)/shard_map/ppermute | solution.py:681
  26.8 0.9 %collective-permute-done.14.refs_1_ = bf16[4,1024]{1,0:T(4,128)(2,1)S(1)} collective-permute-done((bf16[4,1024]{1,0:T(4,128)(2,1)S(1)}, bf16[4,1024]{1,0:T(4,128)(2,1)S(1)}, u32[]{:S(2)}, u32[]{:S(2)}) %collective-permute-start.14) | collective-permute-done | bytes 8224 | tf_op jit(solution)/shard_map/ppermute | solution.py:681
  27.7 0.0 slice-done
  27.7 0.0 slice-done.1
  27.7 0.0 copy-done.1
  27.7 1.2 %shard_map.184 = (f32[4,1024]{1,0:T(4,128)S(1)}, f32[4,128]{1,0:T(4,128)S(1)}) custom-call(bf16[4,1024]{1,0:T(4,128)(2,1)S(1)} %add_convert_fusion.refs_0_.residual_ref, bf16[4,1024]{1,0:T(4,128)(2,1)S(1)} %collective-permute-done.14.refs_1_, f32[1,4096]{1,0:T(1,128)S(1)} %bitcast.12, bf16[1024,4096]{1,0:T(8,128)(2,1)S(1)} %bitcast.9), custom_call_target="tpu_custom_call" | custom-call | flops 20000000000 | bytes 1000000 | tf_op jit(solution)/shard_map/pallas_call | solution.py:245
  28.9 0.3 collective-permute-done.12.refs_0_
  29.3 0.0 collective-permute-done.13.refs_1_
  29.3 0.0 slice-done.2
  29.3 0.0 slice-done.3
  29.3 2.1 %shard_map.185 = (bf16[4,1024]{1,0:T(4,128)(2,1)S(1)}, bf16[4,1024]{1,0:T(4,128)(2,1)S(1)}, bf16[4,1024]{1,0:T(4,128)(2,1)S(1)}, bf16[4,1024]{1,0:T(4,128)(2,1)S(1)}, bf16[1024,1024]{1,0:T(8,128)(2,1)S(1)}) custom-call(bf16[4,1024]{1,0:T(4,128)(2,1)S(1)} %collective-permute-done.12.refs_0_, bf16[4,1024]{1,0:T(4,128)(2,1)S(1)} %collective-permute-done.13.refs_1_, ...), custom_call_target="tpu_custom_call" | custom-call | flops 20000000000 | bytes 1000000 | tf_op jit(solution)/shard_map/pallas_call | solution.py:245
  31.4 0.6 %collective-permute-start.15 = (bf16[4,1024]{1,0:T(4,128)(2,1)S(1)}, bf16[4,1024]{1,0:T(4,128)(2,1)S(1)}, u32[]{:S(2)}, u32[]{:S(2)}) collective-permute-start(bf16[4,1024]{1,0:T(4,128)(2,1)S(1)} %get-tuple-element.28), channel_id=1, source_target_pairs={{0,3},{1,2},{2,5},{3,4},{4,7},{5,6},{6,1},{7,0},{8,11},{9,10},{10,... | collective-permute-start | bytes 24584 | tf_op jit(solution)/shard_map/ppermute | solution.py:681
  32.0 1.7 %collective-permute-start.16 = (bf16[4,1024]{1,0:T(4,128)(2,1)S(1)}, bf16[4,1024]{1,0:T(4,128)(2,1)S(1)}, u32[]{:S(2)}, u32[]{:S(2)}) collective-permute-start(bf16[4,1024]{1,0:T(4,128)(2,1)S(1)} %get-tuple-element.29), channel_id=1, source_target_pairs={{0,5},{1,4},{2,7},{3,6},{4,1},{5,0},{6,3},{7,2},{8,13},{9,12},{10,... | collective-permute-start | bytes 24584 | tf_op jit(solution)/shard_map/ppermute | solution.py:681
  33.7 1.3 %collective-permute-start.17 = (bf16[4,1024]{1,0:T(4,128)(2,1)S(1)}, bf16[4,1024]{1,0:T(4,128)(2,1)S(1)}, u32[]{:S(2)}, u32[]{:S(2)}) collective-permute-start(bf16[4,1024]{1,0:T(4,128)(2,1)S(1)} %get-tuple-element.30), channel_id=1, source_target_pairs={{0,7},{1,6},{2,1},{3,0},{4,3},{5,2},{6,5},{7,4},{8,15},{9,14},{10,... | collective-permute-start | bytes 24584 | tf_op jit(solution)/shard_map/ppermute | solution.py:681
  35.0 0.4 shard_map.186
  35.3 0.9 %collective-permute-done.15 = bf16[4,1024]{1,0:T(4,128)(2,1)S(1)} collective-permute-done((bf16[4,1024]{1,0:T(4,128)(2,1)S(1)}, bf16[4,1024]{1,0:T(4,128)(2,1)S(1)}, u32[]{:S(2)}, u32[]{:S(2)}) %collective-permute-start.15) | collective-permute-done | bytes 8224 | tf_op jit(solution)/shard_map/ppermute | solution.py:681
  36.2 0.0 collective-permute-done.16
  36.2 0.5 %collective-permute-done.17 = bf16[4,1024]{1,0:T(4,128)(2,1)S(1)} collective-permute-done((bf16[4,1024]{1,0:T(4,128)(2,1)S(1)}, bf16[4,1024]{1,0:T(4,128)(2,1)S(1)}, u32[]{:S(2)}, u32[]{:S(2)}) %collective-permute-start.17) | collective-permute-done | bytes 8224 | tf_op jit(solution)/shard_map/ppermute | solution.py:681
  36.8 0.2 collective-permute-start.18
  37.0 1.0 %collective-permute-done.18 = f32[4,512]{1,0:T(4,128)S(1)} collective-permute-done((f32[4,512]{1,0:T(4,128)S(1)}, f32[4,512]{1,0:T(4,128)S(1)}, u32[]{:S(2)}, u32[]{:S(2)}) %collective-permute-start.18) | collective-permute-done | bytes 8224 | tf_op jit(solution)/shard_map/ppermute | solution.py:686
  38.0 0.6 %add_convert_fusion.1 = bf16[4,512]{1,0:T(4,128)(2,1)} fusion(f32[4,512]{1,0:T(4,128)S(1)} %collective-permute-done.18, f32[4,1024]{1,0:T(4,128)S(1)} %convert_add_fusion, s32[]{:T(128)S(6)} %select_n.6), kind=kLoop, calls=%fused_computation.2 | loop fusion | flops 4096 | bytes 20484 | tf_op jit(solution)/shard_map/convert_element_type | solution.py:765
  (6 shorter events, 0.0 us)
Async XLA Ops:
  0.0 14.6 %collective-permute-start.5 = (f32[1,4,512,256]{3,2,1,0:T(8,128)}, f32[1,4,512,256]{3,2,1,0:T(8,128)S(1)}, u32[]{:S(2)}, u32[]{:S(2)}) collective-permute-start(f32[1,4,512,256]{3,2,1,0:T(8,128)} %param.26), channel_id=1, source_target_pairs={{0,1},{1,0},{2,3},{3,2},{4,5},{5,4},{6,7},{7,6},{8,9},{9,8},{10,11... | collective-permute-start | bytes 6291464 | tf_op jit(solution)/shard_map/ppermute | solution.py:686
  5.1 9.6 %collective-permute-start.6 = (bf16[4,64,768]{2,1,0:T(8,128)(2,1)S(1)}, bf16[4,64,768]{2,1,0:T(8,128)(2,1)S(1)}, u32[]{:S(2)}, u32[]{:S(2)}) collective-permute-start(bf16[4,64,768]{2,1,0:T(8,128)(2,1)S(1)} %get-tuple-element.23), channel_id=1, source_target_pairs={{0,1},{1,0},{2,3},{3,2},{4,5},{5,4},{6,7},{7,6},{8,9},{9,8},{10,11... | collective-permute-start | bytes 1179656 | tf_op jit(solution)/shard_map/ppermute | solution.py:686
  5.2 6.5 %collective-permute-start = (f32[1,4224]{1,0:T(1,128)S(1)}, f32[1,4224]{1,0:T(1,128)S(1)}, u32[]{:S(2)}, u32[]{:S(2)}) collective-permute-start(f32[1,4224]{1,0:T(1,128)S(1)} %get-tuple-element.18), channel_id=1, source_target_pairs={{0,5},{1,4},{2,7},{3,6},{4,1},{5,0},{6,3},{7,2},{8,13},{9,12},{10,... | collective-permute-start | bytes 50696 | tf_op jit(solution)/shard_map/ppermute | solution.py:681
  8.9 2.1 %collective-permute-start.4 = (f32[4,512]{1,0:T(4,128)S(1)}, f32[4,512]{1,0:T(4,128)S(1)}, u32[]{:S(2)}, u32[]{:S(2)}) collective-permute-start(f32[4,512]{1,0:T(4,128)S(1)} %get-tuple-element.22), channel_id=1, source_target_pairs={{0,1},{1,0},{2,3},{3,2},{4,5},{5,4},{6,7},{7,6},{8,9},{9,8},{10,11... | collective-permute-start | bytes 24584 | tf_op jit(solution)/shard_map/ppermute | solution.py:686
  9.3 5.1 %collective-permute-start.1 = (f32[1,4224]{1,0:T(1,128)S(1)}, f32[1,4224]{1,0:T(1,128)S(1)}, u32[]{:S(2)}, u32[]{:S(2)}) collective-permute-start(f32[1,4224]{1,0:T(1,128)S(1)} %get-tuple-element.19), channel_id=1, source_target_pairs={{0,7},{1,6},{2,5},{3,4},{4,3},{5,2},{6,1},{7,0},{8,15},{9,14},{10,... | collective-permute-start | bytes 50696 | tf_op jit(solution)/shard_map/ppermute | solution.py:681
  11.0 3.6 %collective-permute-start.2 = (f32[1,4224]{1,0:T(1,128)S(1)}, f32[1,4224]{1,0:T(1,128)S(1)}, u32[]{:S(2)}, u32[]{:S(2)}) collective-permute-start(f32[1,4224]{1,0:T(1,128)S(1)} %get-tuple-element.20), channel_id=1, source_target_pairs={{0,3},{1,2},{2,1},{3,0},{4,7},{5,6},{6,5},{7,4},{8,11},{9,10},{10,... | collective-permute-start | bytes 50696 | tf_op jit(solution)/shard_map/ppermute | solution.py:681
  11.7 2.9 %collective-permute-start.3 = (f32[1,4224]{1,0:T(1,128)S(1)}, f32[1,4224]{1,0:T(1,128)S(1)}, u32[]{:S(2)}, u32[]{:S(2)}) collective-permute-start(f32[1,4224]{1,0:T(1,128)S(1)} %get-tuple-element.21), channel_id=1, source_target_pairs={{0,1},{1,0},{2,3},{3,2},{4,5},{5,4},{6,7},{7,6},{8,9},{9,8},{10,11... | collective-permute-start | bytes 50696 | tf_op jit(solution)/shard_map/ppermute | solution.py:681
  11.9 9.8 %copy-start = (bf16[2048,1024]{1,0:T(8,128)(2,1)S(1)}, bf16[2048,1024]{1,0:T(8,128)(2,1)}, u32[]{:S(2)}) copy-start(bf16[2048,1024]{1,0:T(8,128)(2,1)} %refs_4_.1) | copy-start | bytes 12582916
  14.6 13.1 %slice-start = ((s8[8388608]{0:T(1024)(128)(4,1)}), s8[4194304]{0:T(1024)(128)(4,1)S(1)}, s32[]{:S(2)}) async-start(s8[8388608]{0:T(1024)(128)(4,1)} %bitcast.8), calls=%async_computation | async-start | bytes 8388608
  15.3 8.3 %copy-start.2 = (bf16[4,1024]{1,0:T(4,128)(2,1)S(1)}, bf16[4,1024]{1,0:T(4,128)(2,1)}, u32[]{:S(2)}) copy-start(bf16[4,1024]{1,0:T(4,128)(2,1)} %tokens_hbm.1) | copy-start | bytes 24580
  15.3 12.5 %slice-start.1 = ((s8[8388608]{0:T(1024)(128)(4,1)}), s8[4194304]{0:T(1024)(128)(4,1)S(1)}, s32[]{:S(2)}) async-start(s8[8388608]{0:T(1024)(128)(4,1)} %bitcast.8), calls=%async_computation.1 | async-start | bytes 8388608
  15.3 12.4 %copy-start.1 = (f32[4096]{0:T(1024)S(1)}, f32[4096]{0:T(1024)}, u32[]{:S(2)}) copy-start(f32[4096]{0:T(1024)} %param.35) | copy-start | bytes 49156
  15.3 3.4 %collective-permute-start.10 = (bf16[4,512]{1,0:T(4,128)(2,1)S(1)}, bf16[4,512]{1,0:T(4,128)(2,1)S(1)}, u32[]{:S(2)}, u32[]{:S(2)}) collective-permute-start(bf16[4,512]{1,0:T(4,128)(2,1)S(1)} %shard_map.182), channel_id=1, source_target_pairs={{0,1},{1,0},{2,3},{3,2},{4,5},{5,4},{6,7},{7,6},{8,9},{9,8},{10,11... | collective-permute-start | bytes 12296 | tf_op jit(solution)/shard_map/ppermute | solution.py:681
  15.5 3.9 %collective-permute-start.7 = (bf16[4,512]{1,0:T(4,128)(2,1)S(1)}, bf16[4,512]{1,0:T(4,128)(2,1)S(1)}, u32[]{:S(2)}, u32[]{:S(2)}) collective-permute-start(bf16[4,512]{1,0:T(4,128)(2,1)S(1)} %shard_map.182), channel_id=1, source_target_pairs={{0,5},{1,4},{2,7},{3,6},{4,1},{5,0},{6,3},{7,2},{8,13},{9,12},{10,... | collective-permute-start | bytes 12296 | tf_op jit(solution)/shard_map/ppermute | solution.py:681
  16.8 4.8 %collective-permute-start.8 = (bf16[4,512]{1,0:T(4,128)(2,1)S(1)}, bf16[4,512]{1,0:T(4,128)(2,1)S(1)}, u32[]{:S(2)}, u32[]{:S(2)}) collective-permute-start(bf16[4,512]{1,0:T(4,128)(2,1)S(1)} %shard_map.182), channel_id=1, source_target_pairs={{0,7},{1,6},{2,5},{3,4},{4,3},{5,2},{6,1},{7,0},{8,15},{9,14},{10,... | collective-permute-start | bytes 12296 | tf_op jit(solution)/shard_map/ppermute | solution.py:681
  18.1 3.6 %collective-permute-start.9 = (bf16[4,512]{1,0:T(4,128)(2,1)S(1)}, bf16[4,512]{1,0:T(4,128)(2,1)S(1)}, u32[]{:S(2)}, u32[]{:S(2)}) collective-permute-start(bf16[4,512]{1,0:T(4,128)(2,1)S(1)} %shard_map.182), channel_id=1, source_target_pairs={{0,3},{1,2},{2,1},{3,0},{4,7},{5,6},{6,5},{7,4},{8,11},{9,10},{10,... | collective-permute-start | bytes 12296 | tf_op jit(solution)/shard_map/ppermute | solution.py:681
  21.6 7.6 %slice-start.2 = ((s8[8388608]{0:T(1024)(128)(4,1)}), s8[4194304]{0:T(1024)(128)(4,1)S(1)}, s32[]{:S(2)}) async-start(s8[8388608]{0:T(1024)(128)(4,1)} %bitcast.10), calls=%async_computation.2 | async-start | bytes 8388608
  22.3 7.0 %slice-start.3 = ((s8[8388608]{0:T(1024)(128)(4,1)}), s8[4194304]{0:T(1024)(128)(4,1)S(1)}, s32[]{:S(2)}) async-start(s8[8388608]{0:T(1024)(128)(4,1)} %bitcast.10), calls=%async_computation.3 | async-start | bytes 8388608
  22.3 1.3 %collective-permute-start.11 = (bf16[4,1024]{1,0:T(4,128)(2,1)S(1)}, bf16[4,1024]{1,0:T(4,128)(2,1)S(1)}, u32[]{:S(2)}, u32[]{:S(2)}) collective-permute-start(bf16[4,1024]{1,0:T(4,128)(2,1)S(1)} %shard_map.183), channel_id=1, source_target_pairs={{0,1},{1,0},{2,3},{3,2},{4,5},{5,4},{6,7},{7,6},{8,9},{9,8},{10,11... | collective-permute-start | bytes 24584 | tf_op jit(solution)/shard_map/ppermute | solution.py:686
  23.6 4.1 %collective-permute-start.14 = (bf16[4,1024]{1,0:T(4,128)(2,1)S(1)}, bf16[4,1024]{1,0:T(4,128)(2,1)S(1)}, u32[]{:S(2)}, u32[]{:S(2)}) collective-permute-start(bf16[4,1024]{1,0:T(4,128)(2,1)S(1)} %add_convert_fusion.refs_0_.residual_ref), channel_id=1, source_target_pairs={{0,5},{1,4},{2,7},{3,6},{4,1},{5,0},{6,3},{7,2},{8,13},{9,12},{10,... | collective-permute-start | bytes 24584 | tf_op jit(solution)/shard_map/ppermute | solution.py:681
  24.4 4.9 %collective-permute-start.12 = (bf16[4,1024]{1,0:T(4,128)(2,1)S(1)}, bf16[4,1024]{1,0:T(4,128)(2,1)S(1)}, u32[]{:S(2)}, u32[]{:S(2)}) collective-permute-start(bf16[4,1024]{1,0:T(4,128)(2,1)S(1)} %add_convert_fusion.refs_0_.residual_ref), channel_id=1, source_target_pairs={{0,7},{1,6},{2,5},{3,4},{4,3},{5,2},{6,1},{7,0},{8,15},{9,14},{10,... | collective-permute-start | bytes 24584 | tf_op jit(solution)/shard_map/ppermute | solution.py:681
  25.8 3.5 %collective-permute-start.13 = (bf16[4,1024]{1,0:T(4,128)(2,1)S(1)}, bf16[4,1024]{1,0:T(4,128)(2,1)S(1)}, u32[]{:S(2)}, u32[]{:S(2)}) collective-permute-start(bf16[4,1024]{1,0:T(4,128)(2,1)S(1)} %add_convert_fusion.refs_0_.residual_ref), channel_id=1, source_target_pairs={{0,3},{1,2},{2,1},{3,0},{4,7},{5,6},{6,5},{7,4},{8,11},{9,10},{10,... | collective-permute-start | bytes 24584 | tf_op jit(solution)/shard_map/ppermute | solution.py:681
  31.4 4.9 %collective-permute-start.15 = (bf16[4,1024]{1,0:T(4,128)(2,1)S(1)}, bf16[4,1024]{1,0:T(4,128)(2,1)S(1)}, u32[]{:S(2)}, u32[]{:S(2)}) collective-permute-start(bf16[4,1024]{1,0:T(4,128)(2,1)S(1)} %get-tuple-element.28), channel_id=1, source_target_pairs={{0,3},{1,2},{2,5},{3,4},{4,7},{5,6},{6,1},{7,0},{8,11},{9,10},{10,... | collective-permute-start | bytes 24584 | tf_op jit(solution)/shard_map/ppermute | solution.py:681
  32.0 4.3 %collective-permute-start.16 = (bf16[4,1024]{1,0:T(4,128)(2,1)S(1)}, bf16[4,1024]{1,0:T(4,128)(2,1)S(1)}, u32[]{:S(2)}, u32[]{:S(2)}) collective-permute-start(bf16[4,1024]{1,0:T(4,128)(2,1)S(1)} %get-tuple-element.29), channel_id=1, source_target_pairs={{0,5},{1,4},{2,7},{3,6},{4,1},{5,0},{6,3},{7,2},{8,13},{9,12},{10,... | collective-permute-start | bytes 24584 | tf_op jit(solution)/shard_map/ppermute | solution.py:681
  33.7 3.1 %collective-permute-start.17 = (bf16[4,1024]{1,0:T(4,128)(2,1)S(1)}, bf16[4,1024]{1,0:T(4,128)(2,1)S(1)}, u32[]{:S(2)}, u32[]{:S(2)}) collective-permute-start(bf16[4,1024]{1,0:T(4,128)(2,1)S(1)} %get-tuple-element.30), channel_id=1, source_target_pairs={{0,7},{1,6},{2,1},{3,0},{4,3},{5,2},{6,5},{7,4},{8,15},{9,14},{10,... | collective-permute-start | bytes 24584 | tf_op jit(solution)/shard_map/ppermute | solution.py:681
  36.8 1.2 %collective-permute-start.18 = (f32[4,512]{1,0:T(4,128)S(1)}, f32[4,512]{1,0:T(4,128)S(1)}, u32[]{:S(2)}, u32[]{:S(2)}) collective-permute-start(f32[4,512]{1,0:T(4,128)S(1)} %constant_dynamic-slice_fusion), channel_id=1, source_target_pairs={{0,1},{1,0},{2,3},{3,2},{4,5},{5,4},{6,7},{7,6},{8,9},{9,8},{10,11... | collective-permute-start | bytes 24584 | tf_op jit(solution)/shard_map/ppermute | solution.py:686

commit v5 on v4

--- a/solution.py
+++ b/solution.py
@@ -279,13 +279,10 @@
     forget_bias,
     state_normalizer,
     state_max,
-    block_keys,
-    block_values,
     block_input,
     block_logf,
 ):
     _, heads, dk = state_normalizer.shape
-    span, dv = block_values.shape[2:]
     packed_width = dk + 2 * LANES
     rows, columns = tokens.shape
     size = lax.axis_size("kv")
@@ -299,12 +296,12 @@
     small = (forget_bias.reshape(1, -1), state_normalizer, state_max, block_input, block_logf)
 
     def body(tokens_hbm, gain_hbm, q_hbm, k_hbm, v_hbm, gate_hbm, *rest):
-        small_hbm, (keys_hbm, values_hbm), rest = rest[:5], rest[5:7], rest[7:]
-        outs, small_out, block_out = rest[:size], rest[size], rest[size + 1]
-        rest = rest[size + 2 :]
+        small_hbm, rest = rest[:5], rest[5:]
+        outs, small_out = rest[:size], rest[size]
+        rest = rest[size + 1 :]
         tokens_ref, gain_ref, weight_ref, gate_ref, sums_ref = rest[:5]
-        sems, gate_sem, tokens_sem, gain_sem, small_sems, block_sems = rest[5:11]
-        small_refs = rest[11:]
+        sems, gate_sem, tokens_sem, gain_sem, small_sems = rest[5:10]
+        small_refs = rest[10:]
         position = lax.axis_index("kv")
         tokens_copy = pltpu.make_async_copy(tokens_hbm, tokens_ref, tokens_sem)
         gain_copy = pltpu.make_async_copy(gain_hbm, gain_ref, gain_sem)
@@ -331,13 +328,7 @@
             pltpu.make_async_copy(source, target, small_sems.at[i])
             for i, (source, target) in enumerate(zip(small_hbm, small_refs))
         ]
-        block_copies = [
-            pltpu.make_async_copy(keys_hbm.at[0], block_out.at[:, :, pl.ds(0, dk)], block_sems.at[0]),
-            pltpu.make_async_copy(
-                values_hbm.at[0], block_out.at[:, :, pl.ds(dk, dv)], block_sems.at[1]
-            ),
-        ]
-        for copy in small_copies + block_copies:
+        for copy in small_copies:
             copy.start()
         tokens_copy.wait()
         gain_copy.wait()
@@ -357,8 +348,6 @@
                 if c:
                     product = product + sums_ref[:, at]
                 sums_ref[:, at] = product
-        for copy in block_copies:
-            copy.wait()
         gate_copy.wait()
         gate_sums = dot_nt(normed, gate_ref[...])
         pad = jnp.zeros((rows, LANES - gate_count), jnp.float32)
@@ -387,9 +376,8 @@
         [struct((1, width + LANES), jnp.float32)] * size
         + [
             struct((heads, packed_width), jnp.float32),
-            struct((heads, span, dk + dv), block_keys.dtype),
         ],
-        [ANY_SPEC] * 13,
+        [ANY_SPEC] * 11,
         [
             streamed(a)
             for a in (
@@ -398,8 +386,6 @@
                 *weights,
                 gates,
                 *small,
-                block_keys,
-                block_values,
             )
         ],
         [
@@ -413,21 +399,20 @@
             pltpu.SemaphoreType.DMA(()),
             pltpu.SemaphoreType.DMA(()),
             pltpu.SemaphoreType.DMA((len(small),)),
-            pltpu.SemaphoreType.DMA((2,)),
             *[pltpu.VMEM(a.shape, a.dtype) for a in small],
         ],
         limit=16,
     )
 
 
-def recall(parts, small, state_matrix, blocks, lengths):
+def recall(parts, small, state_matrix, block_keys, block_values, lengths):
     _, heads, dv, dk = state_matrix.shape
     all_heads = heads * lax.axis_size("tp")
     scale = dk ** (-0.5)
     count = len(parts)
 
     def body(*refs):
-        small_ref, state_ref, blocks_ref, lengths_ref, out_ref = refs[count:]
+        small_ref, state_ref, keys_ref, values_ref, lengths_ref, out_ref = refs[count:]
         half = 1 - lax.axis_index("tp")
         row = refs[0][...]
         for r in refs[1:count]:
@@ -490,7 +475,7 @@
                 out = jnp.where(rows == h, make(h), out)
             return out
 
-        scores = pick(lambda h: dot_nt(query, blocks_ref[h, :, :dk]), SPAN_LOCATIONS)
+        scores = pick(lambda h: dot_nt(query, keys_ref[0, h]), SPAN_LOCATIONS)
         mixing = (scores * scale * cache_weight).astype(jnp.bfloat16)
         query_wide = query.astype(jnp.float32)
         own_term = (
@@ -505,7 +490,7 @@
         carried = pick(carry, dv)
         from_cache = pick(
             lambda h: jnp.dot(
-                mixing, blocks_ref[h, :, dk:], preferred_element_type=jnp.float32
+                mixing, values_ref[0, h], preferred_element_type=jnp.float32
             ), dv
         )
         numerator = carried_weight * carried + from_cache + own_term * value.astype(jnp.float32)
@@ -520,12 +505,13 @@
     return call(
         body,
         [struct((heads, dv), jnp.bfloat16)],
-        [VMEM_SPEC] * (count + 4),
+        [VMEM_SPEC] * (count + 5),
         (
             *parts,
             small,
             resident(state_matrix),
-            blocks,
+            block_keys,
+            block_values,
             jnp.pad(lengths, (0, LANES - 1)).reshape(1, -1),
         ),
     )[0]
@@ -723,7 +709,7 @@
     size = lax.axis_size("kv")
     order = distances(size)
     state_matrix = swapped(state_matrix)
-    *parts, small, blocks = project(
+    *parts, small = project(
         tokens,
         norm_gain,
         query_weight,
@@ -733,13 +719,13 @@
         forget_bias,
         state_normalizer,
         state_max,
-        block_keys,
-        block_values,
         block_input,
         block_logf,
     )
     parts = to_partners(parts, [*order, 0])
-    hidden = recall(parts, swapped(small), state_matrix, swapped(blocks), lengths)
+    hidden = recall(
+        parts, swapped(small), state_matrix, swapped(block_keys), swapped(block_values), lengths
+    )
     pieces = to_partners([hidden] * size, [*order, 0])
     partial_out = attend(pieces, out_weight)
     other_out = swapped(partial_out)

time: 38.8 us -> 41.1 us (1.059)
  starting transfers between devices: 17.5 us -> 19.3 us
  waiting for transfers between devices: 10.2 us -> 10.7 us
    ppermute x14, starting transfers between devices: 15.8 us -> 17.6 us  [to_partners(): received.append(lax.ppermute(outgoing[d], ('kv', 'tp'), pairs))]
    ppermute x5 -> x6, starting transfers between devices: 1.67 us -> 1.75 us  [swapped(): return lax.ppermute(array, 'tp', [(0, 1), (1, 0)])]
    ppermute x5 -> x6, waiting for transfers between devices: 1.86 us -> 1.9 us  [swapped(): return lax.ppermute(array, 'tp', [(0, 1), (1, 0)])]
  transfers between devices with their start and end apart: 19 -> 20, of which waited for: 10 -> 11; matrix products, arithmetic and copies ran while one was open for 0% -> 0% of each run, Pallas kernels for 16% -> 15%
where the time goes in v5:
time: 41.1 us; the launch traced here: 40.9 us
  starting transfers between devices  19.3 us (47%)
  waiting for transfers between devices  10.7 us (26%)
  Pallas kernels  9.44 us (23%)
  between operations  0.8 us (2%)
  other arithmetic  0.62 us (2%)
    ppermute x14, starting transfers between devices, to_partners(): received.append(lax.ppermute(outgoing[d], ('kv', 'tp'), pairs))  17.6 us
    pallas_call x6, Pallas kernels, call(): pl.pallas_call(body, out_shape=outs, in_specs=in_specs, out_specs=[VMEM_S...  9.44 us
    ppermute x14, waiting for transfers between devices, to_partners(): received.append(lax.ppermute(outgoing[d], ('kv', 'tp'), pairs))  8.78 us
    ppermute x6, waiting for transfers between devices, swapped(): return lax.ppermute(array, 'tp', [(0, 1), (1, 0)])  1.9 us
    ppermute x6, starting transfers between devices, swapped(): return lax.ppermute(array, 'tp', [(0, 1), (1, 0)])  1.75 us
  transfers between devices with their start and end apart: 20, of which 11 were waited for; matrix products, arithmetic and copies ran while one was open for 0% of the time, Pallas kernels for 15%

profile of v5, /device:TPU:0, one launch (start us, length us, event | category | flops | bytes accessed | tf_op | source)
XLA Modules:
  0.0 40.9 jit_solution(13451496437448097425)
XLA Ops:
  0.0 0.5 %collective-permute-start.5 = (f32[1,4,512,256]{3,2,1,0:T(8,128)}, f32[1,4,512,256]{3,2,1,0:T(8,128)S(1)}, u32[]{:S(2)}, u32[]{:S(2)}) collective-permute-start(f32[1,4,512,256]{3,2,1,0:T(8,128)} %param.26), channel_id=1, source_target_pairs={{0,1},{1,0},{2,3},{3,2},{4,5},{5,4},{6,7},{7,6},{8,9},{9,8},{10,11... | collective-permute-start | bytes 6291464 | tf_op jit(solution)/shard_map/ppermute | solution.py:672
  0.5 0.0 collective-permute-start.7
  0.5 0.0 copy-start.3
  0.5 4.5 %shard_map.181 = (f32[1,4224]{1,0:T(1,128)S(1)}, f32[1,4224]{1,0:T(1,128)S(1)}, f32[1,4224]{1,0:T(1,128)S(1)}, f32[1,4224]{1,0:T(1,128)S(1)}, f32[4,512]{1,0:T(4,128)S(1)}) custom-call(bf16[4,1024]{1,0:T(4,128)(2,1)} %tokens_hbm.1, f32[1,1024]{1,0:T(1,128)} %bitcast.15, bf16[1024,1024]{1,0:T(8,128)(2,1)} %q_hbm.1, bf16[1024,1024]{1,0:T(8,128)(2,1)} %k_hbm.1, ...), custom_call_target="tpu_custom_call" | custom-call | flops 20000000000 | bytes 1000000 | tf_op jit(solution)/shard_map/pallas_call | solution.py:245
  5.1 0.6 %collective-permute-start.4 = (f32[4,512]{1,0:T(4,128)S(1)}, f32[4,512]{1,0:T(4,128)S(1)}, u32[]{:S(2)}, u32[]{:S(2)}) collective-permute-start(f32[4,512]{1,0:T(4,128)S(1)} %get-tuple-element.21), channel_id=1, source_target_pairs={{0,1},{1,0},{2,3},{3,2},{4,5},{5,4},{6,7},{7,6},{8,9},{9,8},{10,11... | collective-permute-start | bytes 24584 | tf_op jit(solution)/shard_map/ppermute | solution.py:672
  5.6 0.0 copy-done.3
  5.6 0.1 collective-permute-start.6
  5.7 3.7 %collective-permute-start = (f32[1,4224]{1,0:T(1,128)S(1)}, f32[1,4224]{1,0:T(1,128)S(1)}, u32[]{:S(2)}, u32[]{:S(2)}) collective-permute-start(f32[1,4224]{1,0:T(1,128)S(1)} %get-tuple-element.17), channel_id=1, source_target_pairs={{0,5},{1,4},{2,7},{3,6},{4,1},{5,0},{6,3},{7,2},{8,13},{9,12},{10,... | collective-permute-start | bytes 50696 | tf_op jit(solution)/shard_map/ppermute | solution.py:667
  9.4 0.0 collective-permute-done.4.refs_4_
  9.4 1.7 %collective-permute-start.1 = (f32[1,4224]{1,0:T(1,128)S(1)}, f32[1,4224]{1,0:T(1,128)S(1)}, u32[]{:S(2)}, u32[]{:S(2)}) collective-permute-start(f32[1,4224]{1,0:T(1,128)S(1)} %get-tuple-element.18), channel_id=1, source_target_pairs={{0,7},{1,6},{2,5},{3,4},{4,3},{5,2},{6,1},{7,0},{8,15},{9,14},{10,... | collective-permute-start | bytes 50696 | tf_op jit(solution)/shard_map/ppermute | solution.py:667
  11.8 0.0 collective-permute-done.refs_0_
  11.8 0.7 %collective-permute-start.2 = (f32[1,4224]{1,0:T(1,128)S(1)}, f32[1,4224]{1,0:T(1,128)S(1)}, u32[]{:S(2)}, u32[]{:S(2)}) collective-permute-start(f32[1,4224]{1,0:T(1,128)S(1)} %get-tuple-element.19), channel_id=1, source_target_pairs={{0,3},{1,2},{2,1},{3,0},{4,7},{5,6},{6,5},{7,4},{8,11},{9,10},{10,... | collective-permute-start | bytes 50696 | tf_op jit(solution)/shard_map/ppermute | solution.py:667
  12.5 1.9 %collective-permute-done.1.refs_1_ = f32[1,4224]{1,0:T(1,128)S(1)} collective-permute-done((f32[1,4224]{1,0:T(1,128)S(1)}, f32[1,4224]{1,0:T(1,128)S(1)}, u32[]{:S(2)}, u32[]{:S(2)}) %collective-permute-start.1) | collective-permute-done | bytes 16928 | tf_op jit(solution)/shard_map/ppermute | solution.py:667
  14.4 0.4 %collective-permute-start.3 = (f32[1,4224]{1,0:T(1,128)S(1)}, f32[1,4224]{1,0:T(1,128)S(1)}, u32[]{:S(2)}, u32[]{:S(2)}) collective-permute-start(f32[1,4224]{1,0:T(1,128)S(1)} %get-tuple-element.20), channel_id=1, source_target_pairs={{0,1},{1,0},{2,3},{3,2},{4,5},{5,4},{6,7},{7,6},{8,9},{9,8},{10,11... | collective-permute-start | bytes 50696 | tf_op jit(solution)/shard_map/ppermute | solution.py:667
  14.8 0.0 copy-start
  14.8 0.3 collective-permute-done.2.refs_2_
  15.2 0.5 %collective-permute-done.3.refs_3_ = f32[1,4224]{1,0:T(1,128)S(1)} collective-permute-done((f32[1,4224]{1,0:T(1,128)S(1)}, f32[1,4224]{1,0:T(1,128)S(1)}, u32[]{:S(2)}, u32[]{:S(2)}) %collective-permute-start.3) | collective-permute-done | bytes 16928 | tf_op jit(solution)/shard_map/ppermute | solution.py:667
  15.6 0.0 collective-permute-done.6.refs_6_
  15.6 0.0 collective-permute-done.7.refs_7_
  15.6 0.0 collective-permute-done.5.refs_5_
  15.7 0.0 slice-start
  15.7 0.6 %shard_map.182 = bf16[4,512]{1,0:T(4,128)(2,1)S(1)} custom-call(f32[1,4224]{1,0:T(1,128)S(1)} %collective-permute-done.refs_0_, f32[1,4224]{1,0:T(1,128)S(1)} %collective-permute-done.1.refs_1_, f32[1,4224]{1,0:T(1,128)S(1)} %collective-permute-done.2.refs_2_, f32[1,4224]{1,0:T(1,128)S(1)} %collective-permute-done.3.refs_3_, ...), custom_call_target="tpu_custom_call" | custom-call | flops 20000000000 | bytes 1000000 | tf_op jit(solution)/shard_map/pallas_call | solution.py:245
  16.3 0.0 copy-start.2
  16.3 0.0 slice-start.1
  16.3 0.0 copy-start.1
  16.3 0.1 collective-permute-start.10
  16.4 0.4 collective-permute-start.11
  16.8 2.6 %collective-permute-start.8 = (bf16[4,512]{1,0:T(4,128)(2,1)S(1)}, bf16[4,512]{1,0:T(4,128)(2,1)S(1)}, u32[]{:S(2)}, u32[]{:S(2)}) collective-permute-start(bf16[4,512]{1,0:T(4,128)(2,1)S(1)} %shard_map.182), channel_id=1, source_target_pairs={{0,5},{1,4},{2,7},{3,6},{4,1},{5,0},{6,3},{7,2},{8,13},{9,12},{10,... | collective-permute-start | bytes 12296 | tf_op jit(solution)/shard_map/ppermute | solution.py:667
  19.4 1.2 %collective-permute-start.9 = (bf16[4,512]{1,0:T(4,128)(2,1)S(1)}, bf16[4,512]{1,0:T(4,128)(2,1)S(1)}, u32[]{:S(2)}, u32[]{:S(2)}) collective-permute-start(bf16[4,512]{1,0:T(4,128)(2,1)S(1)} %shard_map.182), channel_id=1, source_target_pairs={{0,7},{1,6},{2,5},{3,4},{4,3},{5,2},{6,1},{7,0},{8,15},{9,14},{10,... | collective-permute-start | bytes 12296 | tf_op jit(solution)/shard_map/ppermute | solution.py:667
  20.6 0.0 collective-permute-done.10.refs_2_
  20.6 0.0 collective-permute-done.11.refs_3_
  20.6 0.2 collective-permute-done.8.refs_0_
  20.8 3.5 %collective-permute-done.9.refs_1_ = bf16[4,512]{1,0:T(4,128)(2,1)S(1)} collective-permute-done((bf16[4,512]{1,0:T(4,128)(2,1)S(1)}, bf16[4,512]{1,0:T(4,128)(2,1)S(1)}, u32[]{:S(2)}, u32[]{:S(2)}) %collective-permute-start.9) | collective-permute-done | bytes 4128 | tf_op jit(solution)/shard_map/ppermute | solution.py:667
  24.3 0.0 copy-done
  24.3 0.0 slice-start.2
  24.3 0.6 %shard_map.183 = bf16[4,1024]{1,0:T(4,128)(2,1)S(1)} custom-call(bf16[4,512]{1,0:T(4,128)(2,1)S(1)} %collective-permute-done.8.refs_0_, bf16[4,512]{1,0:T(4,128)(2,1)S(1)} %collective-permute-done.9.refs_1_, bf16[4,512]{1,0:T(4,128)(2,1)S(1)} %collective-permute-done.10.refs_2_, bf16[4,512]{1,0:T(4,128)(2,1)S(1)} %collective-permute-done.11.refs_3_, ...), custom_call_target="tpu_custom_call" | custom-call | flops 20000000000 | bytes 1000000 | tf_op jit(solution)/shard_map/pallas_call | solution.py:245
  24.9 0.0 slice-start.3
  24.9 0.4 %collective-permute-start.12 = (bf16[4,1024]{1,0:T(4,128)(2,1)S(1)}, bf16[4,1024]{1,0:T(4,128)(2,1)S(1)}, u32[]{:S(2)}, u32[]{:S(2)}) collective-permute-start(bf16[4,1024]{1,0:T(4,128)(2,1)S(1)} %shard_map.183), channel_id=1, source_target_pairs={{0,1},{1,0},{2,3},{3,2},{4,5},{5,4},{6,7},{7,6},{8,9},{9,8},{10,11... | collective-permute-start | bytes 24584 | tf_op jit(solution)/shard_map/ppermute | solution.py:672
  25.3 0.8 %collective-permute-done.12 = bf16[4,1024]{1,0:T(4,128)(2,1)S(1)} collective-permute-done((bf16[4,1024]{1,0:T(4,128)(2,1)S(1)}, bf16[4,1024]{1,0:T(4,128)(2,1)S(1)}, u32[]{:S(2)}, u32[]{:S(2)}) %collective-permute-start.12) | collective-permute-done | bytes 8224 | tf_op jit(solution)/shard_map/ppermute | solution.py:672
  26.2 0.0 copy-done.2
  26.2 0.1 collective-permute-start.15
  26.3 1.2 %collective-permute-start.13 = (bf16[4,1024]{1,0:T(4,128)(2,1)S(1)}, bf16[4,1024]{1,0:T(4,128)(2,1)S(1)}, u32[]{:S(2)}, u32[]{:S(2)}) collective-permute-start(bf16[4,1024]{1,0:T(4,128)(2,1)S(1)} %add_convert_fusion.refs_0_.residual_ref), channel_id=1, source_target_pairs={{0,7},{1,6},{2,5},{3,4},{4,3},{5,2},{6,1},{7,0},{8,15},{9,14},{10,... | collective-permute-start | bytes 24584 | tf_op jit(solution)/shard_map/ppermute | solution.py:667
  27.4 2.0 %collective-permute-start.14 = (bf16[4,1024]{1,0:T(4,128)(2,1)S(1)}, bf16[4,1024]{1,0:T(4,128)(2,1)S(1)}, u32[]{:S(2)}, u32[]{:S(2)}) collective-permute-start(bf16[4,1024]{1,0:T(4,128)(2,1)S(1)} %add_convert_fusion.refs_0_.residual_ref), channel_id=1, source_target_pairs={{0,3},{1,2},{2,1},{3,0},{4,7},{5,6},{6,5},{7,4},{8,11},{9,10},{10,... | collective-permute-start | bytes 24584 | tf_op jit(solution)/shard_map/ppermute | solution.py:667
  29.4 0.8 %collective-permute-done.15.refs_1_ = bf16[4,1024]{1,0:T(4,128)(2,1)S(1)} collective-permute-done((bf16[4,1024]{1,0:T(4,128)(2,1)S(1)}, bf16[4,1024]{1,0:T(4,128)(2,1)S(1)}, u32[]{:S(2)}, u32[]{:S(2)}) %collective-permute-start.15) | collective-permute-done | bytes 8224 | tf_op jit(solution)/shard_map/ppermute | solution.py:667
  30.2 0.0 slice-done
  30.2 0.0 slice-done.1
  30.2 0.0 copy-done.1
  30.2 1.2 %shard_map.184 = (f32[4,1024]{1,0:T(4,128)S(1)}, f32[4,128]{1,0:T(4,128)S(1)}) custom-call(bf16[4,1024]{1,0:T(4,128)(2,1)S(1)} %add_convert_fusion.refs_0_.residual_ref, bf16[4,1024]{1,0:T(4,128)(2,1)S(1)} %collective-permute-done.15.refs_1_, f32[1,4096]{1,0:T(1,128)S(1)} %bitcast.12, bf16[1024,4096]{1,0:T(8,128)(2,1)S(1)} %bitcast.9), custom_call_target="tpu_custom_call" | custom-call | flops 20000000000 | bytes 1000000 | tf_op jit(solution)/shard_map/pallas_call | solution.py:245
  31.4 0.0 collective-permute-done.13.refs_0_
  31.4 0.0 collective-permute-done.14.refs_1_
  31.5 0.0 slice-done.2
  31.5 0.0 slice-done.3
  31.5 2.1 %shard_map.185 = (bf16[4,1024]{1,0:T(4,128)(2,1)S(1)}, bf16[4,1024]{1,0:T(4,128)(2,1)S(1)}, bf16[4,1024]{1,0:T(4,128)(2,1)S(1)}, bf16[4,1024]{1,0:T(4,128)(2,1)S(1)}, bf16[1024,1024]{1,0:T(8,128)(2,1)S(1)}) custom-call(bf16[4,1024]{1,0:T(4,128)(2,1)S(1)} %collective-permute-done.13.refs_0_, bf16[4,1024]{1,0:T(4,128)(2,1)S(1)} %collective-permute-done.14.refs_1_, ...), custom_call_target="tpu_custom_call" | custom-call | flops 20000000000 | bytes 1000000 | tf_op jit(solution)/shard_map/pallas_call | solution.py:245
  33.6 1.0 %collective-permute-start.16 = (bf16[4,1024]{1,0:T(4,128)(2,1)S(1)}, bf16[4,1024]{1,0:T(4,128)(2,1)S(1)}, u32[]{:S(2)}, u32[]{:S(2)}) collective-permute-start(bf16[4,1024]{1,0:T(4,128)(2,1)S(1)} %get-tuple-element.26), channel_id=1, source_target_pairs={{0,3},{1,2},{2,5},{3,4},{4,7},{5,6},{6,1},{7,0},{8,11},{9,10},{10,... | collective-permute-start | bytes 24584 | tf_op jit(solution)/shard_map/ppermute | solution.py:667
  34.6 1.0 %collective-permute-start.17 = (bf16[4,1024]{1,0:T(4,128)(2,1)S(1)}, bf16[4,1024]{1,0:T(4,128)(2,1)S(1)}, u32[]{:S(2)}, u32[]{:S(2)}) collective-permute-start(bf16[4,1024]{1,0:T(4,128)(2,1)S(1)} %get-tuple-element.27), channel_id=1, source_target_pairs={{0,5},{1,4},{2,7},{3,6},{4,1},{5,0},{6,3},{7,2},{8,13},{9,12},{10,... | collective-permute-start | bytes 24584 | tf_op jit(solution)/shard_map/ppermute | solution.py:667
  35.5 1.6 %collective-permute-start.18 = (bf16[4,1024]{1,0:T(4,128)(2,1)S(1)}, bf16[4,1024]{1,0:T(4,128)(2,1)S(1)}, u32[]{:S(2)}, u32[]{:S(2)}) collective-permute-start(bf16[4,1024]{1,0:T(4,128)(2,1)S(1)} %get-tuple-element.28), channel_id=1, source_target_pairs={{0,7},{1,6},{2,1},{3,0},{4,3},{5,2},{6,5},{7,4},{8,15},{9,14},{10,... | collective-permute-start | bytes 24584 | tf_op jit(solution)/shard_map/ppermute | solution.py:667
  37.1 0.4 shard_map.186
  37.5 0.9 %collective-permute-done.16 = bf16[4,1024]{1,0:T(4,128)(2,1)S(1)} collective-permute-done((bf16[4,1024]{1,0:T(4,128)(2,1)S(1)}, bf16[4,1024]{1,0:T(4,128)(2,1)S(1)}, u32[]{:S(2)}, u32[]{:S(2)}) %collective-permute-start.16) | collective-permute-done | bytes 8224 | tf_op jit(solution)/shard_map/ppermute | solution.py:667
  38.5 0.2 collective-permute-done.17
  38.6 0.4 %collective-permute-done.18 = bf16[4,1024]{1,0:T(4,128)(2,1)S(1)} collective-permute-done((bf16[4,1024]{1,0:T(4,128)(2,1)S(1)}, bf16[4,1024]{1,0:T(4,128)(2,1)S(1)}, u32[]{:S(2)}, u32[]{:S(2)}) %collective-permute-start.18) | collective-permute-done | bytes 8224 | tf_op jit(solution)/shard_map/ppermute | solution.py:667
  39.1 0.2 collective-permute-start.19
  39.3 1.1 %collective-permute-done.19 = f32[4,512]{1,0:T(4,128)S(1)} collective-permute-done((f32[4,512]{1,0:T(4,128)S(1)}, f32[4,512]{1,0:T(4,128)S(1)}, u32[]{:S(2)}, u32[]{:S(2)}) %collective-permute-start.19) | collective-permute-done | bytes 8224 | tf_op jit(solution)/shard_map/ppermute | solution.py:672
  40.3 0.6 %add_convert_fusion.1 = bf16[4,512]{1,0:T(4,128)(2,1)} fusion(f32[4,512]{1,0:T(4,128)S(1)} %collective-permute-done.19, f32[4,1024]{1,0:T(4,128)S(1)} %convert_add_fusion, s32[]{:T(128)S(6)} %select_n.6), kind=kLoop, calls=%fused_computation.2 | loop fusion | flops 4096 | bytes 20484 | tf_op jit(solution)/shard_map/convert_element_type | solution.py:751
  (6 shorter events, 0.0 us)
Async XLA Ops:
  0.0 15.7 %collective-permute-start.5 = (f32[1,4,512,256]{3,2,1,0:T(8,128)}, f32[1,4,512,256]{3,2,1,0:T(8,128)S(1)}, u32[]{:S(2)}, u32[]{:S(2)}) collective-permute-start(f32[1,4,512,256]{3,2,1,0:T(8,128)} %param.26), channel_id=1, source_target_pairs={{0,1},{1,0},{2,3},{3,2},{4,5},{5,4},{6,7},{7,6},{8,9},{9,8},{10,11... | collective-permute-start | bytes 6291464 | tf_op jit(solution)/shard_map/ppermute | solution.py:672
  0.5 15.2 %collective-permute-start.7 = (bf16[1,4,64,512]{3,2,1,0:T(8,128)(2,1)}, bf16[1,4,64,512]{3,2,1,0:T(8,128)(2,1)S(1)}, u32[]{:S(2)}, u32[]{:S(2)}) collective-permute-start(bf16[1,4,64,512]{3,2,1,0:T(8,128)(2,1)} %param.30), channel_id=1, source_target_pairs={{0,1},{1,0},{2,3},{3,2},{4,5},{5,4},{6,7},{7,6},{8,9},{9,8},{10,11... | collective-permute-start | bytes 786440 | tf_op jit(solution)/shard_map/ppermute | solution.py:672
  0.5 5.1 %copy-start.3 = (bf16[1,4,64,256]{3,2,1,0:T(8,128)(2,1)S(1)}, bf16[1,4,64,256]{3,2,1,0:T(8,128)(2,1)}, u32[]{:S(2)}) copy-start(bf16[1,4,64,256]{3,2,1,0:T(8,128)(2,1)} %param.29) | copy-start | bytes 393220
  5.1 4.3 %collective-permute-start.4 = (f32[4,512]{1,0:T(4,128)S(1)}, f32[4,512]{1,0:T(4,128)S(1)}, u32[]{:S(2)}, u32[]{:S(2)}) collective-permute-start(f32[4,512]{1,0:T(4,128)S(1)} %get-tuple-element.21), channel_id=1, source_target_pairs={{0,1},{1,0},{2,3},{3,2},{4,5},{5,4},{6,7},{7,6},{8,9},{9,8},{10,11... | collective-permute-start | bytes 24584 | tf_op jit(solution)/shard_map/ppermute | solution.py:672
  5.6 10.0 %collective-permute-start.6 = (bf16[1,4,64,256]{3,2,1,0:T(8,128)(2,1)S(1)}, bf16[1,4,64,256]{3,2,1,0:T(8,128)(2,1)S(1)}, u32[]{:S(2)}, u32[]{:S(2)}) collective-permute-start(bf16[1,4,64,256]{3,2,1,0:T(8,128)(2,1)S(1)} %copy-done.3), channel_id=1, source_target_pairs={{0,1},{1,0},{2,3},{3,2},{4,5},{5,4},{6,7},{7,6},{8,9},{9,8},{10,11... | collective-permute-start | bytes 393224 | tf_op jit(solution)/shard_map/ppermute | solution.py:672
  5.7 6.1 %collective-permute-start = (f32[1,4224]{1,0:T(1,128)S(1)}, f32[1,4224]{1,0:T(1,128)S(1)}, u32[]{:S(2)}, u32[]{:S(2)}) collective-permute-start(f32[1,4224]{1,0:T(1,128)S(1)} %get-tuple-element.17), channel_id=1, source_target_pairs={{0,5},{1,4},{2,7},{3,6},{4,1},{5,0},{6,3},{7,2},{8,13},{9,12},{10,... | collective-permute-start | bytes 50696 | tf_op jit(solution)/shard_map/ppermute | solution.py:667
  9.4 5.0 %collective-permute-start.1 = (f32[1,4224]{1,0:T(1,128)S(1)}, f32[1,4224]{1,0:T(1,128)S(1)}, u32[]{:S(2)}, u32[]{:S(2)}) collective-permute-start(f32[1,4224]{1,0:T(1,128)S(1)} %get-tuple-element.18), channel_id=1, source_target_pairs={{0,7},{1,6},{2,5},{3,4},{4,3},{5,2},{6,1},{7,0},{8,15},{9,14},{10,... | collective-permute-start | bytes 50696 | tf_op jit(solution)/shard_map/ppermute | solution.py:667
  11.8 3.3 %collective-permute-start.2 = (f32[1,4224]{1,0:T(1,128)S(1)}, f32[1,4224]{1,0:T(1,128)S(1)}, u32[]{:S(2)}, u32[]{:S(2)}) collective-permute-start(f32[1,4224]{1,0:T(1,128)S(1)} %get-tuple-element.19), channel_id=1, source_target_pairs={{0,3},{1,2},{2,1},{3,0},{4,7},{5,6},{6,5},{7,4},{8,11},{9,10},{10,... | collective-permute-start | bytes 50696 | tf_op jit(solution)/shard_map/ppermute | solution.py:667
  14.4 1.3 %collective-permute-start.3 = (f32[1,4224]{1,0:T(1,128)S(1)}, f32[1,4224]{1,0:T(1,128)S(1)}, u32[]{:S(2)}, u32[]{:S(2)}) collective-permute-start(f32[1,4224]{1,0:T(1,128)S(1)} %get-tuple-element.20), channel_id=1, source_target_pairs={{0,1},{1,0},{2,3},{3,2},{4,5},{5,4},{6,7},{7,6},{8,9},{9,8},{10,11... | collective-permute-start | bytes 50696 | tf_op jit(solution)/shard_map/ppermute | solution.py:667
  14.8 9.5 %copy-start = (bf16[2048,1024]{1,0:T(8,128)(2,1)S(1)}, bf16[2048,1024]{1,0:T(8,128)(2,1)}, u32[]{:S(2)}) copy-start(bf16[2048,1024]{1,0:T(8,128)(2,1)} %refs_4_.1) | copy-start | bytes 12582916
  15.7 14.6 %slice-start = ((s8[8388608]{0:T(1024)(128)(4,1)}), s8[4194304]{0:T(1024)(128)(4,1)S(1)}, s32[]{:S(2)}) async-start(s8[8388608]{0:T(1024)(128)(4,1)} %bitcast.8), calls=%async_computation | async-start | bytes 8388608
  16.3 9.9 %copy-start.2 = (bf16[4,1024]{1,0:T(4,128)(2,1)S(1)}, bf16[4,1024]{1,0:T(4,128)(2,1)}, u32[]{:S(2)}) copy-start(bf16[4,1024]{1,0:T(4,128)(2,1)} %tokens_hbm.1) | copy-start | bytes 24580
  16.3 13.9 %slice-start.1 = ((s8[8388608]{0:T(1024)(128)(4,1)}), s8[4194304]{0:T(1024)(128)(4,1)S(1)}, s32[]{:S(2)}) async-start(s8[8388608]{0:T(1024)(128)(4,1)} %bitcast.8), calls=%async_computation.1 | async-start | bytes 8388608
  16.3 13.9 %copy-start.1 = (f32[4096]{0:T(1024)S(1)}, f32[4096]{0:T(1024)}, u32[]{:S(2)}) copy-start(f32[4096]{0:T(1024)} %param.35) | copy-start | bytes 49156
  16.3 4.3 %collective-permute-start.10 = (bf16[4,512]{1,0:T(4,128)(2,1)S(1)}, bf16[4,512]{1,0:T(4,128)(2,1)S(1)}, u32[]{:S(2)}, u32[]{:S(2)}) collective-permute-start(bf16[4,512]{1,0:T(4,128)(2,1)S(1)} %shard_map.182), channel_id=1, source_target_pairs={{0,3},{1,2},{2,1},{3,0},{4,7},{5,6},{6,5},{7,4},{8,11},{9,10},{10,... | collective-permute-start | bytes 12296 | tf_op jit(solution)/shard_map/ppermute | solution.py:667
  16.4 4.2 %collective-permute-start.11 = (bf16[4,512]{1,0:T(4,128)(2,1)S(1)}, bf16[4,512]{1,0:T(4,128)(2,1)S(1)}, u32[]{:S(2)}, u32[]{:S(2)}) collective-permute-start(bf16[4,512]{1,0:T(4,128)(2,1)S(1)} %shard_map.182), channel_id=1, source_target_pairs={{0,1},{1,0},{2,3},{3,2},{4,5},{5,4},{6,7},{7,6},{8,9},{9,8},{10,11... | collective-permute-start | bytes 12296 | tf_op jit(solution)/shard_map/ppermute | solution.py:667
  16.8 4.0 %collective-permute-start.8 = (bf16[4,512]{1,0:T(4,128)(2,1)S(1)}, bf16[4,512]{1,0:T(4,128)(2,1)S(1)}, u32[]{:S(2)}, u32[]{:S(2)}) collective-permute-start(bf16[4,512]{1,0:T(4,128)(2,1)S(1)} %shard_map.182), channel_id=1, source_target_pairs={{0,5},{1,4},{2,7},{3,6},{4,1},{5,0},{6,3},{7,2},{8,13},{9,12},{10,... | collective-permute-start | bytes 12296 | tf_op jit(solution)/shard_map/ppermute | solution.py:667
  19.4 4.8 %collective-permute-start.9 = (bf16[4,512]{1,0:T(4,128)(2,1)S(1)}, bf16[4,512]{1,0:T(4,128)(2,1)S(1)}, u32[]{:S(2)}, u32[]{:S(2)}) collective-permute-start(bf16[4,512]{1,0:T(4,128)(2,1)S(1)} %shard_map.182), channel_id=1, source_target_pairs={{0,7},{1,6},{2,5},{3,4},{4,3},{5,2},{6,1},{7,0},{8,15},{9,14},{10,... | collective-permute-start | bytes 12296 | tf_op jit(solution)/shard_map/ppermute | solution.py:667
  24.3 7.2 %slice-start.2 = ((s8[8388608]{0:T(1024)(128)(4,1)}), s8[4194304]{0:T(1024)(128)(4,1)S(1)}, s32[]{:S(2)}) async-start(s8[8388608]{0:T(1024)(128)(4,1)} %bitcast.10), calls=%async_computation.2 | async-start | bytes 8388608
  24.9 6.6 %slice-start.3 = ((s8[8388608]{0:T(1024)(128)(4,1)}), s8[4194304]{0:T(1024)(128)(4,1)S(1)}, s32[]{:S(2)}) async-start(s8[8388608]{0:T(1024)(128)(4,1)} %bitcast.10), calls=%async_computation.3 | async-start | bytes 8388608
  24.9 1.2 %collective-permute-start.12 = (bf16[4,1024]{1,0:T(4,128)(2,1)S(1)}, bf16[4,1024]{1,0:T(4,128)(2,1)S(1)}, u32[]{:S(2)}, u32[]{:S(2)}) collective-permute-start(bf16[4,1024]{1,0:T(4,128)(2,1)S(1)} %shard_map.183), channel_id=1, source_target_pairs={{0,1},{1,0},{2,3},{3,2},{4,5},{5,4},{6,7},{7,6},{8,9},{9,8},{10,11... | collective-permute-start | bytes 24584 | tf_op jit(solution)/shard_map/ppermute | solution.py:672
  26.2 4.0 %collective-permute-start.15 = (bf16[4,1024]{1,0:T(4,128)(2,1)S(1)}, bf16[4,1024]{1,0:T(4,128)(2,1)S(1)}, u32[]{:S(2)}, u32[]{:S(2)}) collective-permute-start(bf16[4,1024]{1,0:T(4,128)(2,1)S(1)} %add_convert_fusion.refs_0_.residual_ref), channel_id=1, source_target_pairs={{0,5},{1,4},{2,7},{3,6},{4,1},{5,0},{6,3},{7,2},{8,13},{9,12},{10,... | collective-permute-start | bytes 24584 | tf_op jit(solution)/shard_map/ppermute | solution.py:667
  26.3 5.2 %collective-permute-start.13 = (bf16[4,1024]{1,0:T(4,128)(2,1)S(1)}, bf16[4,1024]{1,0:T(4,128)(2,1)S(1)}, u32[]{:S(2)}, u32[]{:S(2)}) collective-permute-start(bf16[4,1024]{1,0:T(4,128)(2,1)S(1)} %add_convert_fusion.refs_0_.residual_ref), channel_id=1, source_target_pairs={{0,7},{1,6},{2,5},{3,4},{4,3},{5,2},{6,1},{7,0},{8,15},{9,14},{10,... | collective-permute-start | bytes 24584 | tf_op jit(solution)/shard_map/ppermute | solution.py:667
  27.4 4.0 %collective-permute-start.14 = (bf16[4,1024]{1,0:T(4,128)(2,1)S(1)}, bf16[4,1024]{1,0:T(4,128)(2,1)S(1)}, u32[]{:S(2)}, u32[]{:S(2)}) collective-permute-start(bf16[4,1024]{1,0:T(4,128)(2,1)S(1)} %add_convert_fusion.refs_0_.residual_ref), channel_id=1, source_target_pairs={{0,3},{1,2},{2,1},{3,0},{4,7},{5,6},{6,5},{7,4},{8,11},{9,10},{10,... | collective-permute-start | bytes 24584 | tf_op jit(solution)/shard_map/ppermute | solution.py:667
  33.6 4.9 %collective-permute-start.16 = (bf16[4,1024]{1,0:T(4,128)(2,1)S(1)}, bf16[4,1024]{1,0:T(4,128)(2,1)S(1)}, u32[]{:S(2)}, u32[]{:S(2)}) collective-permute-start(bf16[4,1024]{1,0:T(4,128)(2,1)S(1)} %get-tuple-element.26), channel_id=1, source_target_pairs={{0,3},{1,2},{2,5},{3,4},{4,7},{5,6},{6,1},{7,0},{8,11},{9,10},{10,... | collective-permute-start | bytes 24584 | tf_op jit(solution)/shard_map/ppermute | solution.py:667
  34.6 4.1 %collective-permute-start.17 = (bf16[4,1024]{1,0:T(4,128)(2,1)S(1)}, bf16[4,1024]{1,0:T(4,128)(2,1)S(1)}, u32[]{:S(2)}, u32[]{:S(2)}) collective-permute-start(bf16[4,1024]{1,0:T(4,128)(2,1)S(1)} %get-tuple-element.27), channel_id=1, source_target_pairs={{0,5},{1,4},{2,7},{3,6},{4,1},{5,0},{6,3},{7,2},{8,13},{9,12},{10,... | collective-permute-start | bytes 24584 | tf_op jit(solution)/shard_map/ppermute | solution.py:667
  35.5 3.5 %collective-permute-start.18 = (bf16[4,1024]{1,0:T(4,128)(2,1)S(1)}, bf16[4,1024]{1,0:T(4,128)(2,1)S(1)}, u32[]{:S(2)}, u32[]{:S(2)}) collective-permute-start(bf16[4,1024]{1,0:T(4,128)(2,1)S(1)} %get-tuple-element.28), channel_id=1, source_target_pairs={{0,7},{1,6},{2,1},{3,0},{4,3},{5,2},{6,5},{7,4},{8,15},{9,14},{10,... | collective-permute-start | bytes 24584 | tf_op jit(solution)/shard_map/ppermute | solution.py:667
  39.1 1.2 %collective-permute-start.19 = (f32[4,512]{1,0:T(4,128)S(1)}, f32[4,512]{1,0:T(4,128)S(1)}, u32[]{:S(2)}, u32[]{:S(2)}) collective-permute-start(f32[4,512]{1,0:T(4,128)S(1)} %constant_dynamic-slice_fusion), channel_id=1, source_target_pairs={{0,1},{1,0},{2,3},{3,2},{4,5},{5,4},{6,7},{7,6},{8,9},{9,8},{10,11... | collective-permute-start | bytes 24584 | tf_op jit(solution)/shard_map/ppermute | solution.py:672
